TPU v7x, 32 devices: a whole 2x2x4 slice. The times are simulated.
32 devices in a mesh: sp: 8 (over z, y), tp: 4 (over x, core).
Axes of the slice: x: 2, y: 2, z: 4, core: 2. Of those that a mesh axis runs over, the one named last changes fastest.
Arguments:
- target: bfloat16 [56, 2048], P('sp'), may hold values from -6 to 6
- source: bfloat16 [2048, 2048], P('sp'), may hold values from -6 to 6
- tgt_gain: float32 [2, 2048], replicated, may hold values from 0.1 to 1.9
- src_gain: float32 [2, 2048], replicated, may hold values from 0.1 to 1.9
- w_query: bfloat16 [2, 2048, 2048], P(None, None, 'tp'), may hold values from -0.125 to 0.125
- w_key: bfloat16 [2, 2048, 2048], P(None, None, 'tp'), may hold values from -0.125 to 0.125
- w_value: bfloat16 [2, 2048, 2048], P(None, None, 'tp'), may hold values from -0.125 to 0.125
- w_out: bfloat16 [2, 2048, 2048], P(None, 'tp'), may hold values from -0.125 to 0.125
- score_scale: float32 [2, 8], P(None, 'tp'), may hold values from 1.5 to 4
Outputs:
- result: bfloat16 [56, 2048], P('sp')
All inputs are finite; a program needn't handle non-finite values.
Results may differ from a plain program's by a relative error of at most 0.015.
Values may be sent and summed in bfloat16 or wider, within the bound.
No kernel may reach another device: no remote copies, remote signals or barrier semaphores. Data moves between devices by JAX's collectives and lax.ppermute only.
A program may use at most 64 MiB of HBM per device.

v0:
```python
import math

import jax
import jax.numpy as jnp
from jax import lax
from jax.sharding import PartitionSpec as P

HEAD_DIM = 256


EPS = 1e-06


def row_scale(values):
    return lax.rsqrt(jnp.mean(values * values, axis=-1, keepdims=True) + EPS)


def head_norm(projected):
    heads = projected.reshape(projected.shape[0], -1, HEAD_DIM)
    heads = heads * row_scale(heads)
    return heads.reshape(projected.shape).astype(jnp.bfloat16)


def source_side(src_float, src_scale, gain_row, key_weight, value_weight):
    normed_src = (src_float * src_scale * gain_row).astype(jnp.bfloat16)
    key_rows = head_norm(jnp.dot(normed_src, key_weight, preferred_element_type=jnp.float32))
    value_rows = jnp.dot(normed_src, value_weight, preferred_element_type=jnp.float32).astype(
        jnp.bfloat16
    )
    return (key_rows, value_rows)


def attend(queries, key_rows, value_rows, scales):
    root = math.sqrt(HEAD_DIM)
    count = queries.shape[0]
    local_heads = scales.shape[0]
    query_heads = queries.reshape(count, local_heads, HEAD_DIM)
    key_heads = key_rows.reshape(key_rows.shape[0], local_heads, HEAD_DIM)
    value_heads = value_rows.reshape(value_rows.shape[0], local_heads, HEAD_DIM)
    scores = jnp.einsum("qhd,khd->hqk", query_heads, key_heads, preferred_element_type=jnp.float32)
    logits = scales[:, None, None] * (scores / root - root)
    weights = jnp.exp(logits)
    denominators = jnp.sum(weights, axis=2).T
    numerators = jnp.einsum(
        "hqk,khd->qhd",
        weights.astype(jnp.bfloat16),
        value_heads,
        preferred_element_type=jnp.float32,
    )
    return (numerators.reshape(count, local_heads * HEAD_DIM), denominators)


def place(terms):
    numer_all = terms[0]
    denom_all = terms[1]
    return (numer_all, denom_all)


def body(target, source, tgt_gain, src_gain, w_query, w_key, w_value, w_out, score_scale):
    local_heads = w_query.shape[2] // HEAD_DIM
    width = local_heads * HEAD_DIM
    tok_rows = target.shape[0]
    layer_count = w_query.shape[0]
    src_float = source.astype(jnp.float32)
    src_scale = row_scale(src_float)
    hidden = target
    for layer_index in range(layer_count):
        key_rows, value_rows = source_side(
            src_float, src_scale, src_gain[layer_index], w_key[layer_index], w_value[layer_index]
        )
        scales = score_scale[layer_index]
        hidden_float = hidden.astype(jnp.float32)
        normed_tgt = (hidden_float * row_scale(hidden_float) * tgt_gain[layer_index]).astype(
            jnp.bfloat16
        )
        weight_now = w_query[layer_index]
        query_rows = head_norm(jnp.dot(normed_tgt, weight_now, preferred_element_type=jnp.float32))
        running = place(
            attend(
                lax.all_gather(query_rows, "sp", axis=0, tiled=True), key_rows, value_rows, scales
            )
        )
        numerators, denominators = (
            lax.psum_scatter(running[0], "sp", scatter_dimension=0, tiled=True),
            lax.psum_scatter(running[1], "sp", scatter_dimension=0, tiled=True),
        )
        attended = (
            (numerators.reshape(tok_rows, local_heads, HEAD_DIM) / denominators[:, :, None])
            .reshape(tok_rows, width)
            .astype(jnp.bfloat16)
        )
        share = jnp.dot(attended, w_out[layer_index], preferred_element_type=jnp.float32).astype(
            jnp.bfloat16
        )
        branch = lax.psum(share.astype(jnp.float32).astype(jnp.bfloat16), "tp").astype(jnp.float32)
        hidden = (hidden_float + branch).astype(jnp.bfloat16)
    return hidden


def solution(mesh):
    placed = (
        P("sp", None),
        P("sp", None),
        P(),
        P(),
        P(None, None, "tp"),
        P(None, None, "tp"),
        P(None, None, "tp"),
        P(None, "tp", None),
        P(None, "tp"),
    )
    return jax.shard_map(body, mesh=mesh, in_specs=placed, out_specs=P("sp", None), check_vma=False)
```

profile of v0, /device:TPU:0, one launch (start us, length us, event | category | flops | bytes accessed | tf_op | source)
XLA Modules:
  0.0 235.5 jit_solution(8419340724434277195)
XLA Ops:
  0.0 1.5 fusion.6
  1.5 0.8 fusion.73
  2.3 3.8 %slice_bitcast_fusion.2 = (bf16[512,2048]{0,1:T(8,128)(2,1)S(1)}, bf16[512,2048]{0,1:T(8,128)(2,1)}) fusion(bf16[2,2048,512]{2,1,0:T(8,128)(2,1)} %param.14), kind=kLoop, calls=%fused_computation.20 | loop fusion | bytes 8388608 | tf_op jit(solution)/shard_map/dot_general | solution.py:26
  6.2 2.5 %copy.31 = bf16[512,2048]{1,0:T(8,128)(2,1)} copy(bf16[512,2048]{0,1:T(8,128)(2,1)S(1)} %get-tuple-element.7) | data formatting | bytes 4194304 | tf_op jit(solution)/shard_map/dot_general | solution.py:26
  8.6 3.4 %multiply_reduce_fusion.1 = (f32[256,2]{0,1:T(2,128)S(1)}, f32[256,2,256]{0,2,1:T(8,128)}) fusion(bf16[2,256,2048]{2,1,0:T(8,128)(2,1)} %bitcast.104, f32[2048]{0:T(1024)S(1)} %bitcast.117, f32[256]{0:T(256)S(1)} %add_rsqrt_fusion.4, bf16[256,2048]{1,0:T(8,128)(2,1)S(1)} %copy-done.3), kind=kOutput, calls=%fused_computation.42 | convolution fusion | flops 539229696 | bytes 3681280 | tf_op jit(solution)/shard_map/dot_general | solution.py:26
  12.0 2.3 slice_bitcast_fusion.3
  14.3 2.9 %copy.30 = bf16[512,2048]{1,0:T(8,128)(2,1)S(1)} copy(bf16[512,2048]{0,1:T(8,128)(2,1)} %get-tuple-element.5) | data formatting | bytes 4194304 | tf_op jit(solution)/shard_map/dot_general | solution.py:77
  17.5 0.7 multiply_reduce_fusion.3
  18.3 32.4 %all-gather = bf16[8,7,512]{2,1,0:T(8,128)(2,1)S(1)} all-gather(bf16[1,7,512]{2,1,0:T(8,128)(2,1)S(1)} %bitcast.113), channel_id=1, replica_groups=mesh['sp'=8,'tp'=4] {'sp'}, dimensions={0}, use_global_device_ids=true | all-gather | bytes 64512 | tf_op jit(solution)/shard_map/all_gather | solution.py:80
  50.7 2.5 %fusion.17 = bf16[256,512]{1,0:T(8,128)(2,1)S(1)} fusion(bf16[2,2048,512]{2,1,0:T(8,128)(2,1)} %param.15, bf16[256,2048]{1,0:T(8,128)(2,1)S(1)} %copy-done.3, f32[2048]{0:T(1024)S(1)} %bitcast.118, f32[256]{0:T(256)S(1)} %add_rsqrt_fusion.4), kind=kOutput, calls=%fused_computation.23 | convolution fusion | flops 539099136 | bytes 3417088 | tf_op jit(solution)/shard_map/dot_general | solution.py:27
  53.2 0.3 fusion.75
  53.5 0.2 convolution_bitcast_fusion.1
  53.7 22.6 %fusion = f32[8,512]{1,0:T(8,128)S(1)} fusion(f32[56,512]{1,0:T(8,128)S(1)} %bitcast.105), kind=kCustom, calls=%all-reduce-scatter | all-reduce-scatter fusion | flops 32769 | bytes 131584
  76.3 1.3 collective-permute-start
  77.7 33.7 %all-reduce.1 = f32[56,2]{1,0:T(8,128)S(1)} all-reduce(f32[56,2]{1,0:T(8,128)S(1)} %copy.36), channel_id=3, replica_groups=mesh['sp'=8,'tp'=4] {'sp'}, use_global_device_ids=true, to_apply=%region_6.0.clone | all-reduce | flops 112 | bytes 896
  111.4 0.6 fusion.74
  112.7 2.5 %copy.38 = bf16[512,2048]{1,0:T(8,128)(2,1)} copy(bf16[512,2048]{0,1:T(8,128)(2,1)S(1)} %copy-done) | data formatting | bytes 4194304 | tf_op jit(solution)/shard_map/dot_general | solution.py:26
  115.2 2.5 %fusion.20 = bf16[256,512]{1,0:T(8,128)(2,1)S(1)} fusion(bf16[2,2048,512]{2,1,0:T(8,128)(2,1)} %param.15, bf16[256,2048]{1,0:T(8,128)(2,1)S(1)} %copy-done.3, f32[2048]{0:T(1024)S(1)} %bitcast.115, f32[256]{0:T(256)S(1)} %add_rsqrt_fusion.4), kind=kOutput, calls=%fused_computation.24 | convolution fusion | flops 539099136 | bytes 3417088 | tf_op jit(solution)/shard_map/dot_general | solution.py:27
  117.7 1.6 multiply_reduce_fusion
  120.0 2.9 %copy.37 = bf16[512,2048]{1,0:T(8,128)(2,1)S(1)} copy(bf16[512,2048]{0,1:T(8,128)(2,1)} %get-tuple-element.6) | data formatting | bytes 4194304 | tf_op jit(solution)/shard_map/dot_general | solution.py:77
  123.1 2.0 convolution_convert_fusion.1
  125.1 10.3 %psum.14 = bf16[7,2048]{1,0:T(8,128)(2,1)S(1)} all-reduce(bf16[7,2048]{1,0:T(8,128)(2,1)S(1)} %convolution_convert_fusion.1), channel_id=1, replica_groups=mesh['sp'=8,'tp'=4] {'tp'}, use_global_device_ids=true, to_apply=%region_7.0 | all-reduce | flops 14336 | bytes 57344 | tf_op jit(solution)/shard_map/psum | solution.py:95
  135.5 0.7 multiply_reduce_fusion.2
  136.3 30.5 %all-gather.1 = bf16[8,7,512]{2,1,0:T(8,128)(2,1)S(1)} all-gather(bf16[1,7,512]{2,1,0:T(8,128)(2,1)S(1)} %bitcast.114), channel_id=1, replica_groups=mesh['sp'=8,'tp'=4] {'sp'}, dimensions={0}, use_global_device_ids=true | all-gather | bytes 64512 | tf_op jit(solution)/shard_map/all_gather | solution.py:80
  166.9 0.3 fusion.76
  167.2 0.2 convolution_bitcast_fusion
  167.4 19.9 %fusion.1 = f32[8,512]{1,0:T(8,128)S(1)} fusion(f32[56,512]{1,0:T(8,128)S(1)} %bitcast.106), kind=kCustom, calls=%all-reduce-scatter.1 | all-reduce-scatter fusion | flops 32769 | bytes 131584
  187.3 1.9 collective-permute-start.1
  189.3 33.1 %all-reduce.3 = f32[56,2]{1,0:T(8,128)S(1)} all-reduce(f32[56,2]{1,0:T(8,128)S(1)} %copy.43), channel_id=5, replica_groups=mesh['sp'=8,'tp'=4] {'sp'}, use_global_device_ids=true, to_apply=%region_13.0.clone | all-reduce | flops 112 | bytes 896
  222.6 2.0 convolution_convert_fusion
  224.6 10.3 %psum.15 = bf16[7,2048]{1,0:T(8,128)(2,1)S(1)} all-reduce(bf16[7,2048]{1,0:T(8,128)(2,1)S(1)} %convolution_convert_fusion), channel_id=1, replica_groups=mesh['sp'=8,'tp'=4] {'tp'}, use_global_device_ids=true, to_apply=%region_14.0 | all-reduce | flops 14336 | bytes 57344 | tf_op jit(solution)/shard_map/psum | solution.py:95
  234.9 0.6 fusion.50
  (51 shorter events, 1.2 us)
Async XLA Ops:
  6.2 2.5 %copy-start.3 = (bf16[256,2048]{1,0:T(8,128)(2,1)S(1)}, bf16[256,2048]{1,0:T(8,128)(2,1)}, u32[]{:S(2)}) copy-start(bf16[256,2048]{1,0:T(8,128)(2,1)} %param.10) | copy-start | bytes 3145732
  8.6 3.4 %copy-start.1 = (bf16[2,2048,512]{2,1,0:T(8,128)(2,1)S(1)}, bf16[2,2048,512]{2,1,0:T(8,128)(2,1)}, u32[]{:S(2)}) copy-start(bf16[2,2048,512]{2,1,0:T(8,128)(2,1)} %param.13) | copy-start | bytes 12582916
  14.3 3.0 %copy-start.7 = (f32[2,2048]{1,0:T(2,128)S(1)}, f32[2,2048]{1,0:T(2,128)}, u32[]{:S(2)}) copy-start(f32[2,2048]{1,0:T(2,128)} %param.11) | copy-start | bytes 49156
  14.3 3.0 %copy-start.4 = (bf16[7,2048]{1,0:T(8,128)(2,1)S(1)}, bf16[7,2048]{1,0:T(8,128)(2,1)}, u32[]{:S(2)}) copy-start(bf16[7,2048]{1,0:T(8,128)(2,1)} %param.9) | copy-start | bytes 86020
  17.3 33.4 %copy-start.9 = (f32[2,2]{1,0:T(2,128)S(1)}, f32[2,2]{1,0:T(2,128)}, u32[]{:S(2)}) copy-start(f32[2,2]{1,0:T(2,128)} %param.17) | copy-start | bytes 52
  50.7 2.5 %copy-start.6 = (f32[256,2,256]{0,2,1:T(8,128)S(1)}, f32[256,2,256]{0,2,1:T(8,128)}, u32[]{:S(2)}) copy-start(f32[256,2,256]{0,2,1:T(8,128)} %get-tuple-element.20) | copy-start | bytes 1572868
  50.7 60.7 %copy-start.8 = (u32[32]{0:T(128)S(1)}, u32[32]{0:T(128)}, u32[]{:S(2)}) copy-start(u32[32]{0:T(128)} %constant.31) | copy-start | bytes 388
  50.7 62.0 %copy-start = (bf16[512,2048]{0,1:T(8,128)(2,1)S(1)}, bf16[512,2048]{0,1:T(8,128)(2,1)}, u32[]{:S(2)}) copy-start(bf16[512,2048]{0,1:T(8,128)(2,1)} %get-tuple-element.8) | copy-start | bytes 6291460
  76.3 46.7 %collective-permute-start = (f32[7,512]{1,0:T(8,128)S(1)}, f32[7,512]{1,0:T(8,128)S(1)}, u32[]{:S(2)}, u32[]{:S(2)}) collective-permute-start(f32[7,512]{1,0:T(8,128)S(1)} %slice.56), channel_id=1, source_target_pairs={{0,4},{4,8},{8,12},{12,16},{16,20},{20,24},{24,28},{1,5},{5,9},{9,... | collective-permute-start | bytes 43016
  115.2 2.5 %copy-start.2 = (bf16[512,2048]{1,0:T(8,128)(2,1)S(1)}, bf16[512,2048]{1,0:T(8,128)(2,1)}, u32[]{:S(2)}) copy-start(bf16[512,2048]{1,0:T(8,128)(2,1)} %copy.38) | copy-start | bytes 6291460
  123.1 43.9 %copy-start.5 = (f32[256,2,256]{0,2,1:T(8,128)S(1)}, f32[256,2,256]{0,2,1:T(8,128)}, u32[]{:S(2)}) copy-start(f32[256,2,256]{0,2,1:T(8,128)} %get-tuple-element.18) | copy-start | bytes 1572868
  187.3 35.2 %collective-permute-start.1 = (f32[7,512]{1,0:T(8,128)S(1)}, f32[7,512]{1,0:T(8,128)S(1)}, u32[]{:S(2)}, u32[]{:S(2)}) collective-permute-start(f32[7,512]{1,0:T(8,128)S(1)} %slice.57), channel_id=1, source_target_pairs={{0,4},{4,8},{8,12},{12,16},{16,20},{20,24},{24,28},{1,5},{5,9},{9,... | collective-permute-start | bytes 43016
where the time goes:
time: 236 us; the launch traced here: 235 us
  blocking collectives  193 us (82%)
  local copies, waits for them, and re-layouts  19.1 us (8%)
  matrix products  16.3 us (7%)
  starting transfers between devices  3.19 us (1%)
  other arithmetic  2.62 us (1%)
    unnamed x4, blocking collectives  109 us
    all_gather x2, blocking collectives, body(): lax.all_gather(query_rows, 'sp', axis=0, tiled=True)  62.9 us
    psum x2, blocking collectives, body(): lax.psum(share.astype(jnp.float32).astype(jnp.bfloat16), 'tp')  20.5 us
    dot_general x3, local copies, waits for them, and re-layouts, source_side(): jnp.dot(normed_src, key_weight, preferred_element_type=jnp.float32)  8.79 us
    dot_general x3, local copies, waits for them, and re-layouts, body(): jnp.dot(normed_tgt, weight_now, preferred_element_type=jnp.float32)  8.14 us
    dot_general x2, matrix products, source_side(): jnp.dot(normed_src, key_weight, preferred_element_type=jnp.float32)  4.99 us
    dot_general x2, matrix products, source_side(): jnp.dot(normed_src, value_weight, preferred_element_type=jnp.float32)  4.98 us
  transfers between devices with their start and end apart: 2, of which 0 were waited for; matrix products, arithmetic and copies ran while one was open for 4% of the time, Pallas kernels for 0%

commit v1 on v0

v1 whole, which is shorter than its diff:
```python
import functools
import math

import jax
import jax.numpy as jnp
from jax import lax
from jax.experimental import pallas as pl
from jax.experimental.pallas import tpu as pltpu
from jax.sharding import PartitionSpec as P

HEAD_DIM = 256
EPS = 1e-06
LANES = 128
SUBLANES = 8
VMEM = pltpu.VMEM


def whole(shape):
    return pl.BlockSpec(shape, lambda *_: (0,) * len(shape))


def layer_of(shape, layer):
    return pl.BlockSpec((1, *shape[1:]), lambda *_: (layer,) + (0,) * (len(shape) - 1))


def row_scale(values):
    return lax.rsqrt(jnp.mean(values * values, axis=-1, keepdims=True) + EPS)


def cost(flops, moved):
    return pl.CostEstimate(flops=flops, bytes_accessed=moved, transcendentals=0)


def source_kernel(source, gain, w_key, w_value, keys, values, normed):
    @pl.when(pl.program_id(1) == 0)
    def _():
        rows = source[...].astype(jnp.float32)
        gains = gain[pl.ds(pl.program_id(0), 1), :]
        normed[...] = (rows * row_scale(rows) * gains).astype(jnp.bfloat16)

    key = jnp.dot(normed[...], w_key[0], preferred_element_type=jnp.float32)
    keys[0] = (key * row_scale(key)).astype(jnp.bfloat16)
    value = jnp.dot(normed[...], w_value[0], preferred_element_type=jnp.float32)
    values[0] = value.astype(jnp.bfloat16)


def source_side(source, gain, w_key, w_value):
    layers, width, columns = w_key.shape
    rows = source.shape[0]
    weight = pl.BlockSpec((1, width, HEAD_DIM), lambda l, h: (l, 0, h))
    out = pl.BlockSpec((1, rows, HEAD_DIM), lambda l, h: (l, 0, h))
    shape = jax.ShapeDtypeStruct((layers, rows, columns), jnp.bfloat16)
    return pl.pallas_call(
        source_kernel,
        grid=(layers, columns // HEAD_DIM),
        in_specs=[whole(source.shape), whole(gain.shape), weight, weight],
        out_specs=[out, out],
        out_shape=[shape, shape],
        scratch_shapes=[VMEM((rows, width), jnp.bfloat16)],
        cost_estimate=cost(4 * layers * rows * width * columns, 4 * layers * width * columns),
        name="source_side",
    )(source, gain, w_key, w_value)


def project(hidden, gains, weight, queries):
    normed = (hidden * row_scale(hidden) * gains).astype(jnp.bfloat16)
    raw = jnp.dot(normed, weight, preferred_element_type=jnp.float32)
    rows, columns = raw.shape
    for start in range(0, columns, HEAD_DIM):
        head = raw[:, start : start + HEAD_DIM]
        head = (head * row_scale(head)).astype(jnp.bfloat16)
        queries[:, :rows, start : start + HEAD_DIM] = jnp.broadcast_to(
            head[None], (queries.shape[0], rows, HEAD_DIM)
        )
    if rows < queries.shape[1]:
        queries[:, rows:, :] = jnp.zeros(
            (queries.shape[0], queries.shape[1] - rows, columns), jnp.bfloat16
        )


def first_kernel(layer, hidden, gain, w_query, queries):
    project(
        hidden[...].astype(jnp.float32), gain[layer : layer + 1, :], w_query[0], queries
    )


def next_kernel(layer, hidden, shares, gain, w_query, queries, result):
    rows = hidden.shape[0]
    branch = shares[0, :rows, :].astype(jnp.float32)
    for group in range(1, shares.shape[0]):
        branch = branch + shares[group, :rows, :].astype(jnp.float32)
    after = (hidden[...].astype(jnp.float32) + branch).astype(jnp.bfloat16)
    result[...] = after
    project(after.astype(jnp.float32), gain[layer : layer + 1, :], w_query[0], queries)


def last_kernel(hidden, shares, result):
    rows = hidden.shape[0]
    branch = shares[0, :rows, :].astype(jnp.float32)
    for group in range(1, shares.shape[0]):
        branch = branch + shares[group, :rows, :].astype(jnp.float32)
    result[...] = (hidden[...].astype(jnp.float32) + branch).astype(jnp.bfloat16)


def first_queries(layer, hidden, gain, w_query, blocks, padded):
    shape = (blocks, padded, w_query.shape[2])
    return pl.pallas_call(
        functools.partial(first_kernel, layer),
        grid=(1,),
        in_specs=[whole(hidden.shape), whole(gain.shape), layer_of(w_query.shape, layer)],
        out_specs=whole(shape),
        out_shape=jax.ShapeDtypeStruct(shape, jnp.bfloat16),
        cost_estimate=cost(2 * padded * math.prod(w_query.shape[1:]), 2 * math.prod(w_query.shape[1:])),
        name="first_queries",
    )(hidden, gain, w_query)


def next_queries(layer, hidden, shares, gain, w_query, blocks, padded):
    shape = (blocks, padded, w_query.shape[2])
    return pl.pallas_call(
        functools.partial(next_kernel, layer),
        grid=(1,),
        in_specs=[
            whole(hidden.shape),
            whole(shares.shape),
            whole(gain.shape),
            layer_of(w_query.shape, layer),
        ],
        out_specs=[whole(shape), whole(hidden.shape)],
        out_shape=[
            jax.ShapeDtypeStruct(shape, jnp.bfloat16),
            jax.ShapeDtypeStruct(hidden.shape, jnp.bfloat16),
        ],
        cost_estimate=cost(2 * padded * math.prod(w_query.shape[1:]), 2 * math.prod(w_query.shape[1:])),
        name="next_queries",
    )(hidden, shares, gain, w_query)


def last_rows(hidden, shares):
    return pl.pallas_call(
        last_kernel,
        grid=(1,),
        in_specs=[whole(hidden.shape), whole(shares.shape)],
        out_specs=whole(hidden.shape),
        out_shape=jax.ShapeDtypeStruct(hidden.shape, jnp.bfloat16),
        name="last_rows",
    )(hidden, shares)


def attend_kernel(layer, queries, keys, values, scales, packed):
    blocks, padded, columns = queries.shape
    rows = blocks * padded
    root = math.sqrt(HEAD_DIM)
    lane = lax.broadcasted_iota(jnp.int32, (rows, LANES), 1)
    sums = jnp.zeros((rows, LANES), jnp.float32)
    for head in range(columns // HEAD_DIM):
        cut = slice(head * HEAD_DIM, (head + 1) * HEAD_DIM)
        query = queries[:, :, cut].reshape(rows, HEAD_DIM)
        scores = lax.dot_general(
            query, keys[0, :, cut], (((1,), (1,)), ((), ())), preferred_element_type=jnp.float32
        )
        weights = jnp.exp(scales[layer, head] * (scores / root - root))
        total = jnp.sum(weights, axis=1, keepdims=True)
        high = total.astype(jnp.bfloat16).astype(jnp.float32)
        sums = jnp.where(lane == 2 * head, high, sums)
        sums = jnp.where(lane == 2 * head + 1, total - high, sums)
        part = jnp.dot(
            weights.astype(jnp.bfloat16), values[0, :, cut], preferred_element_type=jnp.float32
        )
        packed[:, :, cut] = part.astype(jnp.bfloat16).reshape(blocks, padded, HEAD_DIM)
    packed[:, :, columns:] = sums.astype(jnp.bfloat16).reshape(blocks, padded, LANES)


def attend(layer, queries, keys, values, scales):
    blocks, padded, columns = queries.shape
    shape = (blocks, padded, columns + LANES)
    return pl.pallas_call(
        functools.partial(attend_kernel, layer),
        grid=(1,),
        in_specs=[
            whole(queries.shape),
            layer_of(keys.shape, layer),
            layer_of(values.shape, layer),
            pl.BlockSpec(memory_space=pltpu.SMEM),
        ],
        out_specs=whole(shape),
        out_shape=jax.ShapeDtypeStruct(shape, jnp.bfloat16),
        cost_estimate=cost(4 * blocks * padded * math.prod(keys.shape[1:]), 4 * math.prod(keys.shape[1:])),
        name="attend",
    )(queries, keys, values, scales)


def share_kernel(packed, w_out, share):
    width = w_out.shape[1]
    total = jnp.sum(packed[...].astype(jnp.float32), axis=0)
    branch = jnp.zeros(share.shape, jnp.float32)
    for head in range(width // HEAD_DIM):
        cut = slice(head * HEAD_DIM, (head + 1) * HEAD_DIM)
        at = width + 2 * head
        below = total[:, at : at + 1] + total[:, at + 1 : at + 2]
        attended = (total[:, cut] / below).astype(jnp.bfloat16)
        branch = branch + jnp.dot(attended, w_out[0, cut, :], preferred_element_type=jnp.float32)
    share[...] = branch.astype(jnp.bfloat16)


def share_of(layer, packed, w_out):
    shape = (packed.shape[1], w_out.shape[2])
    return pl.pallas_call(
        share_kernel,
        grid=(1,),
        in_specs=[whole(packed.shape), layer_of(w_out.shape, layer)],
        out_specs=whole(shape),
        out_shape=jax.ShapeDtypeStruct(shape, jnp.bfloat16),
        cost_estimate=cost(2 * packed.shape[1] * math.prod(w_out.shape[1:]), 2 * math.prod(w_out.shape[1:])),
        name="share",
    )(packed, w_out)


def body(target, source, tgt_gain, src_gain, w_query, w_key, w_value, w_out, score_scale):
    layers = w_query.shape[0]
    blocks = lax.axis_size("sp")
    padded = -(-target.shape[0] // SUBLANES) * SUBLANES
    hidden = target
    queries = first_queries(0, hidden, tgt_gain, w_query, blocks, padded)
    keys, values = source_side(source, src_gain, w_key, w_value)
    for layer in range(layers):
        queries = lax.all_to_all(queries, "sp", 0, 0)
        packed = attend(layer, queries, keys, values, score_scale)
        packed = lax.all_to_all(packed, "sp", 0, 0)
        shares = lax.all_gather(share_of(layer, packed, w_out), "tp")
        if layer + 1 < layers:
            queries, hidden = next_queries(
                layer + 1, hidden, shares, tgt_gain, w_query, blocks, padded
            )
        else:
            hidden = last_rows(hidden, shares)
    return hidden


def solution(mesh):
    placed = (
        P("sp", None),
        P("sp", None),
        P(),
        P(),
        P(None, None, "tp"),
        P(None, None, "tp"),
        P(None, None, "tp"),
        P(None, "tp", None),
        P(None, "tp"),
    )
    return jax.shard_map(body, mesh=mesh, in_specs=placed, out_specs=P("sp", None), check_vma=False)
```

time: 236 us -> 81.2 us (0.34)
  blocking collectives: 193 us -> 47.9 us
  Pallas kernels: 0 us -> 24.6 us
  local copies, waits for them, and re-layouts: 19.1 us -> 0.61 us
  matrix products: 16.3 us -> 0 us
  starting transfers between devices: 3.19 us -> 7.31 us
  other arithmetic: 2.62 us -> 0 us
    unnamed x4 -> x0, blocking collectives: 109 us -> none
    all_gather x2, blocking collectives: 62.9 us -> 12.9 us  [body(): shares = lax.all_gather(share_of(layer, packed, w_out), 'tp')]
    all_to_all x0 -> x3, blocking collectives: none -> 35 us  [the longest x2 24.1 us: body(): packed = lax.all_to_all(packed, 'sp', 0, 0)]
    pallas_call x0 -> x8, Pallas kernels: none -> 24.6 us  [the longest x1 7.37 us: source_side(): pl.pallas_call(source_kernel, grid=(layers, columns // HEAD_DIM), in_spec...]
    psum x2 -> x0, blocking collectives: 20.5 us -> none  [body(): lax.psum(share.astype(jnp.float32).astype(jnp.bfloat16), 'tp')]
    dot_general x6 -> x0, local copies, waits for them, and re-layouts: 16.9 us -> none  [the longest x3 8.79 us: source_side(): jnp.dot(normed_src, key_weight, preferred_element_type=jnp.float32)]
    dot_general x12 -> x0, matrix products: 16.3 us -> none  [the longest x2 4.99 us: source_side(): jnp.dot(normed_src, key_weight, preferred_element_type=jnp.float32)]
    all_to_all x0 -> x1, starting transfers between devices: none -> 7.31 us  [body(): queries = lax.all_to_all(queries, 'sp', 0, 0)]
  transfers between devices with their start and end apart: 2 -> 1, of which waited for: 0 -> 0; matrix products, arithmetic and copies ran while one was open for 4% -> 0% of each run, Pallas kernels for 0% -> 9%
where the time goes in v1:
time: 81.2 us; the launch traced here: 80.4 us
  blocking collectives  47.9 us (59%)
  Pallas kernels  24.6 us (30%)
  starting transfers between devices  7.31 us (9%)
    all_to_all x2, blocking collectives, body(): packed = lax.all_to_all(packed, 'sp', 0, 0)  24.1 us
    all_gather x2, blocking collectives, body(): shares = lax.all_gather(share_of(layer, packed, w_out), 'tp')  12.9 us
    all_to_all x1, blocking collectives, body(): queries = lax.all_to_all(queries, 'sp', 0, 0)  10.9 us
    pallas_call x1, Pallas kernels, source_side(): pl.pallas_call(source_kernel, grid=(layers, columns // HEAD_DIM), in_spec...  7.37 us
    all_to_all x1, starting transfers between devices, body(): queries = lax.all_to_all(queries, 'sp', 0, 0)  7.31 us
    pallas_call x2, Pallas kernels, share_of(): pl.pallas_call(share_kernel, grid=(1,), in_specs=[whole(packed.shape), la...  5.52 us
    pallas_call x2, Pallas kernels, attend(): pl.pallas_call(functools.partial(attend_kernel, layer), grid=(1,), in_spe...  4.44 us
    pallas_call x1, Pallas kernels, next_queries(): pl.pallas_call(functools.partial(next_kernel, layer), grid=(1,), in_specs...  2.91 us
  transfers between devices with their start and end apart: 1, of which 0 were waited for; matrix products, arithmetic and copies ran while one was open for 0% of the time, Pallas kernels for 9%

profile of v1, /device:TPU:0, one launch (start us, length us, event | category | flops | bytes accessed | tf_op | source)
XLA Modules:
  0.0 80.4 jit_solution(5275952419263739219)
XLA Ops:
  0.0 2.8 %first_queries.1 = bf16[8,8,512]{2,1,0:T(8,128)(2,1)} custom-call(bf16[7,2048]{1,0:T(8,128)(2,1)} %hidden.3, f32[2,2048]{1,0:T(2,128)} %gain.5, bf16[2,2048,512]{2,1,0:T(8,128)(2,1)} %w_query.3), custom_call_target="tpu_custom_call" | custom-call | flops 16777216 | bytes 2097152 | tf_op jit(solution)/shard_map/first_queries/pallas_call | solution.py:107
  2.8 7.3 %all-to-all-start = ((bf16[8,8,512]{2,1,0:T(8,128)(2,1)}), bf16[8,8,512]{2,1,0:T(8,128)(2,1)S(1)}, u32[]{:S(2)}, u32[]{:S(2)}) async-start(bf16[8,8,512]{2,1,0:T(8,128)(2,1)} %first_queries.1), calls=%async_computation | async-start | bytes 131072 | tf_op jit(solution)/shard_map/all_to_all | solution.py:227
  10.1 7.4 %source_side.1 = (bf16[2,256,512]{2,1,0:T(8,128)(2,1)}, bf16[2,256,512]{2,1,0:T(8,128)(2,1)}) custom-call(bf16[256,2048]{1,0:T(8,128)(2,1)} %source.1, f32[2,2048]{1,0:T(2,128)} %gain.4, bf16[2,2048,512]{2,1,0:T(8,128)(2,1)} %w_key.1, bf16[2,2048,512]{2,1,0:T(8,128)(2,1)} %w_value.1), custom_call_target="tpu_custom_call" | custom-call | flops 2147483648 | bytes 8388608 | tf_op jit(solution)/shard_map/source_side/pallas_call | solution.py:53
  17.5 0.0 all-to-all-done.queries
  17.5 0.0 copy-start
  17.5 0.6 copy-done
  18.1 2.2 %attend.2 = bf16[8,8,640]{2,1,0:T(8,128)(2,1)} custom-call(bf16[8,8,512]{2,1,0:T(8,128)(2,1)} %copy-done, bf16[2,256,512]{2,1,0:T(8,128)(2,1)} %get-tuple-element.9.keys, bf16[2,256,512]{2,1,0:T(8,128)(2,1)} %get-tuple-element.10.values, f32[2,2]{1,0:T(2,128)} %scales.3), custom_call_target="tpu_custom_call" | custom-call | flops 33554432 | bytes 524288 | tf_op jit(solution)/shard_map/attend/pallas_call | solution.py:177
  20.3 13.1 %all_to_all.20.packed = bf16[8,8,640]{2,1,0:T(8,128)(2,1)} all-to-all(bf16[8,8,640]{2,1,0:T(8,128)(2,1)} %attend.2), channel_id=1, replica_groups=mesh['sp'=8,'tp'=4] {'sp'}, dimensions={0} | all-to-all | bytes 163840 | tf_op jit(solution)/shard_map/all_to_all | solution.py:229
  33.4 2.8 %share.2 = bf16[8,2048]{1,0:T(8,128)(2,1)} custom-call(bf16[8,8,640]{2,1,0:T(8,128)(2,1)} %all_to_all.20.packed, bf16[2,512,2048]{2,1,0:T(8,128)(2,1)} %w_out.3), custom_call_target="tpu_custom_call" | custom-call | flops 16777216 | bytes 2097152 | tf_op jit(solution)/shard_map/share/pallas_call | solution.py:208
  36.2 6.9 %all-gather = bf16[32,2048]{1,0:T(8,128)(2,1)} all-gather(bf16[8,2048]{1,0:T(8,128)(2,1)} %share.2), channel_id=2, replica_groups=mesh['sp'=8,'tp'=4] {'tp'}, dimensions={0}, use_global_device_ids=true | all-gather | bytes 163840 | tf_op jit(solution)/shard_map/all_gather | solution.py:230
  43.1 2.9 %next_queries.1 = (bf16[8,8,512]{2,1,0:T(8,128)(2,1)}, bf16[7,2048]{1,0:T(8,128)(2,1)}) custom-call(bf16[7,2048]{1,0:T(8,128)(2,1)} %hidden.3, bf16[4,8,2048]{2,1,0:T(8,128)(2,1)} %bitcast.2, f32[2,2048]{1,0:T(2,128)} %gain.5, bf16[2,2048,512]{2,1,0:T(8,128)(2,1)} %w_query.3), custom_call_target="tpu_custom_call" | custom-call | flops 16777216 | bytes 2097152 | tf_op jit(solution)/shard_map/next_queries/pallas_call | solution.py:120
  46.0 10.9 %all_to_all.21.queries = bf16[8,8,512]{2,1,0:T(8,128)(2,1)} all-to-all(bf16[8,8,512]{2,1,0:T(8,128)(2,1)} %get-tuple-element.12), channel_id=1, replica_groups=mesh['sp'=8,'tp'=4] {'sp'}, dimensions={0} | all-to-all | bytes 131072 | tf_op jit(solution)/shard_map/all_to_all | solution.py:227
  56.8 2.2 %attend.3 = bf16[8,8,640]{2,1,0:T(8,128)(2,1)} custom-call(bf16[8,8,512]{2,1,0:T(8,128)(2,1)} %all_to_all.21.queries, bf16[2,256,512]{2,1,0:T(8,128)(2,1)} %get-tuple-element.9.keys, bf16[2,256,512]{2,1,0:T(8,128)(2,1)} %get-tuple-element.10.values, f32[2,2]{1,0:T(2,128)} %scales.3), custom_call_target="tpu_custom_call" | custom-call | flops 33554432 | bytes 524288 | tf_op jit(solution)/shard_map/attend/pallas_call | solution.py:177
  59.1 11.0 %all_to_all.22.packed = bf16[8,8,640]{2,1,0:T(8,128)(2,1)} all-to-all(bf16[8,8,640]{2,1,0:T(8,128)(2,1)} %attend.3), channel_id=1, replica_groups=mesh['sp'=8,'tp'=4] {'sp'}, dimensions={0} | all-to-all | bytes 163840 | tf_op jit(solution)/shard_map/all_to_all | solution.py:229
  70.1 2.8 %share.3 = bf16[8,2048]{1,0:T(8,128)(2,1)} custom-call(bf16[8,8,640]{2,1,0:T(8,128)(2,1)} %all_to_all.22.packed, bf16[2,512,2048]{2,1,0:T(8,128)(2,1)} %w_out.3), custom_call_target="tpu_custom_call" | custom-call | flops 16777216 | bytes 2097152 | tf_op jit(solution)/shard_map/share/pallas_call | solution.py:208
  72.8 6.1 %all-gather.1 = bf16[32,2048]{1,0:T(8,128)(2,1)} all-gather(bf16[8,2048]{1,0:T(8,128)(2,1)} %share.3), channel_id=3, replica_groups=mesh['sp'=8,'tp'=4] {'tp'}, dimensions={0}, use_global_device_ids=true | all-gather | bytes 163840 | tf_op jit(solution)/shard_map/all_gather | solution.py:230
  78.9 1.6 %last_rows.1 = bf16[7,2048]{1,0:T(8,128)(2,1)} custom-call(bf16[7,2048]{1,0:T(8,128)(2,1)} %get-tuple-element.11.hidden, bf16[4,8,2048]{2,1,0:T(8,128)(2,1)} %bitcast.3), custom_call_target="tpu_custom_call" | custom-call | tf_op jit(solution)/shard_map/last_rows/pallas_call | solution.py:140
Async XLA Ops:
  2.8 14.7 %all-to-all-start = ((bf16[8,8,512]{2,1,0:T(8,128)(2,1)}), bf16[8,8,512]{2,1,0:T(8,128)(2,1)S(1)}, u32[]{:S(2)}, u32[]{:S(2)}) async-start(bf16[8,8,512]{2,1,0:T(8,128)(2,1)} %first_queries.1), calls=%async_computation | async-start | bytes 131072 | tf_op jit(solution)/shard_map/all_to_all | solution.py:227
  17.5 0.6 copy-start

commit v2 on v1

--- a/solution.py
+++ b/solution.py
@@ -23,6 +23,10 @@
     return pl.BlockSpec((1, *shape[1:]), lambda *_: (layer,) + (0,) * (len(shape) - 1))
 
 
+def in_hbm(array):
+    return pltpu.with_memory_space_constraint(array, pltpu.HBM)
+
+
 def row_scale(values):
     return lax.rsqrt(jnp.mean(values * values, axis=-1, keepdims=True) + EPS)
 
@@ -31,35 +35,36 @@
     return pl.CostEstimate(flops=flops, bytes_accessed=moved, transcendentals=0)
 
 
-def source_kernel(source, gain, w_key, w_value, keys, values, normed):
-    @pl.when(pl.program_id(1) == 0)
+def source_kernel(layer, source, gain, w_key, w_value, keys, values, normed):
+    @pl.when(pl.program_id(0) == 0)
     def _():
         rows = source[...].astype(jnp.float32)
-        gains = gain[pl.ds(pl.program_id(0), 1), :]
+        gains = gain[layer : layer + 1, :]
         normed[...] = (rows * row_scale(rows) * gains).astype(jnp.bfloat16)
 
     key = jnp.dot(normed[...], w_key[0], preferred_element_type=jnp.float32)
-    keys[0] = (key * row_scale(key)).astype(jnp.bfloat16)
+    keys[...] = (key * row_scale(key)).astype(jnp.bfloat16)
     value = jnp.dot(normed[...], w_value[0], preferred_element_type=jnp.float32)
-    values[0] = value.astype(jnp.bfloat16)
-
-
-def source_side(source, gain, w_key, w_value):
-    layers, width, columns = w_key.shape
+    values[...] = value.astype(jnp.bfloat16)
+
+
+def source_side(layer, source, gain, w_key, w_value):
+    _, width, columns = w_key.shape
     rows = source.shape[0]
-    weight = pl.BlockSpec((1, width, HEAD_DIM), lambda l, h: (l, 0, h))
-    out = pl.BlockSpec((1, rows, HEAD_DIM), lambda l, h: (l, 0, h))
-    shape = jax.ShapeDtypeStruct((layers, rows, columns), jnp.bfloat16)
-    return pl.pallas_call(
-        source_kernel,
-        grid=(layers, columns // HEAD_DIM),
+    weight = pl.BlockSpec((1, width, HEAD_DIM), lambda h: (layer, 0, h))
+    out = pl.BlockSpec((rows, HEAD_DIM), lambda h: (0, h))
+    shape = jax.ShapeDtypeStruct((rows, columns), jnp.bfloat16)
+    return pl.pallas_call(
+        functools.partial(source_kernel, layer),
+        grid=(columns // HEAD_DIM,),
         in_specs=[whole(source.shape), whole(gain.shape), weight, weight],
         out_specs=[out, out],
         out_shape=[shape, shape],
         scratch_shapes=[VMEM((rows, width), jnp.bfloat16)],
-        cost_estimate=cost(4 * layers * rows * width * columns, 4 * layers * width * columns),
+        cost_estimate=cost(4 * rows * width * columns, 4 * width * columns),
+        compiler_params=pltpu.CompilerParams(vmem_limit_bytes=16 << 20),
         name="source_side",
-    )(source, gain, w_key, w_value)
+    )(source, gain, in_hbm(w_key), in_hbm(w_value))
 
 
 def project(hidden, gains, weight, queries):
@@ -84,35 +89,43 @@
     )
 
 
-def next_kernel(layer, hidden, shares, gain, w_query, queries, result):
-    rows = hidden.shape[0]
-    branch = shares[0, :rows, :].astype(jnp.float32)
-    for group in range(1, shares.shape[0]):
-        branch = branch + shares[group, :rows, :].astype(jnp.float32)
+def branch_of(shares, rows):
+    sums = [share[:rows, :].astype(jnp.float32) for share in shares]
+    while len(sums) > 1:
+        sums = [sums[at] + sums[at + 1] for at in range(0, len(sums), 2)]
+    return sums[0]
+
+
+def next_kernel(layer, hidden, gain, w_query, *rest):
+    *shares, queries, result = rest
+    branch = branch_of(shares, hidden.shape[0])
     after = (hidden[...].astype(jnp.float32) + branch).astype(jnp.bfloat16)
     result[...] = after
     project(after.astype(jnp.float32), gain[layer : layer + 1, :], w_query[0], queries)
 
 
-def last_kernel(hidden, shares, result):
-    rows = hidden.shape[0]
-    branch = shares[0, :rows, :].astype(jnp.float32)
-    for group in range(1, shares.shape[0]):
-        branch = branch + shares[group, :rows, :].astype(jnp.float32)
+def last_kernel(hidden, *rest):
+    *shares, result = rest
+    branch = branch_of(shares, hidden.shape[0])
     result[...] = (hidden[...].astype(jnp.float32) + branch).astype(jnp.bfloat16)
 
 
 def first_queries(layer, hidden, gain, w_query, blocks, padded):
-    shape = (blocks, padded, w_query.shape[2])
+    _, width, columns = w_query.shape
     return pl.pallas_call(
         functools.partial(first_kernel, layer),
-        grid=(1,),
-        in_specs=[whole(hidden.shape), whole(gain.shape), layer_of(w_query.shape, layer)],
-        out_specs=whole(shape),
-        out_shape=jax.ShapeDtypeStruct(shape, jnp.bfloat16),
-        cost_estimate=cost(2 * padded * math.prod(w_query.shape[1:]), 2 * math.prod(w_query.shape[1:])),
+        grid=(columns // HEAD_DIM,),
+        in_specs=[
+            whole(hidden.shape),
+            whole(gain.shape),
+            pl.BlockSpec((1, width, HEAD_DIM), lambda h: (layer, 0, h)),
+        ],
+        out_specs=pl.BlockSpec((blocks, padded, HEAD_DIM), lambda h: (0, 0, h)),
+        out_shape=jax.ShapeDtypeStruct((blocks, padded, columns), jnp.bfloat16),
+        cost_estimate=cost(2 * padded * width * columns, 2 * width * columns),
+        compiler_params=pltpu.CompilerParams(vmem_limit_bytes=8 << 20),
         name="first_queries",
-    )(hidden, gain, w_query)
+    )(in_hbm(hidden), in_hbm(gain), in_hbm(w_query))
 
 
 def next_queries(layer, hidden, shares, gain, w_query, blocks, padded):
@@ -122,9 +135,9 @@
         grid=(1,),
         in_specs=[
             whole(hidden.shape),
-            whole(shares.shape),
             whole(gain.shape),
             layer_of(w_query.shape, layer),
+            *(whole(share.shape) for share in shares),
         ],
         out_specs=[whole(shape), whole(hidden.shape)],
         out_shape=[
@@ -132,19 +145,21 @@
             jax.ShapeDtypeStruct(hidden.shape, jnp.bfloat16),
         ],
         cost_estimate=cost(2 * padded * math.prod(w_query.shape[1:]), 2 * math.prod(w_query.shape[1:])),
+        compiler_params=pltpu.CompilerParams(vmem_limit_bytes=8 << 20),
         name="next_queries",
-    )(hidden, shares, gain, w_query)
+    )(hidden, gain, w_query, *shares)
 
 
 def last_rows(hidden, shares):
     return pl.pallas_call(
         last_kernel,
         grid=(1,),
-        in_specs=[whole(hidden.shape), whole(shares.shape)],
+        in_specs=[whole(hidden.shape), *(whole(share.shape) for share in shares)],
         out_specs=whole(hidden.shape),
         out_shape=jax.ShapeDtypeStruct(hidden.shape, jnp.bfloat16),
+        compiler_params=pltpu.CompilerParams(vmem_limit_bytes=8 << 20),
         name="last_rows",
-    )(hidden, shares)
+    )(hidden, *shares)
 
 
 def attend_kernel(layer, queries, keys, values, scales, packed):
@@ -157,7 +172,7 @@
         cut = slice(head * HEAD_DIM, (head + 1) * HEAD_DIM)
         query = queries[:, :, cut].reshape(rows, HEAD_DIM)
         scores = lax.dot_general(
-            query, keys[0, :, cut], (((1,), (1,)), ((), ())), preferred_element_type=jnp.float32
+            query, keys[:, cut], (((1,), (1,)), ((), ())), preferred_element_type=jnp.float32
         )
         weights = jnp.exp(scales[layer, head] * (scores / root - root))
         total = jnp.sum(weights, axis=1, keepdims=True)
@@ -165,7 +180,7 @@
         sums = jnp.where(lane == 2 * head, high, sums)
         sums = jnp.where(lane == 2 * head + 1, total - high, sums)
         part = jnp.dot(
-            weights.astype(jnp.bfloat16), values[0, :, cut], preferred_element_type=jnp.float32
+            weights.astype(jnp.bfloat16), values[:, cut], preferred_element_type=jnp.float32
         )
         packed[:, :, cut] = part.astype(jnp.bfloat16).reshape(blocks, padded, HEAD_DIM)
     packed[:, :, columns:] = sums.astype(jnp.bfloat16).reshape(blocks, padded, LANES)
@@ -179,13 +194,14 @@
         grid=(1,),
         in_specs=[
             whole(queries.shape),
-            layer_of(keys.shape, layer),
-            layer_of(values.shape, layer),
+            whole(keys.shape),
+            whole(values.shape),
             pl.BlockSpec(memory_space=pltpu.SMEM),
         ],
         out_specs=whole(shape),
         out_shape=jax.ShapeDtypeStruct(shape, jnp.bfloat16),
-        cost_estimate=cost(4 * blocks * padded * math.prod(keys.shape[1:]), 4 * math.prod(keys.shape[1:])),
+        cost_estimate=cost(400 * blocks * padded * math.prod(keys.shape), 4 * math.prod(keys.shape)),
+        compiler_params=pltpu.CompilerParams(vmem_limit_bytes=8 << 20),
         name="attend",
     )(queries, keys, values, scales)
 
@@ -212,8 +228,17 @@
         out_specs=whole(shape),
         out_shape=jax.ShapeDtypeStruct(shape, jnp.bfloat16),
         cost_estimate=cost(2 * packed.shape[1] * math.prod(w_out.shape[1:]), 2 * math.prod(w_out.shape[1:])),
+        compiler_params=pltpu.CompilerParams(vmem_limit_bytes=8 << 20),
         name="share",
     )(packed, w_out)
+
+
+def over_groups(share):
+    count = lax.axis_size("tp")
+    return [share] + [
+        lax.ppermute(share, "tp", [(i, (i ^ m) % count) for i in range(count)])
+        for m in range(1, count)
+    ]
 
 
 def body(target, source, tgt_gain, src_gain, w_query, w_key, w_value, w_out, score_scale):
@@ -222,12 +247,15 @@
     padded = -(-target.shape[0] // SUBLANES) * SUBLANES
     hidden = target
     queries = first_queries(0, hidden, tgt_gain, w_query, blocks, padded)
-    keys, values = source_side(source, src_gain, w_key, w_value)
+    keys, values = source_side(0, source, src_gain, w_key, w_value)
     for layer in range(layers):
         queries = lax.all_to_all(queries, "sp", 0, 0)
         packed = attend(layer, queries, keys, values, score_scale)
+        if layer + 1 < layers:
+            source, packed = lax.optimization_barrier((source, packed))
+            keys, values = source_side(layer + 1, source, src_gain, w_key, w_value)
         packed = lax.all_to_all(packed, "sp", 0, 0)
-        shares = lax.all_gather(share_of(layer, packed, w_out), "tp")
+        shares = over_groups(share_of(layer, packed, w_out))
         if layer + 1 < layers:
             queries, hidden = next_queries(
                 layer + 1, hidden, shares, tgt_gain, w_query, blocks, padded

time: 81.2 us -> 60.3 us (0.74)
  blocking collectives: 47.9 us -> 19.5 us
  waiting for transfers between devices: 0.01 us -> 10.8 us
  Pallas kernels: 24.6 us -> 15 us
  starting transfers between devices: 7.31 us -> 14.4 us
    all_gather x2 -> x0, blocking collectives: 12.9 us -> none  [body(): shares = lax.all_gather(share_of(layer, packed, w_out), 'tp')]
    all_to_all x1 -> x0, blocking collectives: 10.9 us -> none  [body(): queries = lax.all_to_all(queries, 'sp', 0, 0)]
    all_to_all x1 -> x2, waiting for transfers between devices: 0.01 us -> 6.44 us  [body(): queries = lax.all_to_all(queries, 'sp', 0, 0)]
    all_to_all x2, blocking collectives: 24.1 us -> 19.5 us  [body(): packed = lax.all_to_all(packed, 'sp', 0, 0)]
    pallas_call x2, Pallas kernels: 5.52 us -> 0.99 us  [share_of(): pl.pallas_call(share_kernel, grid=(1,), in_specs=[whole(packed.shape), la...]
    ppermute x0 -> x6, waiting for transfers between devices: none -> 4.36 us  [over_groups(): lax.ppermute(share, 'tp', [(i, (i ^ m) % count) for i in range(count)])]
    ppermute x0 -> x6, starting transfers between devices: none -> 3.73 us  [over_groups(): lax.ppermute(share, 'tp', [(i, (i ^ m) % count) for i in range(count)])]
    all_to_all x1 -> x2, starting transfers between devices: 7.31 us -> 10.7 us  [body(): queries = lax.all_to_all(queries, 'sp', 0, 0)]
  transfers between devices with their start and end apart: 1 -> 8, of which waited for: 0 -> 6; matrix products, arithmetic and copies ran while one was open for 0% -> 0% of each run, Pallas kernels for 9% -> 12%
where the time goes in v2:
time: 60.3 us; the launch traced here: 59.9 us
  blocking collectives  19.5 us (32%)
  Pallas kernels  15 us (25%)
  starting transfers between devices  14.4 us (24%)
  waiting for transfers between devices  10.8 us (18%)
    all_to_all x2, blocking collectives, body(): packed = lax.all_to_all(packed, 'sp', 0, 0)  19.5 us
    all_to_all x2, starting transfers between devices, body(): queries = lax.all_to_all(queries, 'sp', 0, 0)  10.7 us
    pallas_call x2, Pallas kernels, source_side(): pl.pallas_call(functools.partial(source_kernel, layer), grid=(columns //...  7.26 us
    all_to_all x2, waiting for transfers between devices, body(): queries = lax.all_to_all(queries, 'sp', 0, 0)  6.44 us
    ppermute x6, waiting for transfers between devices, over_groups(): lax.ppermute(share, 'tp', [(i, (i ^ m) % count) for i in range(count)])  4.36 us
    ppermute x6, starting transfers between devices, over_groups(): lax.ppermute(share, 'tp', [(i, (i ^ m) % count) for i in range(count)])  3.73 us
    pallas_call x1, Pallas kernels, first_queries(): pl.pallas_call(functools.partial(first_kernel, layer), grid=(columns // H...  2.78 us
    pallas_call x2, Pallas kernels, attend(): pl.pallas_call(functools.partial(attend_kernel, layer), grid=(1,), in_spe...  2.12 us
  transfers between devices with their start and end apart: 8, of which 6 were waited for; matrix products, arithmetic and copies ran while one was open for 0% of the time, Pallas kernels for 12%

profile of v2, /device:TPU:0, one launch (start us, length us, event | category | flops | bytes accessed | tf_op | source)
XLA Modules:
  0.0 59.9 jit_solution(5876145666668910500)
XLA Ops:
  0.0 2.8 %first_queries.1 = bf16[8,8,512]{2,1,0:T(8,128)(2,1)} custom-call(bf16[7,2048]{1,0:T(8,128)(2,1)} %hidden.3, f32[2,2048]{1,0:T(2,128)} %gain.6, bf16[2,2048,512]{2,1,0:T(8,128)(2,1)} %w_query.3), custom_call_target="tpu_custom_call" | custom-call | flops 16777216 | bytes 2097152 | tf_op jit(solution)/shard_map/first_queries/pallas_call | solution.py:115
  2.8 7.3 %all-to-all-start = ((bf16[8,8,512]{2,1,0:T(8,128)(2,1)}), bf16[8,8,512]{2,1,0:T(8,128)(2,1)S(1)}, u32[]{:S(2)}, u32[]{:S(2)}) async-start(bf16[8,8,512]{2,1,0:T(8,128)(2,1)} %first_queries.1), calls=%async_computation | async-start | bytes 131072 | tf_op jit(solution)/shard_map/all_to_all | solution.py:252
  10.1 0.0 copy-start.7
  10.1 3.6 %source_side.2 = (bf16[256,512]{1,0:T(8,128)(2,1)S(1)}, bf16[256,512]{1,0:T(8,128)(2,1)S(1)}) custom-call(bf16[256,2048]{1,0:T(8,128)(2,1)S(1)} %copy-done.3, f32[2,2048]{1,0:T(2,128)S(1)} %copy-done.6, bf16[2,2048,512]{2,1,0:T(8,128)(2,1)} %w_key.3, bf16[2,2048,512]{2,1,0:T(8,128)(2,1)} %w_value.3), custom_call_target="tpu_custom_call" | custom-call | flops 1073741824 | bytes 4194304 | tf_op jit(solution)/shard_map/source_side/pallas_call | solution.py:57
  13.8 3.2 %all-to-all-done.queries = bf16[8,8,512]{2,1,0:T(8,128)(2,1)S(1)} async-done(((bf16[8,8,512]{2,1,0:T(8,128)(2,1)}), bf16[8,8,512]{2,1,0:T(8,128)(2,1)S(1)}, u32[]{:S(2)}, u32[]{:S(2)}) %all-to-all-start) | async-done | bytes 65568 | tf_op jit(solution)/shard_map/all_to_all | solution.py:252
  17.0 1.1 %attend.2 = bf16[8,8,640]{2,1,0:T(8,128)(2,1)S(1)} custom-call(bf16[8,8,512]{2,1,0:T(8,128)(2,1)S(1)} %all-to-all-done.queries, bf16[256,512]{1,0:T(8,128)(2,1)S(1)} %get-tuple-element.13.keys, bf16[256,512]{1,0:T(8,128)(2,1)S(1)} %get-tuple-element.14.values, f32[2,2]{1,0:T(2,128)S(1)} %copy-done.7), custom_call_target="tpu_custom_call" | custom-call | flops 3355443200 | bytes 524288 | tf_op jit(solution)/shard_map/attend/pallas_call | solution.py:192
  18.1 0.0 copy-start
  18.1 0.0 copy-start.4
  18.1 0.0 copy-start.5
  18.1 9.9 %all_to_all.20.packed = bf16[8,8,640]{2,1,0:T(8,128)(2,1)S(1)} all-to-all(bf16[8,8,640]{2,1,0:T(8,128)(2,1)S(1)} %attend.2), channel_id=1, replica_groups=mesh['sp'=8,'tp'=4] {'sp'}, dimensions={0} | all-to-all | bytes 163840 | tf_op jit(solution)/shard_map/all_to_all | solution.py:257
  28.0 0.0 copy-done.1
  28.0 0.5 share.2.rest_0_
  28.5 0.0 collective-permute-start.2
  28.5 1.6 %collective-permute-start.1 = (bf16[8,2048]{1,0:T(8,128)(2,1)S(1)}, bf16[8,2048]{1,0:T(8,128)(2,1)S(1)}, u32[]{:S(2)}, u32[]{:S(2)}) collective-permute-start(bf16[8,2048]{1,0:T(8,128)(2,1)S(1)} %share.2.rest_0_), channel_id=1, source_target_pairs={{0,2},{1,3},{2,0},{3,1},{4,6},{5,7},{6,4},{7,5},{8,10},{9,11},{10,... | collective-permute-start | bytes 98312 | tf_op jit(solution)/shard_map/ppermute | solution.py:239
  30.0 0.3 collective-permute-start
  30.3 1.8 %collective-permute-done.2.rest_3_ = bf16[8,2048]{1,0:T(8,128)(2,1)S(1)} collective-permute-done((bf16[8,2048]{1,0:T(8,128)(2,1)S(1)}, bf16[8,2048]{1,0:T(8,128)(2,1)S(1)}, u32[]{:S(2)}, u32[]{:S(2)}) %collective-permute-start.2) | collective-permute-done | bytes 32800 | tf_op jit(solution)/shard_map/ppermute | solution.py:239
  32.1 0.4 collective-permute-done.1.rest_2_
  32.5 0.0 collective-permute-done.rest_1_
  32.5 1.2 %next_queries.1 = (bf16[8,8,512]{2,1,0:T(8,128)(2,1)}, bf16[7,2048]{1,0:T(8,128)(2,1)S(1)}) custom-call(bf16[7,2048]{1,0:T(8,128)(2,1)S(1)} %copy-done.4, f32[2,2048]{1,0:T(2,128)S(1)} %copy-done.5, bf16[2,2048,512]{2,1,0:T(8,128)(2,1)S(1)} %copy-done, bf16[8,2048]{1,0:T(8,128)(2,1)S(1)} %share.2.rest_0_, bf16[8,2048]{1,0:T(8,128)(2,1)S(1)} %collective-permute-done.rest_1_, ...), custom_call_target="tpu_custom_call" | custom-call | flops 16777216 | bytes 2097152 | tf_op jit(solution)/shard_map/next_queries/pallas_call | solution.py:133
  33.7 3.3 %all-to-all-start.2 = ((bf16[8,8,512]{2,1,0:T(8,128)(2,1)}), bf16[8,8,512]{2,1,0:T(8,128)(2,1)S(1)}, u32[]{:S(2)}, u32[]{:S(2)}) async-start(bf16[8,8,512]{2,1,0:T(8,128)(2,1)} %get-tuple-element.17), calls=%async_computation.2 | async-start | bytes 131072 | tf_op jit(solution)/shard_map/all_to_all | solution.py:252
  37.1 3.6 %source_side.3 = (bf16[256,512]{1,0:T(8,128)(2,1)S(1)}, bf16[256,512]{1,0:T(8,128)(2,1)S(1)}) custom-call(bf16[256,2048]{1,0:T(8,128)(2,1)S(1)} %copy-done.3, f32[2,2048]{1,0:T(2,128)S(1)} %copy-done.6, bf16[2,2048,512]{2,1,0:T(8,128)(2,1)} %w_key.3, bf16[2,2048,512]{2,1,0:T(8,128)(2,1)} %w_value.3), custom_call_target="tpu_custom_call" | custom-call | flops 1073741824 | bytes 4194304 | tf_op jit(solution)/shard_map/source_side/pallas_call | solution.py:57
  40.7 3.2 %all-to-all-done.2.queries = bf16[8,8,512]{2,1,0:T(8,128)(2,1)S(1)} async-done(((bf16[8,8,512]{2,1,0:T(8,128)(2,1)}), bf16[8,8,512]{2,1,0:T(8,128)(2,1)S(1)}, u32[]{:S(2)}, u32[]{:S(2)}) %all-to-all-start.2) | async-done | bytes 65568 | tf_op jit(solution)/shard_map/all_to_all | solution.py:252
  43.9 1.1 %attend.3 = bf16[8,8,640]{2,1,0:T(8,128)(2,1)S(1)} custom-call(bf16[8,8,512]{2,1,0:T(8,128)(2,1)S(1)} %all-to-all-done.2.queries, bf16[256,512]{1,0:T(8,128)(2,1)S(1)} %get-tuple-element.19.keys, bf16[256,512]{1,0:T(8,128)(2,1)S(1)} %get-tuple-element.20.values, f32[2,2]{1,0:T(2,128)S(1)} %copy-done.7), custom_call_target="tpu_custom_call" | custom-call | flops 3355443200 | bytes 524288 | tf_op jit(solution)/shard_map/attend/pallas_call | solution.py:192
  45.0 9.7 %all_to_all.21.packed = bf16[8,8,640]{2,1,0:T(8,128)(2,1)S(1)} all-to-all(bf16[8,8,640]{2,1,0:T(8,128)(2,1)S(1)} %attend.3), channel_id=1, replica_groups=mesh['sp'=8,'tp'=4] {'sp'}, dimensions={0} | all-to-all | bytes 163840 | tf_op jit(solution)/shard_map/all_to_all | solution.py:257
  54.7 0.5 share.3.rest_0_
  55.2 0.0 collective-permute-start.5
  55.2 1.6 %collective-permute-start.4 = (bf16[8,2048]{1,0:T(8,128)(2,1)S(1)}, bf16[8,2048]{1,0:T(8,128)(2,1)S(1)}, u32[]{:S(2)}, u32[]{:S(2)}) collective-permute-start(bf16[8,2048]{1,0:T(8,128)(2,1)S(1)} %share.3.rest_0_), channel_id=1, source_target_pairs={{0,2},{1,3},{2,0},{3,1},{4,6},{5,7},{6,4},{7,5},{8,10},{9,11},{10,... | collective-permute-start | bytes 98312 | tf_op jit(solution)/shard_map/ppermute | solution.py:239
  56.8 0.3 collective-permute-start.3
  57.1 1.8 %collective-permute-done.5.rest_3_ = bf16[8,2048]{1,0:T(8,128)(2,1)S(1)} collective-permute-done((bf16[8,2048]{1,0:T(8,128)(2,1)S(1)}, bf16[8,2048]{1,0:T(8,128)(2,1)S(1)}, u32[]{:S(2)}, u32[]{:S(2)}) %collective-permute-start.5) | collective-permute-done | bytes 32800 | tf_op jit(solution)/shard_map/ppermute | solution.py:239
  58.8 0.4 collective-permute-done.4.rest_2_
  59.2 0.0 collective-permute-done.3.rest_1_
  59.2 0.6 %last_rows.1 = bf16[7,2048]{1,0:T(8,128)(2,1)} custom-call(bf16[7,2048]{1,0:T(8,128)(2,1)S(1)} %get-tuple-element.16.hidden, bf16[8,2048]{1,0:T(8,128)(2,1)S(1)} %share.3.rest_0_, bf16[8,2048]{1,0:T(8,128)(2,1)S(1)} %collective-permute-done.3.rest_1_, bf16[8,2048]{1,0:T(8,128)(2,1)S(1)} %collective-permute-done.4.rest_2_, ...), custom_call_target="tpu_custom_call" | custom-call | tf_op jit(solution)/shard_map/last_rows/pallas_call | solution.py:154
  (11 shorter events, 0.0 us)
Async XLA Ops:
  0.0 10.1 %copy-start.6 = (f32[2,2048]{1,0:T(2,128)S(1)}, f32[2,2048]{1,0:T(2,128)}, u32[]{:S(2)}) copy-start(f32[2,2048]{1,0:T(2,128)} %gain.7) | copy-start | bytes 49156
  0.0 10.1 %copy-start.3 = (bf16[256,2048]{1,0:T(8,128)(2,1)S(1)}, bf16[256,2048]{1,0:T(8,128)(2,1)}, u32[]{:S(2)}) copy-start(bf16[256,2048]{1,0:T(8,128)(2,1)} %source.2) | copy-start | bytes 3145732
  2.8 14.2 %all-to-all-start = ((bf16[8,8,512]{2,1,0:T(8,128)(2,1)}), bf16[8,8,512]{2,1,0:T(8,128)(2,1)S(1)}, u32[]{:S(2)}, u32[]{:S(2)}) async-start(bf16[8,8,512]{2,1,0:T(8,128)(2,1)} %first_queries.1), calls=%async_computation | async-start | bytes 131072 | tf_op jit(solution)/shard_map/all_to_all | solution.py:252
  10.1 6.9 %copy-start.7 = (f32[2,2]{1,0:T(2,128)S(1)}, f32[2,2]{1,0:T(2,128)}, u32[]{:S(2)}) copy-start(f32[2,2]{1,0:T(2,128)} %scales.3) | copy-start | bytes 52
  17.0 11.0 %copy-start.1 = (bf16[2,512,2048]{2,1,0:T(8,128)(2,1)S(1)}, bf16[2,512,2048]{2,1,0:T(8,128)(2,1)}, u32[]{:S(2)}) copy-start(bf16[2,512,2048]{2,1,0:T(8,128)(2,1)} %w_out.3) | copy-start | bytes 12582916
  18.1 14.4 %copy-start = (bf16[2,2048,512]{2,1,0:T(8,128)(2,1)S(1)}, bf16[2,2048,512]{2,1,0:T(8,128)(2,1)}, u32[]{:S(2)}) copy-start(bf16[2,2048,512]{2,1,0:T(8,128)(2,1)} %w_query.3) | copy-start | bytes 12582916
  18.1 14.4 %copy-start.4 = (bf16[7,2048]{1,0:T(8,128)(2,1)S(1)}, bf16[7,2048]{1,0:T(8,128)(2,1)}, u32[]{:S(2)}) copy-start(bf16[7,2048]{1,0:T(8,128)(2,1)} %hidden.3) | copy-start | bytes 86020
  18.1 14.4 %copy-start.5 = (f32[2,2048]{1,0:T(2,128)S(1)}, f32[2,2048]{1,0:T(2,128)}, u32[]{:S(2)}) copy-start(f32[2,2048]{1,0:T(2,128)} %gain.6) | copy-start | bytes 49156
  28.5 3.7 %collective-permute-start.2 = (bf16[8,2048]{1,0:T(8,128)(2,1)S(1)}, bf16[8,2048]{1,0:T(8,128)(2,1)S(1)}, u32[]{:S(2)}, u32[]{:S(2)}) collective-permute-start(bf16[8,2048]{1,0:T(8,128)(2,1)S(1)} %share.2.rest_0_), channel_id=1, source_target_pairs={{0,3},{1,2},{2,1},{3,0},{4,7},{5,6},{6,5},{7,4},{8,11},{9,10},{10,... | collective-permute-start | bytes 98312 | tf_op jit(solution)/shard_map/ppermute | solution.py:239
  28.5 4.0 %collective-permute-start.1 = (bf16[8,2048]{1,0:T(8,128)(2,1)S(1)}, bf16[8,2048]{1,0:T(8,128)(2,1)S(1)}, u32[]{:S(2)}, u32[]{:S(2)}) collective-permute-start(bf16[8,2048]{1,0:T(8,128)(2,1)S(1)} %share.2.rest_0_), channel_id=1, source_target_pairs={{0,2},{1,3},{2,0},{3,1},{4,6},{5,7},{6,4},{7,5},{8,10},{9,11},{10,... | collective-permute-start | bytes 98312 | tf_op jit(solution)/shard_map/ppermute | solution.py:239
  30.0 2.5 %collective-permute-start = (bf16[8,2048]{1,0:T(8,128)(2,1)S(1)}, bf16[8,2048]{1,0:T(8,128)(2,1)S(1)}, u32[]{:S(2)}, u32[]{:S(2)}) collective-permute-start(bf16[8,2048]{1,0:T(8,128)(2,1)S(1)} %share.2.rest_0_), channel_id=1, source_target_pairs={{0,1},{1,0},{2,3},{3,2},{4,5},{5,4},{6,7},{7,6},{8,9},{9,8},{10,11... | collective-permute-start | bytes 98312 | tf_op jit(solution)/shard_map/ppermute | solution.py:239
  33.7 10.2 %all-to-all-start.2 = ((bf16[8,8,512]{2,1,0:T(8,128)(2,1)}), bf16[8,8,512]{2,1,0:T(8,128)(2,1)S(1)}, u32[]{:S(2)}, u32[]{:S(2)}) async-start(bf16[8,8,512]{2,1,0:T(8,128)(2,1)} %get-tuple-element.17), calls=%async_computation.2 | async-start | bytes 131072 | tf_op jit(solution)/shard_map/all_to_all | solution.py:252
  43.9 10.8 %copy-start.2 = (bf16[2,512,2048]{2,1,0:T(8,128)(2,1)S(1)}, bf16[2,512,2048]{2,1,0:T(8,128)(2,1)}, u32[]{:S(2)}) copy-start(bf16[2,512,2048]{2,1,0:T(8,128)(2,1)} %w_out.3) | copy-start | bytes 12582916
  55.2 3.7 %collective-permute-start.5 = (bf16[8,2048]{1,0:T(8,128)(2,1)S(1)}, bf16[8,2048]{1,0:T(8,128)(2,1)S(1)}, u32[]{:S(2)}, u32[]{:S(2)}) collective-permute-start(bf16[8,2048]{1,0:T(8,128)(2,1)S(1)} %share.3.rest_0_), channel_id=1, source_target_pairs={{0,3},{1,2},{2,1},{3,0},{4,7},{5,6},{6,5},{7,4},{8,11},{9,10},{10,... | collective-permute-start | bytes 98312 | tf_op jit(solution)/shard_map/ppermute | solution.py:239
  55.2 4.0 %collective-permute-start.4 = (bf16[8,2048]{1,0:T(8,128)(2,1)S(1)}, bf16[8,2048]{1,0:T(8,128)(2,1)S(1)}, u32[]{:S(2)}, u32[]{:S(2)}) collective-permute-start(bf16[8,2048]{1,0:T(8,128)(2,1)S(1)} %share.3.rest_0_), channel_id=1, source_target_pairs={{0,2},{1,3},{2,0},{3,1},{4,6},{5,7},{6,4},{7,5},{8,10},{9,11},{10,... | collective-permute-start | bytes 98312 | tf_op jit(solution)/shard_map/ppermute | solution.py:239
  56.8 2.5 %collective-permute-start.3 = (bf16[8,2048]{1,0:T(8,128)(2,1)S(1)}, bf16[8,2048]{1,0:T(8,128)(2,1)S(1)}, u32[]{:S(2)}, u32[]{:S(2)}) collective-permute-start(bf16[8,2048]{1,0:T(8,128)(2,1)S(1)} %share.3.rest_0_), channel_id=1, source_target_pairs={{0,1},{1,0},{2,3},{3,2},{4,5},{5,4},{6,7},{7,6},{8,9},{9,8},{10,11... | collective-permute-start | bytes 98312 | tf_op jit(solution)/shard_map/ppermute | solution.py:239

commit v3 on v2

--- a/solution.py
+++ b/solution.py
@@ -13,6 +13,9 @@
 LANES = 128
 SUBLANES = 8
 VMEM = pltpu.VMEM
+IN_VMEM = pl.BlockSpec(memory_space=pltpu.VMEM)
+IN_PLACE = pl.BlockSpec(memory_space=pl.ANY)
+PIECES = 4
 
 
 def whole(shape):
@@ -35,41 +38,93 @@
     return pl.CostEstimate(flops=flops, bytes_accessed=moved, transcendentals=0)
 
 
-def source_kernel(layer, source, gain, w_key, w_value, keys, values, normed):
-    @pl.when(pl.program_id(0) == 0)
-    def _():
-        rows = source[...].astype(jnp.float32)
-        gains = gain[layer : layer + 1, :]
-        normed[...] = (rows * row_scale(rows) * gains).astype(jnp.bfloat16)
-
-    key = jnp.dot(normed[...], w_key[0], preferred_element_type=jnp.float32)
-    keys[...] = (key * row_scale(key)).astype(jnp.bfloat16)
-    value = jnp.dot(normed[...], w_value[0], preferred_element_type=jnp.float32)
-    values[...] = value.astype(jnp.bfloat16)
-
-
-def source_side(layer, source, gain, w_key, w_value):
+def keys_of(normed, weight, keys):
+    raw = jnp.dot(normed, weight, preferred_element_type=jnp.float32)
+    for start in range(0, keys.shape[1], HEAD_DIM):
+        head = raw[:, start : start + HEAD_DIM]
+        keys[:, start : start + HEAD_DIM] = (head * row_scale(head)).astype(jnp.bfloat16)
+
+
+def values_of(normed, weight, values):
+    raw = jnp.dot(normed, weight, preferred_element_type=jnp.float32)
+    values[...] = raw.astype(jnp.bfloat16)
+
+
+def streaming_source_kernel(layer, source, gain, w_key, w_value, keys, values, *scratch):
+    rows, gains, held_key, held_value, arrived = scratch
+    depth = w_key.shape[1] // PIECES
+    copies = [
+        pltpu.make_async_copy(source, rows, arrived.at[0]),
+        pltpu.make_async_copy(gain, gains, arrived.at[1]),
+    ]
+    for weight, held in ((w_key, held_key), (w_value, held_value)):
+        for piece in range(PIECES):
+            cut = pl.ds(piece * depth, depth)
+            copies.append(
+                pltpu.make_async_copy(
+                    weight.at[layer, cut, :], held.at[cut, :], arrived.at[len(copies)]
+                )
+            )
+    for copy in copies:
+        copy.start()
+    copies[0].wait()
+    copies[1].wait()
+    normed = normed_rows(rows[...].astype(jnp.float32), gains[layer : layer + 1, :])
+    for copy in copies[2 : 2 + PIECES]:
+        copy.wait()
+    keys_of(normed, held_key[...], keys)
+    for copy in copies[2 + PIECES :]:
+        copy.wait()
+    values_of(normed, held_value[...], values)
+
+
+def source_kernel(layer, source, gain, w_key, w_value, keys, values):
+    normed = normed_rows(source[...].astype(jnp.float32), gain[layer : layer + 1, :])
+    keys_of(normed, w_key[0], keys)
+    values_of(normed, w_value[0], values)
+
+
+def source_side(layer, source, gain, w_key, w_value, streaming):
     _, width, columns = w_key.shape
     rows = source.shape[0]
-    weight = pl.BlockSpec((1, width, HEAD_DIM), lambda h: (layer, 0, h))
-    out = pl.BlockSpec((rows, HEAD_DIM), lambda h: (0, h))
     shape = jax.ShapeDtypeStruct((rows, columns), jnp.bfloat16)
+    common = dict(
+        out_shape=[shape, shape],
+        cost_estimate=cost(4 * rows * width * columns, 4 * width * columns),
+        name="source_side",
+    )
+    if streaming:
+        return pl.pallas_call(
+            functools.partial(streaming_source_kernel, layer),
+            in_specs=[IN_PLACE] * 4,
+            out_specs=[IN_VMEM] * 2,
+            scratch_shapes=[
+                VMEM(source.shape, source.dtype),
+                VMEM(gain.shape, gain.dtype),
+                VMEM((width, columns), jnp.bfloat16),
+                VMEM((width, columns), jnp.bfloat16),
+                pltpu.SemaphoreType.DMA((2 + 2 * PIECES,)),
+            ],
+            compiler_params=pltpu.CompilerParams(vmem_limit_bytes=16 << 20),
+            **common,
+        )(in_hbm(source), in_hbm(gain), in_hbm(w_key), in_hbm(w_value))
+    weight = layer_of(w_key.shape, layer)
     return pl.pallas_call(
         functools.partial(source_kernel, layer),
-        grid=(columns // HEAD_DIM,),
+        grid=(1,),
         in_specs=[whole(source.shape), whole(gain.shape), weight, weight],
-        out_specs=[out, out],
-        out_shape=[shape, shape],
-        scratch_shapes=[VMEM((rows, width), jnp.bfloat16)],
-        cost_estimate=cost(4 * rows * width * columns, 4 * width * columns),
-        compiler_params=pltpu.CompilerParams(vmem_limit_bytes=16 << 20),
-        name="source_side",
-    )(source, gain, in_hbm(w_key), in_hbm(w_value))
-
-
-def project(hidden, gains, weight, queries):
-    normed = (hidden * row_scale(hidden) * gains).astype(jnp.bfloat16)
+        out_specs=[whole(shape.shape)] * 2,
+        compiler_params=pltpu.CompilerParams(vmem_limit_bytes=12 << 20),
+        **common,
+    )(source, gain, w_key, w_value)
+
+
+def project(normed, weight, queries):
     raw = jnp.dot(normed, weight, preferred_element_type=jnp.float32)
+    spread(raw, queries)
+
+
+def spread(raw, queries):
     rows, columns = raw.shape
     for start in range(0, columns, HEAD_DIM):
         head = raw[:, start : start + HEAD_DIM]
@@ -83,10 +138,35 @@
         )
 
 
-def first_kernel(layer, hidden, gain, w_query, queries):
-    project(
-        hidden[...].astype(jnp.float32), gain[layer : layer + 1, :], w_query[0], queries
-    )
+def normed_rows(rows, gains):
+    return (rows * row_scale(rows) * gains).astype(jnp.bfloat16)
+
+
+def first_kernel(layer, hidden, gain, w_query, queries, rows, gains, held, arrived):
+    depth = held.shape[1]
+    copies = [
+        pltpu.make_async_copy(hidden, rows, arrived.at[PIECES]),
+        pltpu.make_async_copy(gain, gains, arrived.at[PIECES + 1]),
+    ]
+    for piece in range(PIECES):
+        copies.append(
+            pltpu.make_async_copy(
+                w_query.at[layer, pl.ds(piece * depth, depth), :],
+                held.at[piece],
+                arrived.at[piece],
+            )
+        )
+    for copy in copies:
+        copy.start()
+    copies[0].wait()
+    copies[1].wait()
+    normed = normed_rows(rows[...].astype(jnp.float32), gains[layer : layer + 1, :])
+    raw = jnp.zeros((rows.shape[0], held.shape[2]), jnp.float32)
+    for piece in range(PIECES):
+        copies[2 + piece].wait()
+        cut = slice(piece * depth, (piece + 1) * depth)
+        raw = raw + jnp.dot(normed[:, cut], held[piece], preferred_element_type=jnp.float32)
+    spread(raw, queries)
 
 
 def branch_of(shares, rows):
@@ -101,7 +181,7 @@
     branch = branch_of(shares, hidden.shape[0])
     after = (hidden[...].astype(jnp.float32) + branch).astype(jnp.bfloat16)
     result[...] = after
-    project(after.astype(jnp.float32), gain[layer : layer + 1, :], w_query[0], queries)
+    project(normed_rows(after.astype(jnp.float32), gain[layer : layer + 1, :]), w_query[0], queries)
 
 
 def last_kernel(hidden, *rest):
@@ -114,14 +194,15 @@
     _, width, columns = w_query.shape
     return pl.pallas_call(
         functools.partial(first_kernel, layer),
-        grid=(columns // HEAD_DIM,),
-        in_specs=[
-            whole(hidden.shape),
-            whole(gain.shape),
-            pl.BlockSpec((1, width, HEAD_DIM), lambda h: (layer, 0, h)),
+        in_specs=[IN_PLACE] * 3,
+        out_specs=IN_VMEM,
+        out_shape=jax.ShapeDtypeStruct((blocks, padded, columns), jnp.bfloat16),
+        scratch_shapes=[
+            VMEM(hidden.shape, hidden.dtype),
+            VMEM(gain.shape, gain.dtype),
+            VMEM((PIECES, width // PIECES, columns), jnp.bfloat16),
+            pltpu.SemaphoreType.DMA((PIECES + 2,)),
         ],
-        out_specs=pl.BlockSpec((blocks, padded, HEAD_DIM), lambda h: (0, 0, h)),
-        out_shape=jax.ShapeDtypeStruct((blocks, padded, columns), jnp.bfloat16),
         cost_estimate=cost(2 * padded * width * columns, 2 * width * columns),
         compiler_params=pltpu.CompilerParams(vmem_limit_bytes=8 << 20),
         name="first_queries",
@@ -174,7 +255,8 @@
         scores = lax.dot_general(
             query, keys[:, cut], (((1,), (1,)), ((), ())), preferred_element_type=jnp.float32
         )
-        weights = jnp.exp(scales[layer, head] * (scores / root - root))
+        scale = scales[layer : layer + 1, head : head + 1]
+        weights = jnp.exp(scale * (scores / root - root))
         total = jnp.sum(weights, axis=1, keepdims=True)
         high = total.astype(jnp.bfloat16).astype(jnp.float32)
         sums = jnp.where(lane == 2 * head, high, sums)
@@ -196,7 +278,7 @@
             whole(queries.shape),
             whole(keys.shape),
             whole(values.shape),
-            pl.BlockSpec(memory_space=pltpu.SMEM),
+            whole(scales.shape),
         ],
         out_specs=whole(shape),
         out_shape=jax.ShapeDtypeStruct(shape, jnp.bfloat16),
@@ -247,15 +329,18 @@
     padded = -(-target.shape[0] // SUBLANES) * SUBLANES
     hidden = target
     queries = first_queries(0, hidden, tgt_gain, w_query, blocks, padded)
-    keys, values = source_side(0, source, src_gain, w_key, w_value)
+    keys, values = source_side(0, source, src_gain, w_key, w_value, True)
     for layer in range(layers):
         queries = lax.all_to_all(queries, "sp", 0, 0)
         packed = attend(layer, queries, keys, values, score_scale)
+        packed = lax.all_to_all(packed, "sp", 0, 0)
+        share = share_of(layer, packed, w_out)
         if layer + 1 < layers:
-            source, packed = lax.optimization_barrier((source, packed))
-            keys, values = source_side(layer + 1, source, src_gain, w_key, w_value)
-        packed = lax.all_to_all(packed, "sp", 0, 0)
-        shares = over_groups(share_of(layer, packed, w_out))
+            source, share = lax.optimization_barrier((source, share))
+            keys, values = source_side(layer + 1, source, src_gain, w_key, w_value, False)
+        shares = over_groups(share)
+        if layer + 1 < layers:
+            *shares, keys, values = lax.optimization_barrier((*shares, keys, values))
         if layer + 1 < layers:
             queries, hidden = next_queries(
                 layer + 1, hidden, shares, tgt_gain, w_query, blocks, padded

time: 60.3 us -> 57.2 us (0.949)
  blocking collectives: 19.5 us -> 28.6 us
  waiting for transfers between devices: 10.8 us -> 6.31 us
  Pallas kernels: 15 us -> 10.7 us
  starting transfers between devices: 14.4 us -> 11.1 us
    all_to_all x0 -> x1, blocking collectives: none -> 9.29 us  [body(): queries = lax.all_to_all(queries, 'sp', 0, 0)]
    all_to_all x2 -> x1, starting transfers between devices: 10.7 us -> 7.32 us  [body(): queries = lax.all_to_all(queries, 'sp', 0, 0)]
    all_to_all x2 -> x1, waiting for transfers between devices: 6.44 us -> 3.44 us  [body(): queries = lax.all_to_all(queries, 'sp', 0, 0)]
    pallas_call x3, Pallas kernels: 10 us -> 7.44 us  [the longest x1 3.45 us: source_side(): pl.pallas_call(functools.partial(streaming_source_kernel, layer), in_spec...]
    ppermute x6, waiting for transfers between devices: 4.36 us -> 2.87 us  [over_groups(): lax.ppermute(share, 'tp', [(i, (i ^ m) % count) for i in range(count)])]
    pallas_call x2, Pallas kernels: 2.12 us -> 1.05 us  [attend(): pl.pallas_call(functools.partial(attend_kernel, layer), grid=(1,), in_spe...]
    pallas_call x1, Pallas kernels: 1.19 us -> 0.58 us  [next_queries(): pl.pallas_call(functools.partial(next_kernel, layer), grid=(1,), in_specs...]
  transfers between devices with their start and end apart: 8 -> 7, of which waited for: 6 -> 5; matrix products, arithmetic and copies ran while one was open for 0% -> 0% of each run, Pallas kernels for 12% -> 9%
where the time goes in v3:
time: 57.2 us; the launch traced here: 56.9 us
  blocking collectives  28.6 us (50%)
  starting transfers between devices  11.1 us (19%)
  Pallas kernels  10.7 us (19%)
  waiting for transfers between devices  6.31 us (11%)
    all_to_all x2, blocking collectives, body(): packed = lax.all_to_all(packed, 'sp', 0, 0)  19.3 us
    all_to_all x1, blocking collectives, body(): queries = lax.all_to_all(queries, 'sp', 0, 0)  9.29 us
    all_to_all x1, starting transfers between devices, body(): queries = lax.all_to_all(queries, 'sp', 0, 0)  7.32 us
    ppermute x6, starting transfers between devices, over_groups(): lax.ppermute(share, 'tp', [(i, (i ^ m) % count) for i in range(count)])  3.78 us
    pallas_call x1, Pallas kernels, source_side(): pl.pallas_call(functools.partial(streaming_source_kernel, layer), in_spec...  3.45 us
    all_to_all x1, waiting for transfers between devices, body(): queries = lax.all_to_all(queries, 'sp', 0, 0)  3.44 us
    ppermute x6, waiting for transfers between devices, over_groups(): lax.ppermute(share, 'tp', [(i, (i ^ m) % count) for i in range(count)])  2.87 us
    pallas_call x1, Pallas kernels, first_queries(): pl.pallas_call(functools.partial(first_kernel, layer), in_specs=[IN_PLACE...  2.51 us
  transfers between devices with their start and end apart: 7, of which 5 were waited for; matrix products, arithmetic and copies ran while one was open for 0% of the time, Pallas kernels for 9%

profile of v3, /device:TPU:0, one launch (start us, length us, event | category | flops | bytes accessed | tf_op | source)
XLA Modules:
  0.0 56.9 jit_solution(14520395425831326816)
XLA Ops:
  0.0 2.5 %first_queries.1 = bf16[8,8,512]{2,1,0:T(8,128)(2,1)} custom-call(bf16[7,2048]{1,0:T(8,128)(2,1)} %hidden.3, f32[2,2048]{1,0:T(2,128)} %gain.7, bf16[2,2048,512]{2,1,0:T(8,128)(2,1)} %w_query.3), custom_call_target="tpu_custom_call" | custom-call | flops 16777216 | bytes 2097152 | tf_op jit(solution)/shard_map/first_queries/pallas_call | solution.py:195
  2.5 7.3 %all-to-all-start = ((bf16[8,8,512]{2,1,0:T(8,128)(2,1)}), bf16[8,8,512]{2,1,0:T(8,128)(2,1)S(1)}, u32[]{:S(2)}, u32[]{:S(2)}) async-start(bf16[8,8,512]{2,1,0:T(8,128)(2,1)} %first_queries.1), calls=%async_computation | async-start | bytes 131072 | tf_op jit(solution)/shard_map/all_to_all | solution.py:334
  9.8 3.5 %source_side.2 = (bf16[256,512]{1,0:T(8,128)(2,1)S(1)}, bf16[256,512]{1,0:T(8,128)(2,1)S(1)}) custom-call(bf16[256,2048]{1,0:T(8,128)(2,1)} %source.2, f32[2,2048]{1,0:T(2,128)} %gain.6, bf16[2,2048,512]{2,1,0:T(8,128)(2,1)} %w_key.3, bf16[2,2048,512]{2,1,0:T(8,128)(2,1)} %w_value.3), custom_call_target="tpu_custom_call" | custom-call | flops 1073741824 | bytes 4194304 | tf_op jit(solution)/shard_map/source_side/pallas_call | solution.py:97
  13.3 3.4 %all-to-all-done.queries = bf16[8,8,512]{2,1,0:T(8,128)(2,1)S(1)} async-done(((bf16[8,8,512]{2,1,0:T(8,128)(2,1)}), bf16[8,8,512]{2,1,0:T(8,128)(2,1)S(1)}, u32[]{:S(2)}, u32[]{:S(2)}) %all-to-all-start) | async-done | bytes 65568 | tf_op jit(solution)/shard_map/all_to_all | solution.py:334
  16.7 0.0 copy-done.8
  16.8 0.5 attend.2
  17.3 0.0 copy-start
  17.3 0.0 copy-start.6
  17.3 9.9 %all_to_all.20.packed = bf16[8,8,640]{2,1,0:T(8,128)(2,1)S(1)} all-to-all(bf16[8,8,640]{2,1,0:T(8,128)(2,1)S(1)} %attend.2), channel_id=1, replica_groups=mesh['sp'=8,'tp'=4] {'sp'}, dimensions={0} | all-to-all | bytes 163840 | tf_op jit(solution)/shard_map/all_to_all | solution.py:336
  27.2 0.5 share.2.rest_0_
  27.8 0.1 collective-permute-start.2
  27.8 1.6 %collective-permute-start.1 = (bf16[8,2048]{1,0:T(8,128)(2,1)S(1)}, bf16[8,2048]{1,0:T(8,128)(2,1)S(1)}, u32[]{:S(2)}, u32[]{:S(2)}) collective-permute-start(bf16[8,2048]{1,0:T(8,128)(2,1)S(1)} %share.2.rest_0_), channel_id=1, source_target_pairs={{0,2},{1,3},{2,0},{3,1},{4,6},{5,7},{6,4},{7,5},{8,10},{9,11},{10,... | collective-permute-start | bytes 98312 | tf_op jit(solution)/shard_map/ppermute | solution.py:321
  29.4 0.3 collective-permute-start
  29.7 0.0 copy-done.4
  29.7 1.5 %source_side.3 = (bf16[256,512]{1,0:T(8,128)(2,1)S(1)}, bf16[256,512]{1,0:T(8,128)(2,1)S(1)}) custom-call(bf16[256,2048]{1,0:T(8,128)(2,1)S(1)} %copy-done.4, f32[2,2048]{1,0:T(2,128)S(1)} %copy-done.6, bf16[2,2048,512]{2,1,0:T(8,128)(2,1)S(1)} %copy-done, bf16[2,2048,512]{2,1,0:T(8,128)(2,1)S(1)} %copy-done.1), custom_call_target="tpu_custom_call" | custom-call | flops 1073741824 | bytes 4194304 | tf_op jit(solution)/shard_map/source_side/pallas_call | solution.py:112
  31.2 0.3 collective-permute-done.2.rest_3_
  31.5 0.4 collective-permute-done.1.rest_2_
  31.9 0.0 collective-permute-done.rest_1_
  31.9 0.0 copy-done.5
  31.9 0.0 copy-done.7
  31.9 0.6 %next_queries.1 = (bf16[8,8,512]{2,1,0:T(8,128)(2,1)S(1)}, bf16[7,2048]{1,0:T(8,128)(2,1)S(1)}) custom-call(bf16[7,2048]{1,0:T(8,128)(2,1)S(1)} %copy-done.5, f32[2,2048]{1,0:T(2,128)S(1)} %copy-done.7, bf16[2,2048,512]{2,1,0:T(8,128)(2,1)S(1)} %copy-done.2, bf16[8,2048]{1,0:T(8,128)(2,1)S(1)} %share.2.rest_0_, ...), custom_call_target="tpu_custom_call" | custom-call | flops 16777216 | bytes 2097152 | tf_op jit(solution)/shard_map/next_queries/pallas_call | solution.py:214
  32.5 9.3 %all_to_all.21.queries = bf16[8,8,512]{2,1,0:T(8,128)(2,1)S(1)} all-to-all(bf16[8,8,512]{2,1,0:T(8,128)(2,1)S(1)} %get-tuple-element.30), channel_id=1, replica_groups=mesh['sp'=8,'tp'=4] {'sp'}, dimensions={0} | all-to-all | bytes 131072 | tf_op jit(solution)/shard_map/all_to_all | solution.py:334
  41.8 0.5 attend.3
  42.3 9.4 %all_to_all.22.packed = bf16[8,8,640]{2,1,0:T(8,128)(2,1)S(1)} all-to-all(bf16[8,8,640]{2,1,0:T(8,128)(2,1)S(1)} %attend.3), channel_id=1, replica_groups=mesh['sp'=8,'tp'=4] {'sp'}, dimensions={0} | all-to-all | bytes 163840 | tf_op jit(solution)/shard_map/all_to_all | solution.py:336
  51.7 0.5 share.3.rest_0_
  52.2 0.0 collective-permute-start.5
  52.2 1.6 %collective-permute-start.4 = (bf16[8,2048]{1,0:T(8,128)(2,1)S(1)}, bf16[8,2048]{1,0:T(8,128)(2,1)S(1)}, u32[]{:S(2)}, u32[]{:S(2)}) collective-permute-start(bf16[8,2048]{1,0:T(8,128)(2,1)S(1)} %share.3.rest_0_), channel_id=1, source_target_pairs={{0,2},{1,3},{2,0},{3,1},{4,6},{5,7},{6,4},{7,5},{8,10},{9,11},{10,... | collective-permute-start | bytes 98312 | tf_op jit(solution)/shard_map/ppermute | solution.py:321
  53.8 0.3 collective-permute-start.3
  54.1 1.8 %collective-permute-done.5.rest_3_ = bf16[8,2048]{1,0:T(8,128)(2,1)S(1)} collective-permute-done((bf16[8,2048]{1,0:T(8,128)(2,1)S(1)}, bf16[8,2048]{1,0:T(8,128)(2,1)S(1)}, u32[]{:S(2)}, u32[]{:S(2)}) %collective-permute-start.5) | collective-permute-done | bytes 32800 | tf_op jit(solution)/shard_map/ppermute | solution.py:321
  55.8 0.4 collective-permute-done.4.rest_2_
  56.2 0.0 collective-permute-done.3.rest_1_
  56.2 0.6 %last_rows.1 = bf16[7,2048]{1,0:T(8,128)(2,1)} custom-call(bf16[7,2048]{1,0:T(8,128)(2,1)S(1)} %get-tuple-element.29.hidden, bf16[8,2048]{1,0:T(8,128)(2,1)S(1)} %share.3.rest_0_, bf16[8,2048]{1,0:T(8,128)(2,1)S(1)} %collective-permute-done.3.rest_1_, bf16[8,2048]{1,0:T(8,128)(2,1)S(1)} %collective-permute-done.4.rest_2_, ...), custom_call_target="tpu_custom_call" | custom-call | tf_op jit(solution)/shard_map/last_rows/pallas_call | solution.py:235
  (12 shorter events, 0.0 us)
Async XLA Ops:
  2.5 14.2 %all-to-all-start = ((bf16[8,8,512]{2,1,0:T(8,128)(2,1)}), bf16[8,8,512]{2,1,0:T(8,128)(2,1)S(1)}, u32[]{:S(2)}, u32[]{:S(2)}) async-start(bf16[8,8,512]{2,1,0:T(8,128)(2,1)} %first_queries.1), calls=%async_computation | async-start | bytes 131072 | tf_op jit(solution)/shard_map/all_to_all | solution.py:334
  9.8 6.9 %copy-start.8 = (f32[2,2]{1,0:T(2,128)S(1)}, f32[2,2]{1,0:T(2,128)}, u32[]{:S(2)}) copy-start(f32[2,2]{1,0:T(2,128)} %scales.3) | copy-start | bytes 52
  16.8 10.5 %copy-start.3 = (bf16[2,512,2048]{2,1,0:T(8,128)(2,1)S(1)}, bf16[2,512,2048]{2,1,0:T(8,128)(2,1)}, u32[]{:S(2)}) copy-start(bf16[2,512,2048]{2,1,0:T(8,128)(2,1)} %w_out.3) | copy-start | bytes 12582916
  16.8 12.9 %copy-start.1 = (bf16[2,2048,512]{2,1,0:T(8,128)(2,1)S(1)}, bf16[2,2048,512]{2,1,0:T(8,128)(2,1)}, u32[]{:S(2)}) copy-start(bf16[2,2048,512]{2,1,0:T(8,128)(2,1)} %w_value.3) | copy-start | bytes 12582916
  16.8 12.9 %copy-start.4 = (bf16[256,2048]{1,0:T(8,128)(2,1)S(1)}, bf16[256,2048]{1,0:T(8,128)(2,1)}, u32[]{:S(2)}) copy-start(bf16[256,2048]{1,0:T(8,128)(2,1)} %source.2) | copy-start | bytes 3145732
  17.3 12.4 %copy-start = (bf16[2,2048,512]{2,1,0:T(8,128)(2,1)S(1)}, bf16[2,2048,512]{2,1,0:T(8,128)(2,1)}, u32[]{:S(2)}) copy-start(bf16[2,2048,512]{2,1,0:T(8,128)(2,1)} %w_key.3) | copy-start | bytes 12582916
  17.3 12.4 %copy-start.6 = (f32[2,2048]{1,0:T(2,128)S(1)}, f32[2,2048]{1,0:T(2,128)}, u32[]{:S(2)}) copy-start(f32[2,2048]{1,0:T(2,128)} %gain.6) | copy-start | bytes 49156
  27.7 4.1 %copy-start.2 = (bf16[2,2048,512]{2,1,0:T(8,128)(2,1)S(1)}, bf16[2,2048,512]{2,1,0:T(8,128)(2,1)}, u32[]{:S(2)}) copy-start(bf16[2,2048,512]{2,1,0:T(8,128)(2,1)} %w_query.3) | copy-start | bytes 12582916
  27.7 4.1 %copy-start.5 = (bf16[7,2048]{1,0:T(8,128)(2,1)S(1)}, bf16[7,2048]{1,0:T(8,128)(2,1)}, u32[]{:S(2)}) copy-start(bf16[7,2048]{1,0:T(8,128)(2,1)} %hidden.3) | copy-start | bytes 86020
  27.7 4.1 %copy-start.7 = (f32[2,2048]{1,0:T(2,128)S(1)}, f32[2,2048]{1,0:T(2,128)}, u32[]{:S(2)}) copy-start(f32[2,2048]{1,0:T(2,128)} %gain.7) | copy-start | bytes 49156
  27.8 3.7 %collective-permute-start.2 = (bf16[8,2048]{1,0:T(8,128)(2,1)S(1)}, bf16[8,2048]{1,0:T(8,128)(2,1)S(1)}, u32[]{:S(2)}, u32[]{:S(2)}) collective-permute-start(bf16[8,2048]{1,0:T(8,128)(2,1)S(1)} %share.2.rest_0_), channel_id=1, source_target_pairs={{0,3},{1,2},{2,1},{3,0},{4,7},{5,6},{6,5},{7,4},{8,11},{9,10},{10,... | collective-permute-start | bytes 98312 | tf_op jit(solution)/shard_map/ppermute | solution.py:321
  27.8 4.0 %collective-permute-start.1 = (bf16[8,2048]{1,0:T(8,128)(2,1)S(1)}, bf16[8,2048]{1,0:T(8,128)(2,1)S(1)}, u32[]{:S(2)}, u32[]{:S(2)}) collective-permute-start(bf16[8,2048]{1,0:T(8,128)(2,1)S(1)} %share.2.rest_0_), channel_id=1, source_target_pairs={{0,2},{1,3},{2,0},{3,1},{4,6},{5,7},{6,4},{7,5},{8,10},{9,11},{10,... | collective-permute-start | bytes 98312 | tf_op jit(solution)/shard_map/ppermute | solution.py:321
  29.4 2.5 %collective-permute-start = (bf16[8,2048]{1,0:T(8,128)(2,1)S(1)}, bf16[8,2048]{1,0:T(8,128)(2,1)S(1)}, u32[]{:S(2)}, u32[]{:S(2)}) collective-permute-start(bf16[8,2048]{1,0:T(8,128)(2,1)S(1)} %share.2.rest_0_), channel_id=1, source_target_pairs={{0,1},{1,0},{2,3},{3,2},{4,5},{5,4},{6,7},{7,6},{8,9},{9,8},{10,11... | collective-permute-start | bytes 98312 | tf_op jit(solution)/shard_map/ppermute | solution.py:321
  52.2 3.7 %collective-permute-start.5 = (bf16[8,2048]{1,0:T(8,128)(2,1)S(1)}, bf16[8,2048]{1,0:T(8,128)(2,1)S(1)}, u32[]{:S(2)}, u32[]{:S(2)}) collective-permute-start(bf16[8,2048]{1,0:T(8,128)(2,1)S(1)} %share.3.rest_0_), channel_id=1, source_target_pairs={{0,3},{1,2},{2,1},{3,0},{4,7},{5,6},{6,5},{7,4},{8,11},{9,10},{10,... | collective-permute-start | bytes 98312 | tf_op jit(solution)/shard_map/ppermute | solution.py:321
  52.2 4.0 %collective-permute-start.4 = (bf16[8,2048]{1,0:T(8,128)(2,1)S(1)}, bf16[8,2048]{1,0:T(8,128)(2,1)S(1)}, u32[]{:S(2)}, u32[]{:S(2)}) collective-permute-start(bf16[8,2048]{1,0:T(8,128)(2,1)S(1)} %share.3.rest_0_), channel_id=1, source_target_pairs={{0,2},{1,3},{2,0},{3,1},{4,6},{5,7},{6,4},{7,5},{8,10},{9,11},{10,... | collective-permute-start | bytes 98312 | tf_op jit(solution)/shard_map/ppermute | solution.py:321
  53.8 2.5 %collective-permute-start.3 = (bf16[8,2048]{1,0:T(8,128)(2,1)S(1)}, bf16[8,2048]{1,0:T(8,128)(2,1)S(1)}, u32[]{:S(2)}, u32[]{:S(2)}) collective-permute-start(bf16[8,2048]{1,0:T(8,128)(2,1)S(1)} %share.3.rest_0_), channel_id=1, source_target_pairs={{0,1},{1,0},{2,3},{3,2},{4,5},{5,4},{6,7},{7,6},{8,9},{9,8},{10,11... | collective-permute-start | bytes 98312 | tf_op jit(solution)/shard_map/ppermute | solution.py:321

commit v4 on v3

--- a/solution.py
+++ b/solution.py
@@ -315,6 +315,13 @@
     )(packed, w_out)
 
 
+def exchange(blocks):
+    count = blocks.shape[0]
+    first = count // 2 + 1
+    order = [(first + place) % count for place in range(count)]
+    return lax.all_to_all(blocks, "sp", 0, 0, axis_index_groups=[order])
+
+
 def over_groups(share):
     count = lax.axis_size("tp")
     return [share] + [
@@ -331,9 +338,9 @@
     queries = first_queries(0, hidden, tgt_gain, w_query, blocks, padded)
     keys, values = source_side(0, source, src_gain, w_key, w_value, True)
     for layer in range(layers):
-        queries = lax.all_to_all(queries, "sp", 0, 0)
+        queries = exchange(queries)
         packed = attend(layer, queries, keys, values, score_scale)
-        packed = lax.all_to_all(packed, "sp", 0, 0)
+        packed = exchange(packed)
         share = share_of(layer, packed, w_out)
         if layer + 1 < layers:
             source, share = lax.optimization_barrier((source, share))

time: 57.2 us -> 52.5 us (0.918)
  waiting for transfers between devices: 6.31 us -> 3.05 us
  blocking collectives: 28.6 us -> 26.2 us
  starting transfers between devices: 11.1 us -> 12.1 us
    all_to_all x1, waiting for transfers between devices: 3.44 us -> 0.17 us  [exchange(): return lax.all_to_all(blocks, 'sp', 0, 0, axis_index_groups=[order])]
    all_to_all x3, blocking collectives: 28.6 us -> 26.2 us  [exchange(): return lax.all_to_all(blocks, 'sp', 0, 0, axis_index_groups=[order])]
    all_to_all x1, starting transfers between devices: 7.32 us -> 8.3 us  [exchange(): return lax.all_to_all(blocks, 'sp', 0, 0, axis_index_groups=[order])]
where the time goes in v4:
time: 52.5 us; the launch traced here: 52.2 us
  blocking collectives  26.2 us (50%)
  starting transfers between devices  12.1 us (23%)
  Pallas kernels  10.7 us (20%)
  waiting for transfers between devices  3.05 us (6%)
    all_to_all x3, blocking collectives, exchange(): return lax.all_to_all(blocks, 'sp', 0, 0, axis_index_groups=[order])  26.2 us
    all_to_all x1, starting transfers between devices, exchange(): return lax.all_to_all(blocks, 'sp', 0, 0, axis_index_groups=[order])  8.3 us
    ppermute x6, starting transfers between devices, over_groups(): lax.ppermute(share, 'tp', [(i, (i ^ m) % count) for i in range(count)])  3.78 us
    pallas_call x1, Pallas kernels, source_side(): pl.pallas_call(functools.partial(streaming_source_kernel, layer), in_spec...  3.46 us
    ppermute x6, waiting for transfers between devices, over_groups(): lax.ppermute(share, 'tp', [(i, (i ^ m) % count) for i in range(count)])  2.88 us
    pallas_call x1, Pallas kernels, first_queries(): pl.pallas_call(functools.partial(first_kernel, layer), in_specs=[IN_PLACE...  2.51 us
    pallas_call x1, Pallas kernels, source_side(): pl.pallas_call(functools.partial(source_kernel, layer), grid=(1,), in_spe...  1.46 us
    pallas_call x2, Pallas kernels, attend(): pl.pallas_call(functools.partial(attend_kernel, layer), grid=(1,), in_spe...  1.05 us
  transfers between devices with their start and end apart: 7, of which 5 were waited for; matrix products, arithmetic and copies ran while one was open for 0% of the time, Pallas kernels for 9%

profile of v4, /device:TPU:0, one launch (start us, length us, event | category | flops | bytes accessed | tf_op | source)
XLA Modules:
  0.0 52.2 jit_solution(17738809912189445055)
XLA Ops:
  0.0 2.5 %first_queries.1 = bf16[8,8,512]{2,1,0:T(8,128)(2,1)} custom-call(bf16[7,2048]{1,0:T(8,128)(2,1)} %hidden.3, f32[2,2048]{1,0:T(2,128)} %gain.7, bf16[2,2048,512]{2,1,0:T(8,128)(2,1)} %w_query.3), custom_call_target="tpu_custom_call" | custom-call | flops 16777216 | bytes 2097152 | tf_op jit(solution)/shard_map/first_queries/pallas_call | solution.py:195
  2.5 8.3 %all-to-all-start = ((bf16[8,8,512]{2,1,0:T(8,128)(2,1)}), bf16[8,8,512]{2,1,0:T(8,128)(2,1)S(1)}, u32[]{:S(2)}, u32[]{:S(2)}) async-start(bf16[8,8,512]{2,1,0:T(8,128)(2,1)} %first_queries.1), calls=%async_computation | async-start | bytes 131072 | tf_op jit(solution)/shard_map/all_to_all | solution.py:322
  10.8 3.5 %source_side.2 = (bf16[256,512]{1,0:T(8,128)(2,1)S(1)}, bf16[256,512]{1,0:T(8,128)(2,1)S(1)}) custom-call(bf16[256,2048]{1,0:T(8,128)(2,1)} %source.2, f32[2,2048]{1,0:T(2,128)} %gain.6, bf16[2,2048,512]{2,1,0:T(8,128)(2,1)} %w_key.3, bf16[2,2048,512]{2,1,0:T(8,128)(2,1)} %w_value.3), custom_call_target="tpu_custom_call" | custom-call | flops 1073741824 | bytes 4194304 | tf_op jit(solution)/shard_map/source_side/pallas_call | solution.py:97
  14.3 0.2 all-to-all-done.queries
  14.5 0.0 copy-done.8
  14.5 0.5 %attend.2 = bf16[8,8,640]{2,1,0:T(8,128)(2,1)S(1)} custom-call(bf16[8,8,512]{2,1,0:T(8,128)(2,1)S(1)} %all-to-all-done.queries, bf16[256,512]{1,0:T(8,128)(2,1)S(1)} %get-tuple-element.19.keys, bf16[256,512]{1,0:T(8,128)(2,1)S(1)} %get-tuple-element.20.values, f32[2,2]{1,0:T(2,128)S(1)} %copy-done.8), custom_call_target="tpu_custom_call" | custom-call | flops 3355443200 | bytes 524288 | tf_op jit(solution)/shard_map/attend/pallas_call | solution.py:274
  15.0 0.0 copy-start
  15.0 0.0 copy-start.6
  15.0 9.0 %all_to_all.20.packed = bf16[8,8,640]{2,1,0:T(8,128)(2,1)S(1)} all-to-all(bf16[8,8,640]{2,1,0:T(8,128)(2,1)S(1)} %attend.2), channel_id=1, replica_groups={{20,24,28,0,4,8,12,16},{21,25,29,1,5,9,13,17},{22,26,30,2,6,10,14,18},{..., dimensions={0} | all-to-all | bytes 163840 | tf_op jit(solution)/shard_map/all_to_all | solution.py:322
  24.0 0.0 copy-done.3
  24.1 0.5 share.2.rest_0_
  24.6 0.1 collective-permute-start.2
  24.6 1.6 %collective-permute-start.1 = (bf16[8,2048]{1,0:T(8,128)(2,1)S(1)}, bf16[8,2048]{1,0:T(8,128)(2,1)S(1)}, u32[]{:S(2)}, u32[]{:S(2)}) collective-permute-start(bf16[8,2048]{1,0:T(8,128)(2,1)S(1)} %share.2.rest_0_), channel_id=1, source_target_pairs={{0,2},{1,3},{2,0},{3,1},{4,6},{5,7},{6,4},{7,5},{8,10},{9,11},{10,... | collective-permute-start | bytes 98312 | tf_op jit(solution)/shard_map/ppermute | solution.py:328
  26.2 0.3 collective-permute-start
  26.5 0.0 copy-done.1
  26.5 1.5 %source_side.3 = (bf16[256,512]{1,0:T(8,128)(2,1)S(1)}, bf16[256,512]{1,0:T(8,128)(2,1)S(1)}) custom-call(bf16[256,2048]{1,0:T(8,128)(2,1)S(1)} %copy-done.4, f32[2,2048]{1,0:T(2,128)S(1)} %copy-done.6, bf16[2,2048,512]{2,1,0:T(8,128)(2,1)S(1)} %copy-done, bf16[2,2048,512]{2,1,0:T(8,128)(2,1)S(1)} %copy-done.1), custom_call_target="tpu_custom_call" | custom-call | flops 1073741824 | bytes 4194304 | tf_op jit(solution)/shard_map/source_side/pallas_call | solution.py:112
  28.0 0.3 collective-permute-done.2.rest_3_
  28.3 0.4 collective-permute-done.1.rest_2_
  28.7 0.0 collective-permute-done.rest_1_
  28.7 0.0 copy-done.2
  28.7 0.6 %next_queries.1 = (bf16[8,8,512]{2,1,0:T(8,128)(2,1)S(1)}, bf16[7,2048]{1,0:T(8,128)(2,1)S(1)}) custom-call(bf16[7,2048]{1,0:T(8,128)(2,1)S(1)} %copy-done.5, f32[2,2048]{1,0:T(2,128)S(1)} %copy-done.7, bf16[2,2048,512]{2,1,0:T(8,128)(2,1)S(1)} %copy-done.2, bf16[8,2048]{1,0:T(8,128)(2,1)S(1)} %share.2.rest_0_, ...), custom_call_target="tpu_custom_call" | custom-call | flops 16777216 | bytes 2097152 | tf_op jit(solution)/shard_map/next_queries/pallas_call | solution.py:214
  29.3 8.5 %all_to_all.21.queries = bf16[8,8,512]{2,1,0:T(8,128)(2,1)S(1)} all-to-all(bf16[8,8,512]{2,1,0:T(8,128)(2,1)S(1)} %get-tuple-element.30), channel_id=1, replica_groups={{20,24,28,0,4,8,12,16},{21,25,29,1,5,9,13,17},{22,26,30,2,6,10,14,18},{..., dimensions={0} | all-to-all | bytes 131072 | tf_op jit(solution)/shard_map/all_to_all | solution.py:322
  37.8 0.5 %attend.3 = bf16[8,8,640]{2,1,0:T(8,128)(2,1)S(1)} custom-call(bf16[8,8,512]{2,1,0:T(8,128)(2,1)S(1)} %all_to_all.21.queries, bf16[256,512]{1,0:T(8,128)(2,1)S(1)} %get-tuple-element.31.keys, bf16[256,512]{1,0:T(8,128)(2,1)S(1)} %get-tuple-element.32.values, f32[2,2]{1,0:T(2,128)S(1)} %copy-done.8), custom_call_target="tpu_custom_call" | custom-call | flops 3355443200 | bytes 524288 | tf_op jit(solution)/shard_map/attend/pallas_call | solution.py:274
  38.3 8.6 %all_to_all.22.packed = bf16[8,8,640]{2,1,0:T(8,128)(2,1)S(1)} all-to-all(bf16[8,8,640]{2,1,0:T(8,128)(2,1)S(1)} %attend.3), channel_id=1, replica_groups={{20,24,28,0,4,8,12,16},{21,25,29,1,5,9,13,17},{22,26,30,2,6,10,14,18},{..., dimensions={0} | all-to-all | bytes 163840 | tf_op jit(solution)/shard_map/all_to_all | solution.py:322
  47.0 0.5 share.3.rest_0_
  47.5 0.0 collective-permute-start.5
  47.5 1.6 %collective-permute-start.4 = (bf16[8,2048]{1,0:T(8,128)(2,1)S(1)}, bf16[8,2048]{1,0:T(8,128)(2,1)S(1)}, u32[]{:S(2)}, u32[]{:S(2)}) collective-permute-start(bf16[8,2048]{1,0:T(8,128)(2,1)S(1)} %share.3.rest_0_), channel_id=1, source_target_pairs={{0,2},{1,3},{2,0},{3,1},{4,6},{5,7},{6,4},{7,5},{8,10},{9,11},{10,... | collective-permute-start | bytes 98312 | tf_op jit(solution)/shard_map/ppermute | solution.py:328
  49.1 0.3 collective-permute-start.3
  49.4 1.8 %collective-permute-done.5.rest_3_ = bf16[8,2048]{1,0:T(8,128)(2,1)S(1)} collective-permute-done((bf16[8,2048]{1,0:T(8,128)(2,1)S(1)}, bf16[8,2048]{1,0:T(8,128)(2,1)S(1)}, u32[]{:S(2)}, u32[]{:S(2)}) %collective-permute-start.5) | collective-permute-done | bytes 32800 | tf_op jit(solution)/shard_map/ppermute | solution.py:328
  51.1 0.4 collective-permute-done.4.rest_2_
  51.5 0.0 collective-permute-done.3.rest_1_
  51.5 0.6 %last_rows.1 = bf16[7,2048]{1,0:T(8,128)(2,1)} custom-call(bf16[7,2048]{1,0:T(8,128)(2,1)S(1)} %get-tuple-element.29.hidden, bf16[8,2048]{1,0:T(8,128)(2,1)S(1)} %share.3.rest_0_, bf16[8,2048]{1,0:T(8,128)(2,1)S(1)} %collective-permute-done.3.rest_1_, bf16[8,2048]{1,0:T(8,128)(2,1)S(1)} %collective-permute-done.4.rest_2_, ...), custom_call_target="tpu_custom_call" | custom-call | tf_op jit(solution)/shard_map/last_rows/pallas_call | solution.py:235
  (12 shorter events, 0.0 us)
Async XLA Ops:
  2.5 11.9 %all-to-all-start = ((bf16[8,8,512]{2,1,0:T(8,128)(2,1)}), bf16[8,8,512]{2,1,0:T(8,128)(2,1)S(1)}, u32[]{:S(2)}, u32[]{:S(2)}) async-start(bf16[8,8,512]{2,1,0:T(8,128)(2,1)} %first_queries.1), calls=%async_computation | async-start | bytes 131072 | tf_op jit(solution)/shard_map/all_to_all | solution.py:322
  10.8 3.6 %copy-start.8 = (f32[2,2]{1,0:T(2,128)S(1)}, f32[2,2]{1,0:T(2,128)}, u32[]{:S(2)}) copy-start(f32[2,2]{1,0:T(2,128)} %scales.3) | copy-start | bytes 52
  14.5 9.6 %copy-start.3 = (bf16[2,512,2048]{2,1,0:T(8,128)(2,1)S(1)}, bf16[2,512,2048]{2,1,0:T(8,128)(2,1)}, u32[]{:S(2)}) copy-start(bf16[2,512,2048]{2,1,0:T(8,128)(2,1)} %w_out.3) | copy-start | bytes 12582916
  14.5 12.0 %copy-start.1 = (bf16[2,2048,512]{2,1,0:T(8,128)(2,1)S(1)}, bf16[2,2048,512]{2,1,0:T(8,128)(2,1)}, u32[]{:S(2)}) copy-start(bf16[2,2048,512]{2,1,0:T(8,128)(2,1)} %w_value.3) | copy-start | bytes 12582916
  14.5 12.0 %copy-start.4 = (bf16[256,2048]{1,0:T(8,128)(2,1)S(1)}, bf16[256,2048]{1,0:T(8,128)(2,1)}, u32[]{:S(2)}) copy-start(bf16[256,2048]{1,0:T(8,128)(2,1)} %source.2) | copy-start | bytes 3145732
  15.0 11.5 %copy-start = (bf16[2,2048,512]{2,1,0:T(8,128)(2,1)S(1)}, bf16[2,2048,512]{2,1,0:T(8,128)(2,1)}, u32[]{:S(2)}) copy-start(bf16[2,2048,512]{2,1,0:T(8,128)(2,1)} %w_key.3) | copy-start | bytes 12582916
  15.0 11.5 %copy-start.6 = (f32[2,2048]{1,0:T(2,128)S(1)}, f32[2,2048]{1,0:T(2,128)}, u32[]{:S(2)}) copy-start(f32[2,2048]{1,0:T(2,128)} %gain.6) | copy-start | bytes 49156
  24.5 4.1 %copy-start.2 = (bf16[2,2048,512]{2,1,0:T(8,128)(2,1)S(1)}, bf16[2,2048,512]{2,1,0:T(8,128)(2,1)}, u32[]{:S(2)}) copy-start(bf16[2,2048,512]{2,1,0:T(8,128)(2,1)} %w_query.3) | copy-start | bytes 12582916
  24.5 4.1 %copy-start.5 = (bf16[7,2048]{1,0:T(8,128)(2,1)S(1)}, bf16[7,2048]{1,0:T(8,128)(2,1)}, u32[]{:S(2)}) copy-start(bf16[7,2048]{1,0:T(8,128)(2,1)} %hidden.3) | copy-start | bytes 86020
  24.6 4.1 %copy-start.7 = (f32[2,2048]{1,0:T(2,128)S(1)}, f32[2,2048]{1,0:T(2,128)}, u32[]{:S(2)}) copy-start(f32[2,2048]{1,0:T(2,128)} %gain.7) | copy-start | bytes 49156
  24.6 3.7 %collective-permute-start.2 = (bf16[8,2048]{1,0:T(8,128)(2,1)S(1)}, bf16[8,2048]{1,0:T(8,128)(2,1)S(1)}, u32[]{:S(2)}, u32[]{:S(2)}) collective-permute-start(bf16[8,2048]{1,0:T(8,128)(2,1)S(1)} %share.2.rest_0_), channel_id=1, source_target_pairs={{0,3},{1,2},{2,1},{3,0},{4,7},{5,6},{6,5},{7,4},{8,11},{9,10},{10,... | collective-permute-start | bytes 98312 | tf_op jit(solution)/shard_map/ppermute | solution.py:328
  24.6 4.0 %collective-permute-start.1 = (bf16[8,2048]{1,0:T(8,128)(2,1)S(1)}, bf16[8,2048]{1,0:T(8,128)(2,1)S(1)}, u32[]{:S(2)}, u32[]{:S(2)}) collective-permute-start(bf16[8,2048]{1,0:T(8,128)(2,1)S(1)} %share.2.rest_0_), channel_id=1, source_target_pairs={{0,2},{1,3},{2,0},{3,1},{4,6},{5,7},{6,4},{7,5},{8,10},{9,11},{10,... | collective-permute-start | bytes 98312 | tf_op jit(solution)/shard_map/ppermute | solution.py:328
  26.2 2.5 %collective-permute-start = (bf16[8,2048]{1,0:T(8,128)(2,1)S(1)}, bf16[8,2048]{1,0:T(8,128)(2,1)S(1)}, u32[]{:S(2)}, u32[]{:S(2)}) collective-permute-start(bf16[8,2048]{1,0:T(8,128)(2,1)S(1)} %share.2.rest_0_), channel_id=1, source_target_pairs={{0,1},{1,0},{2,3},{3,2},{4,5},{5,4},{6,7},{7,6},{8,9},{9,8},{10,11... | collective-permute-start | bytes 98312 | tf_op jit(solution)/shard_map/ppermute | solution.py:328
  47.5 3.7 %collective-permute-start.5 = (bf16[8,2048]{1,0:T(8,128)(2,1)S(1)}, bf16[8,2048]{1,0:T(8,128)(2,1)S(1)}, u32[]{:S(2)}, u32[]{:S(2)}) collective-permute-start(bf16[8,2048]{1,0:T(8,128)(2,1)S(1)} %share.3.rest_0_), channel_id=1, source_target_pairs={{0,3},{1,2},{2,1},{3,0},{4,7},{5,6},{6,5},{7,4},{8,11},{9,10},{10,... | collective-permute-start | bytes 98312 | tf_op jit(solution)/shard_map/ppermute | solution.py:328
  47.5 4.0 %collective-permute-start.4 = (bf16[8,2048]{1,0:T(8,128)(2,1)S(1)}, bf16[8,2048]{1,0:T(8,128)(2,1)S(1)}, u32[]{:S(2)}, u32[]{:S(2)}) collective-permute-start(bf16[8,2048]{1,0:T(8,128)(2,1)S(1)} %share.3.rest_0_), channel_id=1, source_target_pairs={{0,2},{1,3},{2,0},{3,1},{4,6},{5,7},{6,4},{7,5},{8,10},{9,11},{10,... | collective-permute-start | bytes 98312 | tf_op jit(solution)/shard_map/ppermute | solution.py:328
  49.1 2.5 %collective-permute-start.3 = (bf16[8,2048]{1,0:T(8,128)(2,1)S(1)}, bf16[8,2048]{1,0:T(8,128)(2,1)S(1)}, u32[]{:S(2)}, u32[]{:S(2)}) collective-permute-start(bf16[8,2048]{1,0:T(8,128)(2,1)S(1)} %share.3.rest_0_), channel_id=1, source_target_pairs={{0,1},{1,0},{2,3},{3,2},{4,5},{5,4},{6,7},{7,6},{8,9},{9,8},{10,11... | collective-permute-start | bytes 98312 | tf_op jit(solution)/shard_map/ppermute | solution.py:328

commit v5 on v3

--- a/solution.py
+++ b/solution.py
@@ -315,6 +315,20 @@
     )(packed, w_out)
 
 
+def nearest_first(mesh):
+    chips = [getattr(device, "coords", (place,)) for place, device in enumerate(mesh.devices[:, 0])]
+    middle = len(chips) // 2 + 1
+
+    def distance(place):
+        return sum(abs(a - b) for a, b in zip(chips[place], chips[middle % len(chips)]))
+
+    return sorted(range(len(chips)), key=lambda place: (distance(place), -place))
+
+
+def exchange(blocks, order):
+    return lax.all_to_all(blocks, "sp", 0, 0, axis_index_groups=[order])
+
+
 def over_groups(share):
     count = lax.axis_size("tp")
     return [share] + [
@@ -323,7 +337,7 @@
     ]
 
 
-def body(target, source, tgt_gain, src_gain, w_query, w_key, w_value, w_out, score_scale):
+def body(order, target, source, tgt_gain, src_gain, w_query, w_key, w_value, w_out, score_scale):
     layers = w_query.shape[0]
     blocks = lax.axis_size("sp")
     padded = -(-target.shape[0] // SUBLANES) * SUBLANES
@@ -331,9 +345,9 @@
     queries = first_queries(0, hidden, tgt_gain, w_query, blocks, padded)
     keys, values = source_side(0, source, src_gain, w_key, w_value, True)
     for layer in range(layers):
-        queries = lax.all_to_all(queries, "sp", 0, 0)
+        queries = exchange(queries, order)
         packed = attend(layer, queries, keys, values, score_scale)
-        packed = lax.all_to_all(packed, "sp", 0, 0)
+        packed = exchange(packed, order)
         share = share_of(layer, packed, w_out)
         if layer + 1 < layers:
             source, share = lax.optimization_barrier((source, share))
@@ -362,4 +376,5 @@
         P(None, "tp", None),
         P(None, "tp"),
     )
-    return jax.shard_map(body, mesh=mesh, in_specs=placed, out_specs=P("sp", None), check_vma=False)
+    step = functools.partial(body, nearest_first(mesh))
+    return jax.shard_map(step, mesh=mesh, in_specs=placed, out_specs=P("sp", None), check_vma=False)

time: 57.2 us -> 52.1 us (0.911)
  waiting for transfers between devices: 6.31 us -> 2.87 us
  blocking collectives: 28.6 us -> 25.8 us
  starting transfers between devices: 11.1 us -> 12.1 us
    all_to_all x1, waiting for transfers between devices: 3.44 us -> 0.01 us  [exchange(): return lax.all_to_all(blocks, 'sp', 0, 0, axis_index_groups=[order])]
    all_to_all x3, blocking collectives: 28.6 us -> 25.8 us  [exchange(): return lax.all_to_all(blocks, 'sp', 0, 0, axis_index_groups=[order])]
    all_to_all x1, starting transfers between devices: 7.32 us -> 8.32 us  [exchange(): return lax.all_to_all(blocks, 'sp', 0, 0, axis_index_groups=[order])]
  transfers between devices with their start and end apart: 7 -> 7, of which waited for: 5 -> 4; matrix products, arithmetic and copies ran while one was open for 0% -> 0% of each run, Pallas kernels for 9% -> 10%
where the time goes in v5:
time: 52.1 us; the launch traced here: 51.7 us
  blocking collectives  25.8 us (50%)
  starting transfers between devices  12.1 us (23%)
  Pallas kernels  10.7 us (21%)
  waiting for transfers between devices  2.87 us (6%)
    all_to_all x3, blocking collectives, exchange(): return lax.all_to_all(blocks, 'sp', 0, 0, axis_index_groups=[order])  25.8 us
    all_to_all x1, starting transfers between devices, exchange(): return lax.all_to_all(blocks, 'sp', 0, 0, axis_index_groups=[order])  8.32 us
    ppermute x6, starting transfers between devices, over_groups(): lax.ppermute(share, 'tp', [(i, (i ^ m) % count) for i in range(count)])  3.78 us
    pallas_call x1, Pallas kernels, source_side(): pl.pallas_call(functools.partial(streaming_source_kernel, layer), in_spec...  3.45 us
    ppermute x6, waiting for transfers between devices, over_groups(): lax.ppermute(share, 'tp', [(i, (i ^ m) % count) for i in range(count)])  2.87 us
    pallas_call x1, Pallas kernels, first_queries(): pl.pallas_call(functools.partial(first_kernel, layer), in_specs=[IN_PLACE...  2.51 us
    pallas_call x1, Pallas kernels, source_side(): pl.pallas_call(functools.partial(source_kernel, layer), grid=(1,), in_spe...  1.47 us
    pallas_call x2, Pallas kernels, attend(): pl.pallas_call(functools.partial(attend_kernel, layer), grid=(1,), in_spe...  1.05 us
  transfers between devices with their start and end apart: 7, of which 4 were waited for; matrix products, arithmetic and copies ran while one was open for 0% of the time, Pallas kernels for 10%

profile of v5, /device:TPU:0, one launch (start us, length us, event | category | flops | bytes accessed | tf_op | source)
XLA Modules:
  0.0 51.7 jit_solution(17168783037003540937)
XLA Ops:
  0.0 2.5 %first_queries.1 = bf16[8,8,512]{2,1,0:T(8,128)(2,1)} custom-call(bf16[7,2048]{1,0:T(8,128)(2,1)} %hidden.3, f32[2,2048]{1,0:T(2,128)} %gain.7, bf16[2,2048,512]{2,1,0:T(8,128)(2,1)} %w_query.3), custom_call_target="tpu_custom_call" | custom-call | flops 16777216 | bytes 2097152 | tf_op jit(solution)/shard_map/first_queries/pallas_call | solution.py:195
  2.5 8.3 %all-to-all-start = ((bf16[8,8,512]{2,1,0:T(8,128)(2,1)}), bf16[8,8,512]{2,1,0:T(8,128)(2,1)S(1)}, u32[]{:S(2)}, u32[]{:S(2)}) async-start(bf16[8,8,512]{2,1,0:T(8,128)(2,1)} %first_queries.1), calls=%async_computation | async-start | bytes 131072 | tf_op jit(solution)/shard_map/all_to_all | solution.py:329
  10.8 3.5 %source_side.2 = (bf16[256,512]{1,0:T(8,128)(2,1)S(1)}, bf16[256,512]{1,0:T(8,128)(2,1)S(1)}) custom-call(bf16[256,2048]{1,0:T(8,128)(2,1)} %source.2, f32[2,2048]{1,0:T(2,128)} %gain.6, bf16[2,2048,512]{2,1,0:T(8,128)(2,1)} %w_key.3, bf16[2,2048,512]{2,1,0:T(8,128)(2,1)} %w_value.3), custom_call_target="tpu_custom_call" | custom-call | flops 1073741824 | bytes 4194304 | tf_op jit(solution)/shard_map/source_side/pallas_call | solution.py:97
  14.3 0.0 all-to-all-done.queries
  14.3 0.0 copy-start.3
  14.3 0.0 copy-start.1
  14.4 0.0 copy-start.4
  14.4 0.5 %attend.2 = bf16[8,8,640]{2,1,0:T(8,128)(2,1)S(1)} custom-call(bf16[8,8,512]{2,1,0:T(8,128)(2,1)S(1)} %all-to-all-done.queries, bf16[256,512]{1,0:T(8,128)(2,1)S(1)} %get-tuple-element.19.keys, bf16[256,512]{1,0:T(8,128)(2,1)S(1)} %get-tuple-element.20.values, f32[2,2]{1,0:T(2,128)S(1)} %copy-done.8), custom_call_target="tpu_custom_call" | custom-call | flops 3355443200 | bytes 524288 | tf_op jit(solution)/shard_map/attend/pallas_call | solution.py:274
  14.9 0.0 copy-start
  14.9 0.0 copy-start.6
  14.9 8.8 %all_to_all.20.packed = bf16[8,8,640]{2,1,0:T(8,128)(2,1)S(1)} all-to-all(bf16[8,8,640]{2,1,0:T(8,128)(2,1)S(1)} %attend.2), channel_id=1, replica_groups={{20,28,16,12,24,8,4,0},{21,29,17,13,25,9,5,1},{22,30,18,14,26,10,6,2},{..., dimensions={0} | all-to-all | bytes 163840 | tf_op jit(solution)/shard_map/all_to_all | solution.py:329
  23.8 0.5 share.2.rest_0_
  24.3 0.1 collective-permute-start.2
  24.3 1.6 %collective-permute-start.1 = (bf16[8,2048]{1,0:T(8,128)(2,1)S(1)}, bf16[8,2048]{1,0:T(8,128)(2,1)S(1)}, u32[]{:S(2)}, u32[]{:S(2)}) collective-permute-start(bf16[8,2048]{1,0:T(8,128)(2,1)S(1)} %share.2.rest_0_), channel_id=1, source_target_pairs={{0,2},{1,3},{2,0},{3,1},{4,6},{5,7},{6,4},{7,5},{8,10},{9,11},{10,... | collective-permute-start | bytes 98312 | tf_op jit(solution)/shard_map/ppermute | solution.py:335
  25.9 0.3 collective-permute-start
  26.2 0.0 copy-done.6
  26.2 1.5 %source_side.3 = (bf16[256,512]{1,0:T(8,128)(2,1)S(1)}, bf16[256,512]{1,0:T(8,128)(2,1)S(1)}) custom-call(bf16[256,2048]{1,0:T(8,128)(2,1)S(1)} %copy-done.4, f32[2,2048]{1,0:T(2,128)S(1)} %copy-done.6, bf16[2,2048,512]{2,1,0:T(8,128)(2,1)S(1)} %copy-done, bf16[2,2048,512]{2,1,0:T(8,128)(2,1)S(1)} %copy-done.1), custom_call_target="tpu_custom_call" | custom-call | flops 1073741824 | bytes 4194304 | tf_op jit(solution)/shard_map/source_side/pallas_call | solution.py:112
  27.7 0.3 collective-permute-done.2.rest_3_
  28.0 0.4 collective-permute-done.1.rest_2_
  28.4 0.0 collective-permute-done.rest_1_
  28.4 0.6 %next_queries.1 = (bf16[8,8,512]{2,1,0:T(8,128)(2,1)S(1)}, bf16[7,2048]{1,0:T(8,128)(2,1)S(1)}) custom-call(bf16[7,2048]{1,0:T(8,128)(2,1)S(1)} %copy-done.5, f32[2,2048]{1,0:T(2,128)S(1)} %copy-done.7, bf16[2,2048,512]{2,1,0:T(8,128)(2,1)S(1)} %copy-done.2, bf16[8,2048]{1,0:T(8,128)(2,1)S(1)} %share.2.rest_0_, ...), custom_call_target="tpu_custom_call" | custom-call | flops 16777216 | bytes 2097152 | tf_op jit(solution)/shard_map/next_queries/pallas_call | solution.py:214
  29.0 8.5 %all_to_all.21.queries = bf16[8,8,512]{2,1,0:T(8,128)(2,1)S(1)} all-to-all(bf16[8,8,512]{2,1,0:T(8,128)(2,1)S(1)} %get-tuple-element.30), channel_id=1, replica_groups={{20,28,16,12,24,8,4,0},{21,29,17,13,25,9,5,1},{22,30,18,14,26,10,6,2},{..., dimensions={0} | all-to-all | bytes 131072 | tf_op jit(solution)/shard_map/all_to_all | solution.py:329
  37.5 0.5 %attend.3 = bf16[8,8,640]{2,1,0:T(8,128)(2,1)S(1)} custom-call(bf16[8,8,512]{2,1,0:T(8,128)(2,1)S(1)} %all_to_all.21.queries, bf16[256,512]{1,0:T(8,128)(2,1)S(1)} %get-tuple-element.31.keys, bf16[256,512]{1,0:T(8,128)(2,1)S(1)} %get-tuple-element.32.values, f32[2,2]{1,0:T(2,128)S(1)} %copy-done.8), custom_call_target="tpu_custom_call" | custom-call | flops 3355443200 | bytes 524288 | tf_op jit(solution)/shard_map/attend/pallas_call | solution.py:274
  38.0 8.5 %all_to_all.22.packed = bf16[8,8,640]{2,1,0:T(8,128)(2,1)S(1)} all-to-all(bf16[8,8,640]{2,1,0:T(8,128)(2,1)S(1)} %attend.3), channel_id=1, replica_groups={{20,28,16,12,24,8,4,0},{21,29,17,13,25,9,5,1},{22,30,18,14,26,10,6,2},{..., dimensions={0} | all-to-all | bytes 163840 | tf_op jit(solution)/shard_map/all_to_all | solution.py:329
  46.5 0.5 share.3.rest_0_
  47.0 0.0 collective-permute-start.5
  47.0 1.6 %collective-permute-start.4 = (bf16[8,2048]{1,0:T(8,128)(2,1)S(1)}, bf16[8,2048]{1,0:T(8,128)(2,1)S(1)}, u32[]{:S(2)}, u32[]{:S(2)}) collective-permute-start(bf16[8,2048]{1,0:T(8,128)(2,1)S(1)} %share.3.rest_0_), channel_id=1, source_target_pairs={{0,2},{1,3},{2,0},{3,1},{4,6},{5,7},{6,4},{7,5},{8,10},{9,11},{10,... | collective-permute-start | bytes 98312 | tf_op jit(solution)/shard_map/ppermute | solution.py:335
  48.6 0.3 collective-permute-start.3
  48.9 1.8 %collective-permute-done.5.rest_3_ = bf16[8,2048]{1,0:T(8,128)(2,1)S(1)} collective-permute-done((bf16[8,2048]{1,0:T(8,128)(2,1)S(1)}, bf16[8,2048]{1,0:T(8,128)(2,1)S(1)}, u32[]{:S(2)}, u32[]{:S(2)}) %collective-permute-start.5) | collective-permute-done | bytes 32800 | tf_op jit(solution)/shard_map/ppermute | solution.py:335
  50.7 0.4 collective-permute-done.4.rest_2_
  51.1 0.0 collective-permute-done.3.rest_1_
  51.1 0.6 %last_rows.1 = bf16[7,2048]{1,0:T(8,128)(2,1)} custom-call(bf16[7,2048]{1,0:T(8,128)(2,1)S(1)} %get-tuple-element.29.hidden, bf16[8,2048]{1,0:T(8,128)(2,1)S(1)} %share.3.rest_0_, bf16[8,2048]{1,0:T(8,128)(2,1)S(1)} %collective-permute-done.3.rest_1_, bf16[8,2048]{1,0:T(8,128)(2,1)S(1)} %collective-permute-done.4.rest_2_, ...), custom_call_target="tpu_custom_call" | custom-call | tf_op jit(solution)/shard_map/last_rows/pallas_call | solution.py:235
  (12 shorter events, 0.0 us)
Async XLA Ops:
  2.5 11.8 %all-to-all-start = ((bf16[8,8,512]{2,1,0:T(8,128)(2,1)}), bf16[8,8,512]{2,1,0:T(8,128)(2,1)S(1)}, u32[]{:S(2)}, u32[]{:S(2)}) async-start(bf16[8,8,512]{2,1,0:T(8,128)(2,1)} %first_queries.1), calls=%async_computation | async-start | bytes 131072 | tf_op jit(solution)/shard_map/all_to_all | solution.py:329
  10.8 3.5 %copy-start.8 = (f32[2,2]{1,0:T(2,128)S(1)}, f32[2,2]{1,0:T(2,128)}, u32[]{:S(2)}) copy-start(f32[2,2]{1,0:T(2,128)} %scales.3) | copy-start | bytes 52
  14.3 9.4 %copy-start.3 = (bf16[2,512,2048]{2,1,0:T(8,128)(2,1)S(1)}, bf16[2,512,2048]{2,1,0:T(8,128)(2,1)}, u32[]{:S(2)}) copy-start(bf16[2,512,2048]{2,1,0:T(8,128)(2,1)} %w_out.3) | copy-start | bytes 12582916
  14.3 11.8 %copy-start.1 = (bf16[2,2048,512]{2,1,0:T(8,128)(2,1)S(1)}, bf16[2,2048,512]{2,1,0:T(8,128)(2,1)}, u32[]{:S(2)}) copy-start(bf16[2,2048,512]{2,1,0:T(8,128)(2,1)} %w_value.3) | copy-start | bytes 12582916
  14.4 11.8 %copy-start.4 = (bf16[256,2048]{1,0:T(8,128)(2,1)S(1)}, bf16[256,2048]{1,0:T(8,128)(2,1)}, u32[]{:S(2)}) copy-start(bf16[256,2048]{1,0:T(8,128)(2,1)} %source.2) | copy-start | bytes 3145732
  14.9 11.3 %copy-start = (bf16[2,2048,512]{2,1,0:T(8,128)(2,1)S(1)}, bf16[2,2048,512]{2,1,0:T(8,128)(2,1)}, u32[]{:S(2)}) copy-start(bf16[2,2048,512]{2,1,0:T(8,128)(2,1)} %w_key.3) | copy-start | bytes 12582916
  14.9 11.3 %copy-start.6 = (f32[2,2048]{1,0:T(2,128)S(1)}, f32[2,2048]{1,0:T(2,128)}, u32[]{:S(2)}) copy-start(f32[2,2048]{1,0:T(2,128)} %gain.6) | copy-start | bytes 49156
  24.2 4.1 %copy-start.2 = (bf16[2,2048,512]{2,1,0:T(8,128)(2,1)S(1)}, bf16[2,2048,512]{2,1,0:T(8,128)(2,1)}, u32[]{:S(2)}) copy-start(bf16[2,2048,512]{2,1,0:T(8,128)(2,1)} %w_query.3) | copy-start | bytes 12582916
  24.3 4.1 %copy-start.5 = (bf16[7,2048]{1,0:T(8,128)(2,1)S(1)}, bf16[7,2048]{1,0:T(8,128)(2,1)}, u32[]{:S(2)}) copy-start(bf16[7,2048]{1,0:T(8,128)(2,1)} %hidden.3) | copy-start | bytes 86020
  24.3 4.1 %copy-start.7 = (f32[2,2048]{1,0:T(2,128)S(1)}, f32[2,2048]{1,0:T(2,128)}, u32[]{:S(2)}) copy-start(f32[2,2048]{1,0:T(2,128)} %gain.7) | copy-start | bytes 49156
  24.3 3.7 %collective-permute-start.2 = (bf16[8,2048]{1,0:T(8,128)(2,1)S(1)}, bf16[8,2048]{1,0:T(8,128)(2,1)S(1)}, u32[]{:S(2)}, u32[]{:S(2)}) collective-permute-start(bf16[8,2048]{1,0:T(8,128)(2,1)S(1)} %share.2.rest_0_), channel_id=1, source_target_pairs={{0,3},{1,2},{2,1},{3,0},{4,7},{5,6},{6,5},{7,4},{8,11},{9,10},{10,... | collective-permute-start | bytes 98312 | tf_op jit(solution)/shard_map/ppermute | solution.py:335
  24.3 4.0 %collective-permute-start.1 = (bf16[8,2048]{1,0:T(8,128)(2,1)S(1)}, bf16[8,2048]{1,0:T(8,128)(2,1)S(1)}, u32[]{:S(2)}, u32[]{:S(2)}) collective-permute-start(bf16[8,2048]{1,0:T(8,128)(2,1)S(1)} %share.2.rest_0_), channel_id=1, source_target_pairs={{0,2},{1,3},{2,0},{3,1},{4,6},{5,7},{6,4},{7,5},{8,10},{9,11},{10,... | collective-permute-start | bytes 98312 | tf_op jit(solution)/shard_map/ppermute | solution.py:335
  25.9 2.5 %collective-permute-start = (bf16[8,2048]{1,0:T(8,128)(2,1)S(1)}, bf16[8,2048]{1,0:T(8,128)(2,1)S(1)}, u32[]{:S(2)}, u32[]{:S(2)}) collective-permute-start(bf16[8,2048]{1,0:T(8,128)(2,1)S(1)} %share.2.rest_0_), channel_id=1, source_target_pairs={{0,1},{1,0},{2,3},{3,2},{4,5},{5,4},{6,7},{7,6},{8,9},{9,8},{10,11... | collective-permute-start | bytes 98312 | tf_op jit(solution)/shard_map/ppermute | solution.py:335
  47.0 3.7 %collective-permute-start.5 = (bf16[8,2048]{1,0:T(8,128)(2,1)S(1)}, bf16[8,2048]{1,0:T(8,128)(2,1)S(1)}, u32[]{:S(2)}, u32[]{:S(2)}) collective-permute-start(bf16[8,2048]{1,0:T(8,128)(2,1)S(1)} %share.3.rest_0_), channel_id=1, source_target_pairs={{0,3},{1,2},{2,1},{3,0},{4,7},{5,6},{6,5},{7,4},{8,11},{9,10},{10,... | collective-permute-start | bytes 98312 | tf_op jit(solution)/shard_map/ppermute | solution.py:335
  47.0 4.0 %collective-permute-start.4 = (bf16[8,2048]{1,0:T(8,128)(2,1)S(1)}, bf16[8,2048]{1,0:T(8,128)(2,1)S(1)}, u32[]{:S(2)}, u32[]{:S(2)}) collective-permute-start(bf16[8,2048]{1,0:T(8,128)(2,1)S(1)} %share.3.rest_0_), channel_id=1, source_target_pairs={{0,2},{1,3},{2,0},{3,1},{4,6},{5,7},{6,4},{7,5},{8,10},{9,11},{10,... | collective-permute-start | bytes 98312 | tf_op jit(solution)/shard_map/ppermute | solution.py:335
  48.6 2.5 %collective-permute-start.3 = (bf16[8,2048]{1,0:T(8,128)(2,1)S(1)}, bf16[8,2048]{1,0:T(8,128)(2,1)S(1)}, u32[]{:S(2)}, u32[]{:S(2)}) collective-permute-start(bf16[8,2048]{1,0:T(8,128)(2,1)S(1)} %share.3.rest_0_), channel_id=1, source_target_pairs={{0,1},{1,0},{2,3},{3,2},{4,5},{5,4},{6,7},{7,6},{8,9},{9,8},{10,11... | collective-permute-start | bytes 98312 | tf_op jit(solution)/shard_map/ppermute | solution.py:335

commit v6 on v5

--- a/solution.py
+++ b/solution.py
@@ -119,11 +119,6 @@
     )(source, gain, w_key, w_value)
 
 
-def project(normed, weight, queries):
-    raw = jnp.dot(normed, weight, preferred_element_type=jnp.float32)
-    spread(raw, queries)
-
-
 def spread(raw, queries):
     rows, columns = raw.shape
     for start in range(0, columns, HEAD_DIM):
@@ -181,7 +176,10 @@
     branch = branch_of(shares, hidden.shape[0])
     after = (hidden[...].astype(jnp.float32) + branch).astype(jnp.bfloat16)
     result[...] = after
-    project(normed_rows(after.astype(jnp.float32), gain[layer : layer + 1, :]), w_query[0], queries)
+    rows = after.astype(jnp.float32)
+    gained = (rows * gain[layer : layer + 1, :]).astype(jnp.bfloat16)
+    raw = jnp.dot(gained, w_query[0], preferred_element_type=jnp.float32)
+    spread(raw * row_scale(rows), queries)
 
 
 def last_kernel(hidden, *rest):
@@ -247,23 +245,35 @@
     blocks, padded, columns = queries.shape
     rows = blocks * padded
     root = math.sqrt(HEAD_DIM)
+    heads = range(columns // HEAD_DIM)
+    cuts = [slice(head * HEAD_DIM, (head + 1) * HEAD_DIM) for head in heads]
+    scores = [
+        lax.dot_general(
+            queries[:, :, cut].reshape(rows, HEAD_DIM),
+            keys[:, cut],
+            (((1,), (1,)), ((), ())),
+            preferred_element_type=jnp.float32,
+        )
+        for cut in cuts
+    ]
+    weights = [
+        jnp.exp(scales[layer : layer + 1, head : head + 1] * (scores[head] / root - root))
+        for head in heads
+    ]
+    parts = [
+        jnp.dot(
+            weights[head].astype(jnp.bfloat16), values[:, cut], preferred_element_type=jnp.float32
+        )
+        for head, cut in zip(heads, cuts)
+    ]
     lane = lax.broadcasted_iota(jnp.int32, (rows, LANES), 1)
     sums = jnp.zeros((rows, LANES), jnp.float32)
-    for head in range(columns // HEAD_DIM):
-        cut = slice(head * HEAD_DIM, (head + 1) * HEAD_DIM)
-        query = queries[:, :, cut].reshape(rows, HEAD_DIM)
-        scores = lax.dot_general(
-            query, keys[:, cut], (((1,), (1,)), ((), ())), preferred_element_type=jnp.float32
-        )
-        scale = scales[layer : layer + 1, head : head + 1]
-        weights = jnp.exp(scale * (scores / root - root))
-        total = jnp.sum(weights, axis=1, keepdims=True)
+    for head in heads:
+        total = jnp.sum(weights[head], axis=1, keepdims=True)
         high = total.astype(jnp.bfloat16).astype(jnp.float32)
         sums = jnp.where(lane == 2 * head, high, sums)
         sums = jnp.where(lane == 2 * head + 1, total - high, sums)
-        part = jnp.dot(
-            weights.astype(jnp.bfloat16), values[:, cut], preferred_element_type=jnp.float32
-        )
+    for part, cut in zip(parts, cuts):
         packed[:, :, cut] = part.astype(jnp.bfloat16).reshape(blocks, padded, HEAD_DIM)
     packed[:, :, columns:] = sums.astype(jnp.bfloat16).reshape(blocks, padded, LANES)
 

time: 52.1 us -> 51.6 us (level)
  no operation moved by 1% of the time
where the time goes in v6:
time: 51.6 us; the launch traced here: 51.3 us
  blocking collectives  25.8 us (50%)
  starting transfers between devices  12.1 us (23%)
  Pallas kernels  10.3 us (20%)
  waiting for transfers between devices  2.88 us (6%)
    all_to_all x3, blocking collectives, exchange(): return lax.all_to_all(blocks, 'sp', 0, 0, axis_index_groups=[order])  25.8 us
    all_to_all x1, starting transfers between devices, exchange(): return lax.all_to_all(blocks, 'sp', 0, 0, axis_index_groups=[order])  8.32 us
    ppermute x6, starting transfers between devices, over_groups(): lax.ppermute(share, 'tp', [(i, (i ^ m) % count) for i in range(count)])  3.78 us
    pallas_call x1, Pallas kernels, source_side(): pl.pallas_call(functools.partial(streaming_source_kernel, layer), in_spec...  3.45 us
    ppermute x6, waiting for transfers between devices, over_groups(): lax.ppermute(share, 'tp', [(i, (i ^ m) % count) for i in range(count)])  2.88 us
    pallas_call x1, Pallas kernels, first_queries(): pl.pallas_call(functools.partial(first_kernel, layer), in_specs=[IN_PLACE...  2.51 us
    pallas_call x1, Pallas kernels, source_side(): pl.pallas_call(functools.partial(source_kernel, layer), grid=(1,), in_spe...  1.46 us
  transfers between devices with their start and end apart: 7, of which 4 were waited for; matrix products, arithmetic and copies ran while one was open for 0% of the time, Pallas kernels for 10%

profile of v6, /device:TPU:0, one launch (start us, length us, event | category | flops | bytes accessed | tf_op | source)
XLA Modules:
  0.0 51.3 jit_solution(12505387019350679590)
XLA Ops:
  0.0 2.5 %first_queries.1 = bf16[8,8,512]{2,1,0:T(8,128)(2,1)} custom-call(bf16[7,2048]{1,0:T(8,128)(2,1)} %hidden.3, f32[2,2048]{1,0:T(2,128)} %gain.7, bf16[2,2048,512]{2,1,0:T(8,128)(2,1)} %w_query.3), custom_call_target="tpu_custom_call" | custom-call | flops 16777216 | bytes 2097152 | tf_op jit(solution)/shard_map/first_queries/pallas_call | solution.py:193
  2.5 8.3 %all-to-all-start = ((bf16[8,8,512]{2,1,0:T(8,128)(2,1)}), bf16[8,8,512]{2,1,0:T(8,128)(2,1)S(1)}, u32[]{:S(2)}, u32[]{:S(2)}) async-start(bf16[8,8,512]{2,1,0:T(8,128)(2,1)} %first_queries.1), calls=%async_computation | async-start | bytes 131072 | tf_op jit(solution)/shard_map/all_to_all | solution.py:339
  10.8 3.5 %source_side.2 = (bf16[256,512]{1,0:T(8,128)(2,1)S(1)}, bf16[256,512]{1,0:T(8,128)(2,1)S(1)}) custom-call(bf16[256,2048]{1,0:T(8,128)(2,1)} %source.2, f32[2,2048]{1,0:T(2,128)} %gain.6, bf16[2,2048,512]{2,1,0:T(8,128)(2,1)} %w_key.3, bf16[2,2048,512]{2,1,0:T(8,128)(2,1)} %w_value.3), custom_call_target="tpu_custom_call" | custom-call | flops 1073741824 | bytes 4194304 | tf_op jit(solution)/shard_map/source_side/pallas_call | solution.py:97
  14.3 0.0 all-to-all-done.queries
  14.3 0.0 copy-start.3
  14.3 0.0 copy-start.1
  14.4 0.0 copy-start.4
  14.4 0.4 attend.2
  14.7 0.0 copy-start
  14.7 0.0 copy-start.6
  14.8 8.8 %all_to_all.20.packed = bf16[8,8,640]{2,1,0:T(8,128)(2,1)S(1)} all-to-all(bf16[8,8,640]{2,1,0:T(8,128)(2,1)S(1)} %attend.2), channel_id=1, replica_groups={{20,28,16,12,24,8,4,0},{21,29,17,13,25,9,5,1},{22,30,18,14,26,10,6,2},{..., dimensions={0} | all-to-all | bytes 163840 | tf_op jit(solution)/shard_map/all_to_all | solution.py:339
  23.6 0.5 share.2.rest_0_
  24.1 0.1 collective-permute-start.2
  24.2 1.6 %collective-permute-start.1 = (bf16[8,2048]{1,0:T(8,128)(2,1)S(1)}, bf16[8,2048]{1,0:T(8,128)(2,1)S(1)}, u32[]{:S(2)}, u32[]{:S(2)}) collective-permute-start(bf16[8,2048]{1,0:T(8,128)(2,1)S(1)} %share.2.rest_0_), channel_id=1, source_target_pairs={{0,2},{1,3},{2,0},{3,1},{4,6},{5,7},{6,4},{7,5},{8,10},{9,11},{10,... | collective-permute-start | bytes 98312 | tf_op jit(solution)/shard_map/ppermute | solution.py:345
  25.7 0.3 collective-permute-start
  26.0 0.0 copy-done.4
  26.0 1.5 %source_side.3 = (bf16[256,512]{1,0:T(8,128)(2,1)S(1)}, bf16[256,512]{1,0:T(8,128)(2,1)S(1)}) custom-call(bf16[256,2048]{1,0:T(8,128)(2,1)S(1)} %copy-done.4, f32[2,2048]{1,0:T(2,128)S(1)} %copy-done.6, bf16[2,2048,512]{2,1,0:T(8,128)(2,1)S(1)} %copy-done, bf16[2,2048,512]{2,1,0:T(8,128)(2,1)S(1)} %copy-done.1), custom_call_target="tpu_custom_call" | custom-call | flops 1073741824 | bytes 4194304 | tf_op jit(solution)/shard_map/source_side/pallas_call | solution.py:112
  27.5 0.3 collective-permute-done.2.rest_3_
  27.8 0.4 collective-permute-done.1.rest_2_
  28.2 0.0 collective-permute-done.rest_1_
  28.2 0.5 next_queries.1
  28.7 8.5 %all_to_all.21.queries = bf16[8,8,512]{2,1,0:T(8,128)(2,1)S(1)} all-to-all(bf16[8,8,512]{2,1,0:T(8,128)(2,1)S(1)} %get-tuple-element.30), channel_id=1, replica_groups={{20,28,16,12,24,8,4,0},{21,29,17,13,25,9,5,1},{22,30,18,14,26,10,6,2},{..., dimensions={0} | all-to-all | bytes 131072 | tf_op jit(solution)/shard_map/all_to_all | solution.py:339
  37.2 0.4 attend.3
  37.6 8.5 %all_to_all.22.packed = bf16[8,8,640]{2,1,0:T(8,128)(2,1)S(1)} all-to-all(bf16[8,8,640]{2,1,0:T(8,128)(2,1)S(1)} %attend.3), channel_id=1, replica_groups={{20,28,16,12,24,8,4,0},{21,29,17,13,25,9,5,1},{22,30,18,14,26,10,6,2},{..., dimensions={0} | all-to-all | bytes 163840 | tf_op jit(solution)/shard_map/all_to_all | solution.py:339
  46.1 0.5 share.3.rest_0_
  46.6 0.0 collective-permute-start.5
  46.6 1.6 %collective-permute-start.4 = (bf16[8,2048]{1,0:T(8,128)(2,1)S(1)}, bf16[8,2048]{1,0:T(8,128)(2,1)S(1)}, u32[]{:S(2)}, u32[]{:S(2)}) collective-permute-start(bf16[8,2048]{1,0:T(8,128)(2,1)S(1)} %share.3.rest_0_), channel_id=1, source_target_pairs={{0,2},{1,3},{2,0},{3,1},{4,6},{5,7},{6,4},{7,5},{8,10},{9,11},{10,... | collective-permute-start | bytes 98312 | tf_op jit(solution)/shard_map/ppermute | solution.py:345
  48.1 0.3 collective-permute-start.3
  48.4 1.8 %collective-permute-done.5.rest_3_ = bf16[8,2048]{1,0:T(8,128)(2,1)S(1)} collective-permute-done((bf16[8,2048]{1,0:T(8,128)(2,1)S(1)}, bf16[8,2048]{1,0:T(8,128)(2,1)S(1)}, u32[]{:S(2)}, u32[]{:S(2)}) %collective-permute-start.5) | collective-permute-done | bytes 32800 | tf_op jit(solution)/shard_map/ppermute | solution.py:345
  50.2 0.4 collective-permute-done.4.rest_2_
  50.6 0.0 collective-permute-done.3.rest_1_
  50.6 0.6 %last_rows.1 = bf16[7,2048]{1,0:T(8,128)(2,1)} custom-call(bf16[7,2048]{1,0:T(8,128)(2,1)S(1)} %get-tuple-element.29.hidden, bf16[8,2048]{1,0:T(8,128)(2,1)S(1)} %share.3.rest_0_, bf16[8,2048]{1,0:T(8,128)(2,1)S(1)} %collective-permute-done.3.rest_1_, bf16[8,2048]{1,0:T(8,128)(2,1)S(1)} %collective-permute-done.4.rest_2_, ...), custom_call_target="tpu_custom_call" | custom-call | tf_op jit(solution)/shard_map/last_rows/pallas_call | solution.py:233
  (12 shorter events, 0.0 us)
Async XLA Ops:
  2.5 11.8 %all-to-all-start = ((bf16[8,8,512]{2,1,0:T(8,128)(2,1)}), bf16[8,8,512]{2,1,0:T(8,128)(2,1)S(1)}, u32[]{:S(2)}, u32[]{:S(2)}) async-start(bf16[8,8,512]{2,1,0:T(8,128)(2,1)} %first_queries.1), calls=%async_computation | async-start | bytes 131072 | tf_op jit(solution)/shard_map/all_to_all | solution.py:339
  10.8 3.5 %copy-start.8 = (f32[2,2]{1,0:T(2,128)S(1)}, f32[2,2]{1,0:T(2,128)}, u32[]{:S(2)}) copy-start(f32[2,2]{1,0:T(2,128)} %scales.3) | copy-start | bytes 52
  14.3 9.2 %copy-start.3 = (bf16[2,512,2048]{2,1,0:T(8,128)(2,1)S(1)}, bf16[2,512,2048]{2,1,0:T(8,128)(2,1)}, u32[]{:S(2)}) copy-start(bf16[2,512,2048]{2,1,0:T(8,128)(2,1)} %w_out.3) | copy-start | bytes 12582916
  14.3 11.7 %copy-start.1 = (bf16[2,2048,512]{2,1,0:T(8,128)(2,1)S(1)}, bf16[2,2048,512]{2,1,0:T(8,128)(2,1)}, u32[]{:S(2)}) copy-start(bf16[2,2048,512]{2,1,0:T(8,128)(2,1)} %w_value.3) | copy-start | bytes 12582916
  14.4 11.7 %copy-start.4 = (bf16[256,2048]{1,0:T(8,128)(2,1)S(1)}, bf16[256,2048]{1,0:T(8,128)(2,1)}, u32[]{:S(2)}) copy-start(bf16[256,2048]{1,0:T(8,128)(2,1)} %source.2) | copy-start | bytes 3145732
  14.7 11.3 %copy-start = (bf16[2,2048,512]{2,1,0:T(8,128)(2,1)S(1)}, bf16[2,2048,512]{2,1,0:T(8,128)(2,1)}, u32[]{:S(2)}) copy-start(bf16[2,2048,512]{2,1,0:T(8,128)(2,1)} %w_key.3) | copy-start | bytes 12582916
  14.7 11.3 %copy-start.6 = (f32[2,2048]{1,0:T(2,128)S(1)}, f32[2,2048]{1,0:T(2,128)}, u32[]{:S(2)}) copy-start(f32[2,2048]{1,0:T(2,128)} %gain.6) | copy-start | bytes 49156
  24.1 4.1 %copy-start.2 = (bf16[2,2048,512]{2,1,0:T(8,128)(2,1)S(1)}, bf16[2,2048,512]{2,1,0:T(8,128)(2,1)}, u32[]{:S(2)}) copy-start(bf16[2,2048,512]{2,1,0:T(8,128)(2,1)} %w_query.3) | copy-start | bytes 12582916
  24.1 4.1 %copy-start.5 = (bf16[7,2048]{1,0:T(8,128)(2,1)S(1)}, bf16[7,2048]{1,0:T(8,128)(2,1)}, u32[]{:S(2)}) copy-start(bf16[7,2048]{1,0:T(8,128)(2,1)} %hidden.3) | copy-start | bytes 86020
  24.1 4.1 %copy-start.7 = (f32[2,2048]{1,0:T(2,128)S(1)}, f32[2,2048]{1,0:T(2,128)}, u32[]{:S(2)}) copy-start(f32[2,2048]{1,0:T(2,128)} %gain.7) | copy-start | bytes 49156
  24.1 3.7 %collective-permute-start.2 = (bf16[8,2048]{1,0:T(8,128)(2,1)S(1)}, bf16[8,2048]{1,0:T(8,128)(2,1)S(1)}, u32[]{:S(2)}, u32[]{:S(2)}) collective-permute-start(bf16[8,2048]{1,0:T(8,128)(2,1)S(1)} %share.2.rest_0_), channel_id=1, source_target_pairs={{0,3},{1,2},{2,1},{3,0},{4,7},{5,6},{6,5},{7,4},{8,11},{9,10},{10,... | collective-permute-start | bytes 98312 | tf_op jit(solution)/shard_map/ppermute | solution.py:345
  24.2 4.0 %collective-permute-start.1 = (bf16[8,2048]{1,0:T(8,128)(2,1)S(1)}, bf16[8,2048]{1,0:T(8,128)(2,1)S(1)}, u32[]{:S(2)}, u32[]{:S(2)}) collective-permute-start(bf16[8,2048]{1,0:T(8,128)(2,1)S(1)} %share.2.rest_0_), channel_id=1, source_target_pairs={{0,2},{1,3},{2,0},{3,1},{4,6},{5,7},{6,4},{7,5},{8,10},{9,11},{10,... | collective-permute-start | bytes 98312 | tf_op jit(solution)/shard_map/ppermute | solution.py:345
  25.7 2.5 %collective-permute-start = (bf16[8,2048]{1,0:T(8,128)(2,1)S(1)}, bf16[8,2048]{1,0:T(8,128)(2,1)S(1)}, u32[]{:S(2)}, u32[]{:S(2)}) collective-permute-start(bf16[8,2048]{1,0:T(8,128)(2,1)S(1)} %share.2.rest_0_), channel_id=1, source_target_pairs={{0,1},{1,0},{2,3},{3,2},{4,5},{5,4},{6,7},{7,6},{8,9},{9,8},{10,11... | collective-permute-start | bytes 98312 | tf_op jit(solution)/shard_map/ppermute | solution.py:345
  46.6 3.7 %collective-permute-start.5 = (bf16[8,2048]{1,0:T(8,128)(2,1)S(1)}, bf16[8,2048]{1,0:T(8,128)(2,1)S(1)}, u32[]{:S(2)}, u32[]{:S(2)}) collective-permute-start(bf16[8,2048]{1,0:T(8,128)(2,1)S(1)} %share.3.rest_0_), channel_id=1, source_target_pairs={{0,3},{1,2},{2,1},{3,0},{4,7},{5,6},{6,5},{7,4},{8,11},{9,10},{10,... | collective-permute-start | bytes 98312 | tf_op jit(solution)/shard_map/ppermute | solution.py:345
  46.6 4.0 %collective-permute-start.4 = (bf16[8,2048]{1,0:T(8,128)(2,1)S(1)}, bf16[8,2048]{1,0:T(8,128)(2,1)S(1)}, u32[]{:S(2)}, u32[]{:S(2)}) collective-permute-start(bf16[8,2048]{1,0:T(8,128)(2,1)S(1)} %share.3.rest_0_), channel_id=1, source_target_pairs={{0,2},{1,3},{2,0},{3,1},{4,6},{5,7},{6,4},{7,5},{8,10},{9,11},{10,... | collective-permute-start | bytes 98312 | tf_op jit(solution)/shard_map/ppermute | solution.py:345
  48.1 2.5 %collective-permute-start.3 = (bf16[8,2048]{1,0:T(8,128)(2,1)S(1)}, bf16[8,2048]{1,0:T(8,128)(2,1)S(1)}, u32[]{:S(2)}, u32[]{:S(2)}) collective-permute-start(bf16[8,2048]{1,0:T(8,128)(2,1)S(1)} %share.3.rest_0_), channel_id=1, source_target_pairs={{0,1},{1,0},{2,3},{3,2},{4,5},{5,4},{6,7},{7,6},{8,9},{9,8},{10,11... | collective-permute-start | bytes 98312 | tf_op jit(solution)/shard_map/ppermute | solution.py:345

commit v7 on v6

--- a/solution.py
+++ b/solution.py
@@ -38,16 +38,16 @@
     return pl.CostEstimate(flops=flops, bytes_accessed=moved, transcendentals=0)
 
 
-def keys_of(normed, weight, keys):
-    raw = jnp.dot(normed, weight, preferred_element_type=jnp.float32)
+def keys_of(gained, scale, weight, keys):
+    raw = jnp.dot(gained, weight, preferred_element_type=jnp.float32) * scale
     for start in range(0, keys.shape[1], HEAD_DIM):
         head = raw[:, start : start + HEAD_DIM]
         keys[:, start : start + HEAD_DIM] = (head * row_scale(head)).astype(jnp.bfloat16)
 
 
-def values_of(normed, weight, values):
-    raw = jnp.dot(normed, weight, preferred_element_type=jnp.float32)
-    values[...] = raw.astype(jnp.bfloat16)
+def values_of(gained, scale, weight, values):
+    raw = jnp.dot(gained, weight, preferred_element_type=jnp.float32)
+    values[...] = (raw * scale).astype(jnp.bfloat16)
 
 
 def streaming_source_kernel(layer, source, gain, w_key, w_value, keys, values, *scratch):
@@ -69,19 +69,23 @@
         copy.start()
     copies[0].wait()
     copies[1].wait()
-    normed = normed_rows(rows[...].astype(jnp.float32), gains[layer : layer + 1, :])
+    values_in = rows[...].astype(jnp.float32)
+    gained = (values_in * gains[layer : layer + 1, :]).astype(jnp.bfloat16)
+    scale = row_scale(values_in)
     for copy in copies[2 : 2 + PIECES]:
         copy.wait()
-    keys_of(normed, held_key[...], keys)
+    keys_of(gained, scale, held_key[...], keys)
     for copy in copies[2 + PIECES :]:
         copy.wait()
-    values_of(normed, held_value[...], values)
+    values_of(gained, scale, held_value[...], values)
 
 
 def source_kernel(layer, source, gain, w_key, w_value, keys, values):
-    normed = normed_rows(source[...].astype(jnp.float32), gain[layer : layer + 1, :])
-    keys_of(normed, w_key[0], keys)
-    values_of(normed, w_value[0], values)
+    rows = source[...].astype(jnp.float32)
+    gained = (rows * gain[layer : layer + 1, :]).astype(jnp.bfloat16)
+    scale = row_scale(rows)
+    values_of(gained, scale, w_value[0], values)
+    keys_of(gained, scale, w_key[0], keys)
 
 
 def source_side(layer, source, gain, w_key, w_value, streaming):
@@ -133,10 +137,6 @@
         )
 
 
-def normed_rows(rows, gains):
-    return (rows * row_scale(rows) * gains).astype(jnp.bfloat16)
-
-
 def first_kernel(layer, hidden, gain, w_query, queries, rows, gains, held, arrived):
     depth = held.shape[1]
     copies = [
@@ -155,13 +155,14 @@
         copy.start()
     copies[0].wait()
     copies[1].wait()
-    normed = normed_rows(rows[...].astype(jnp.float32), gains[layer : layer + 1, :])
+    own = rows[...].astype(jnp.float32)
+    gained = (own * gains[layer : layer + 1, :]).astype(jnp.bfloat16)
     raw = jnp.zeros((rows.shape[0], held.shape[2]), jnp.float32)
     for piece in range(PIECES):
         copies[2 + piece].wait()
         cut = slice(piece * depth, (piece + 1) * depth)
-        raw = raw + jnp.dot(normed[:, cut], held[piece], preferred_element_type=jnp.float32)
-    spread(raw, queries)
+        raw = raw + jnp.dot(gained[:, cut], held[piece], preferred_element_type=jnp.float32)
+    spread(raw * row_scale(own), queries)
 
 
 def branch_of(shares, rows):

time: 51.6 us -> 51.6 us (level)
  transfers between devices with their start and end apart: 7 -> 7, of which waited for: 4 -> 4; matrix products, arithmetic and copies ran while one was open for 0% -> 0% of each run, Pallas kernels for 10% -> 9%
where the time goes in v7:
time: 51.6 us; the launch traced here: 51.3 us
  blocking collectives  25.8 us (50%)
  starting transfers between devices  12.1 us (23%)
  Pallas kernels  10.2 us (20%)
  waiting for transfers between devices  2.99 us (6%)
    all_to_all x3, blocking collectives, exchange(): return lax.all_to_all(blocks, 'sp', 0, 0, axis_index_groups=[order])  25.8 us
    all_to_all x1, starting transfers between devices, exchange(): return lax.all_to_all(blocks, 'sp', 0, 0, axis_index_groups=[order])  8.32 us
    ppermute x6, starting transfers between devices, over_groups(): lax.ppermute(share, 'tp', [(i, (i ^ m) % count) for i in range(count)])  3.78 us
    pallas_call x1, Pallas kernels, source_side(): pl.pallas_call(functools.partial(streaming_source_kernel, layer), in_spec...  3.46 us
    ppermute x6, waiting for transfers between devices, over_groups(): lax.ppermute(share, 'tp', [(i, (i ^ m) % count) for i in range(count)])  2.99 us
    pallas_call x1, Pallas kernels, first_queries(): pl.pallas_call(functools.partial(first_kernel, layer), in_specs=[IN_PLACE...  2.51 us
    pallas_call x1, Pallas kernels, source_side(): pl.pallas_call(functools.partial(source_kernel, layer), grid=(1,), in_spe...  1.36 us
  transfers between devices with their start and end apart: 7, of which 4 were waited for; matrix products, arithmetic and copies ran while one was open for 0% of the time, Pallas kernels for 9%

profile of v7, /device:TPU:0, one launch (start us, length us, event | category | flops | bytes accessed | tf_op | source)
XLA Modules:
  0.0 51.3 jit_solution(6699055239982781191)
XLA Ops:
  0.0 2.5 %first_queries.1 = bf16[8,8,512]{2,1,0:T(8,128)(2,1)} custom-call(bf16[7,2048]{1,0:T(8,128)(2,1)} %hidden.3, f32[2,2048]{1,0:T(2,128)} %gain.7, bf16[2,2048,512]{2,1,0:T(8,128)(2,1)} %w_query.3), custom_call_target="tpu_custom_call" | custom-call | flops 16777216 | bytes 2097152 | tf_op jit(solution)/shard_map/first_queries/pallas_call | solution.py:194
  2.5 8.3 %all-to-all-start = ((bf16[8,8,512]{2,1,0:T(8,128)(2,1)}), bf16[8,8,512]{2,1,0:T(8,128)(2,1)S(1)}, u32[]{:S(2)}, u32[]{:S(2)}) async-start(bf16[8,8,512]{2,1,0:T(8,128)(2,1)} %first_queries.1), calls=%async_computation | async-start | bytes 131072 | tf_op jit(solution)/shard_map/all_to_all | solution.py:340
  10.8 3.5 %source_side.2 = (bf16[256,512]{1,0:T(8,128)(2,1)S(1)}, bf16[256,512]{1,0:T(8,128)(2,1)S(1)}) custom-call(bf16[256,2048]{1,0:T(8,128)(2,1)} %source.2, f32[2,2048]{1,0:T(2,128)} %gain.6, bf16[2,2048,512]{2,1,0:T(8,128)(2,1)} %w_key.3, bf16[2,2048,512]{2,1,0:T(8,128)(2,1)} %w_value.3), custom_call_target="tpu_custom_call" | custom-call | flops 1073741824 | bytes 4194304 | tf_op jit(solution)/shard_map/source_side/pallas_call | solution.py:101
  14.3 0.0 all-to-all-done.queries
  14.3 0.0 copy-start.3
  14.3 0.0 copy-start.1
  14.4 0.0 copy-start.4
  14.4 0.4 attend.2
  14.7 0.0 copy-start.6
  14.8 8.8 %all_to_all.20.packed = bf16[8,8,640]{2,1,0:T(8,128)(2,1)S(1)} all-to-all(bf16[8,8,640]{2,1,0:T(8,128)(2,1)S(1)} %attend.2), channel_id=1, replica_groups={{20,28,16,12,24,8,4,0},{21,29,17,13,25,9,5,1},{22,30,18,14,26,10,6,2},{..., dimensions={0} | all-to-all | bytes 163840 | tf_op jit(solution)/shard_map/all_to_all | solution.py:340
  23.6 0.5 share.2.rest_0_
  24.1 0.1 collective-permute-start.2
  24.2 1.6 %collective-permute-start.1 = (bf16[8,2048]{1,0:T(8,128)(2,1)S(1)}, bf16[8,2048]{1,0:T(8,128)(2,1)S(1)}, u32[]{:S(2)}, u32[]{:S(2)}) collective-permute-start(bf16[8,2048]{1,0:T(8,128)(2,1)S(1)} %share.2.rest_0_), channel_id=1, source_target_pairs={{0,2},{1,3},{2,0},{3,1},{4,6},{5,7},{6,4},{7,5},{8,10},{9,11},{10,... | collective-permute-start | bytes 98312 | tf_op jit(solution)/shard_map/ppermute | solution.py:346
  25.7 0.3 collective-permute-start
  26.0 0.0 copy-done.1
  26.0 1.4 %source_side.3 = (bf16[256,512]{1,0:T(8,128)(2,1)S(1)}, bf16[256,512]{1,0:T(8,128)(2,1)S(1)}) custom-call(bf16[256,2048]{1,0:T(8,128)(2,1)S(1)} %copy-done.4, f32[2,2048]{1,0:T(2,128)S(1)} %copy-done.6, bf16[2,2048,512]{2,1,0:T(8,128)(2,1)S(1)} %copy-done, bf16[2,2048,512]{2,1,0:T(8,128)(2,1)S(1)} %copy-done.1), custom_call_target="tpu_custom_call" | custom-call | flops 1073741824 | bytes 4194304 | tf_op jit(solution)/shard_map/source_side/pallas_call | solution.py:116
  27.4 0.4 collective-permute-done.2.rest_3_
  27.8 0.4 collective-permute-done.1.rest_2_
  28.2 0.0 collective-permute-done.rest_1_
  28.2 0.0 copy-done.2
  28.2 0.5 next_queries.1
  28.7 8.5 %all_to_all.21.queries = bf16[8,8,512]{2,1,0:T(8,128)(2,1)S(1)} all-to-all(bf16[8,8,512]{2,1,0:T(8,128)(2,1)S(1)} %get-tuple-element.30), channel_id=1, replica_groups={{20,28,16,12,24,8,4,0},{21,29,17,13,25,9,5,1},{22,30,18,14,26,10,6,2},{..., dimensions={0} | all-to-all | bytes 131072 | tf_op jit(solution)/shard_map/all_to_all | solution.py:340
  37.2 0.4 attend.3
  37.6 8.5 %all_to_all.22.packed = bf16[8,8,640]{2,1,0:T(8,128)(2,1)S(1)} all-to-all(bf16[8,8,640]{2,1,0:T(8,128)(2,1)S(1)} %attend.3), channel_id=1, replica_groups={{20,28,16,12,24,8,4,0},{21,29,17,13,25,9,5,1},{22,30,18,14,26,10,6,2},{..., dimensions={0} | all-to-all | bytes 163840 | tf_op jit(solution)/shard_map/all_to_all | solution.py:340
  46.1 0.5 share.3.rest_0_
  46.6 0.0 collective-permute-start.5
  46.6 1.6 %collective-permute-start.4 = (bf16[8,2048]{1,0:T(8,128)(2,1)S(1)}, bf16[8,2048]{1,0:T(8,128)(2,1)S(1)}, u32[]{:S(2)}, u32[]{:S(2)}) collective-permute-start(bf16[8,2048]{1,0:T(8,128)(2,1)S(1)} %share.3.rest_0_), channel_id=1, source_target_pairs={{0,2},{1,3},{2,0},{3,1},{4,6},{5,7},{6,4},{7,5},{8,10},{9,11},{10,... | collective-permute-start | bytes 98312 | tf_op jit(solution)/shard_map/ppermute | solution.py:346
  48.1 0.3 collective-permute-start.3
  48.4 1.8 %collective-permute-done.5.rest_3_ = bf16[8,2048]{1,0:T(8,128)(2,1)S(1)} collective-permute-done((bf16[8,2048]{1,0:T(8,128)(2,1)S(1)}, bf16[8,2048]{1,0:T(8,128)(2,1)S(1)}, u32[]{:S(2)}, u32[]{:S(2)}) %collective-permute-start.5) | collective-permute-done | bytes 32800 | tf_op jit(solution)/shard_map/ppermute | solution.py:346
  50.2 0.4 collective-permute-done.4.rest_2_
  50.6 0.0 collective-permute-done.3.rest_1_
  50.6 0.6 %last_rows.1 = bf16[7,2048]{1,0:T(8,128)(2,1)} custom-call(bf16[7,2048]{1,0:T(8,128)(2,1)S(1)} %get-tuple-element.29.hidden, bf16[8,2048]{1,0:T(8,128)(2,1)S(1)} %share.3.rest_0_, bf16[8,2048]{1,0:T(8,128)(2,1)S(1)} %collective-permute-done.3.rest_1_, bf16[8,2048]{1,0:T(8,128)(2,1)S(1)} %collective-permute-done.4.rest_2_, ...), custom_call_target="tpu_custom_call" | custom-call | tf_op jit(solution)/shard_map/last_rows/pallas_call | solution.py:234
  (12 shorter events, 0.0 us)
Async XLA Ops:
  2.5 11.8 %all-to-all-start = ((bf16[8,8,512]{2,1,0:T(8,128)(2,1)}), bf16[8,8,512]{2,1,0:T(8,128)(2,1)S(1)}, u32[]{:S(2)}, u32[]{:S(2)}) async-start(bf16[8,8,512]{2,1,0:T(8,128)(2,1)} %first_queries.1), calls=%async_computation | async-start | bytes 131072 | tf_op jit(solution)/shard_map/all_to_all | solution.py:340
  10.8 3.5 %copy-start.8 = (f32[2,2]{1,0:T(2,128)S(1)}, f32[2,2]{1,0:T(2,128)}, u32[]{:S(2)}) copy-start(f32[2,2]{1,0:T(2,128)} %scales.3) | copy-start | bytes 52
  14.3 9.2 %copy-start.3 = (bf16[2,512,2048]{2,1,0:T(8,128)(2,1)S(1)}, bf16[2,512,2048]{2,1,0:T(8,128)(2,1)}, u32[]{:S(2)}) copy-start(bf16[2,512,2048]{2,1,0:T(8,128)(2,1)} %w_out.3) | copy-start | bytes 12582916
  14.3 11.7 %copy-start.1 = (bf16[2,2048,512]{2,1,0:T(8,128)(2,1)S(1)}, bf16[2,2048,512]{2,1,0:T(8,128)(2,1)}, u32[]{:S(2)}) copy-start(bf16[2,2048,512]{2,1,0:T(8,128)(2,1)} %w_value.3) | copy-start | bytes 12582916
  14.4 11.7 %copy-start.4 = (bf16[256,2048]{1,0:T(8,128)(2,1)S(1)}, bf16[256,2048]{1,0:T(8,128)(2,1)}, u32[]{:S(2)}) copy-start(bf16[256,2048]{1,0:T(8,128)(2,1)} %source.2) | copy-start | bytes 3145732
  14.7 11.3 %copy-start = (bf16[2,2048,512]{2,1,0:T(8,128)(2,1)S(1)}, bf16[2,2048,512]{2,1,0:T(8,128)(2,1)}, u32[]{:S(2)}) copy-start(bf16[2,2048,512]{2,1,0:T(8,128)(2,1)} %w_key.3) | copy-start | bytes 12582916
  14.7 11.3 %copy-start.6 = (f32[2,2048]{1,0:T(2,128)S(1)}, f32[2,2048]{1,0:T(2,128)}, u32[]{:S(2)}) copy-start(f32[2,2048]{1,0:T(2,128)} %gain.6) | copy-start | bytes 49156
  24.1 4.1 %copy-start.2 = (bf16[2,2048,512]{2,1,0:T(8,128)(2,1)S(1)}, bf16[2,2048,512]{2,1,0:T(8,128)(2,1)}, u32[]{:S(2)}) copy-start(bf16[2,2048,512]{2,1,0:T(8,128)(2,1)} %w_query.3) | copy-start | bytes 12582916
  24.1 4.1 %copy-start.5 = (bf16[7,2048]{1,0:T(8,128)(2,1)S(1)}, bf16[7,2048]{1,0:T(8,128)(2,1)}, u32[]{:S(2)}) copy-start(bf16[7,2048]{1,0:T(8,128)(2,1)} %hidden.3) | copy-start | bytes 86020
  24.1 4.1 %copy-start.7 = (f32[2,2048]{1,0:T(2,128)S(1)}, f32[2,2048]{1,0:T(2,128)}, u32[]{:S(2)}) copy-start(f32[2,2048]{1,0:T(2,128)} %gain.7) | copy-start | bytes 49156
  24.1 3.7 %collective-permute-start.2 = (bf16[8,2048]{1,0:T(8,128)(2,1)S(1)}, bf16[8,2048]{1,0:T(8,128)(2,1)S(1)}, u32[]{:S(2)}, u32[]{:S(2)}) collective-permute-start(bf16[8,2048]{1,0:T(8,128)(2,1)S(1)} %share.2.rest_0_), channel_id=1, source_target_pairs={{0,3},{1,2},{2,1},{3,0},{4,7},{5,6},{6,5},{7,4},{8,11},{9,10},{10,... | collective-permute-start | bytes 98312 | tf_op jit(solution)/shard_map/ppermute | solution.py:346
  24.2 4.0 %collective-permute-start.1 = (bf16[8,2048]{1,0:T(8,128)(2,1)S(1)}, bf16[8,2048]{1,0:T(8,128)(2,1)S(1)}, u32[]{:S(2)}, u32[]{:S(2)}) collective-permute-start(bf16[8,2048]{1,0:T(8,128)(2,1)S(1)} %share.2.rest_0_), channel_id=1, source_target_pairs={{0,2},{1,3},{2,0},{3,1},{4,6},{5,7},{6,4},{7,5},{8,10},{9,11},{10,... | collective-permute-start | bytes 98312 | tf_op jit(solution)/shard_map/ppermute | solution.py:346
  25.7 2.5 %collective-permute-start = (bf16[8,2048]{1,0:T(8,128)(2,1)S(1)}, bf16[8,2048]{1,0:T(8,128)(2,1)S(1)}, u32[]{:S(2)}, u32[]{:S(2)}) collective-permute-start(bf16[8,2048]{1,0:T(8,128)(2,1)S(1)} %share.2.rest_0_), channel_id=1, source_target_pairs={{0,1},{1,0},{2,3},{3,2},{4,5},{5,4},{6,7},{7,6},{8,9},{9,8},{10,11... | collective-permute-start | bytes 98312 | tf_op jit(solution)/shard_map/ppermute | solution.py:346
  46.6 3.7 %collective-permute-start.5 = (bf16[8,2048]{1,0:T(8,128)(2,1)S(1)}, bf16[8,2048]{1,0:T(8,128)(2,1)S(1)}, u32[]{:S(2)}, u32[]{:S(2)}) collective-permute-start(bf16[8,2048]{1,0:T(8,128)(2,1)S(1)} %share.3.rest_0_), channel_id=1, source_target_pairs={{0,3},{1,2},{2,1},{3,0},{4,7},{5,6},{6,5},{7,4},{8,11},{9,10},{10,... | collective-permute-start | bytes 98312 | tf_op jit(solution)/shard_map/ppermute | solution.py:346
  46.6 4.0 %collective-permute-start.4 = (bf16[8,2048]{1,0:T(8,128)(2,1)S(1)}, bf16[8,2048]{1,0:T(8,128)(2,1)S(1)}, u32[]{:S(2)}, u32[]{:S(2)}) collective-permute-start(bf16[8,2048]{1,0:T(8,128)(2,1)S(1)} %share.3.rest_0_), channel_id=1, source_target_pairs={{0,2},{1,3},{2,0},{3,1},{4,6},{5,7},{6,4},{7,5},{8,10},{9,11},{10,... | collective-permute-start | bytes 98312 | tf_op jit(solution)/shard_map/ppermute | solution.py:346
  48.1 2.5 %collective-permute-start.3 = (bf16[8,2048]{1,0:T(8,128)(2,1)S(1)}, bf16[8,2048]{1,0:T(8,128)(2,1)S(1)}, u32[]{:S(2)}, u32[]{:S(2)}) collective-permute-start(bf16[8,2048]{1,0:T(8,128)(2,1)S(1)} %share.3.rest_0_), channel_id=1, source_target_pairs={{0,1},{1,0},{2,3},{3,2},{4,5},{5,4},{6,7},{7,6},{8,9},{9,8},{10,11... | collective-permute-start | bytes 98312 | tf_op jit(solution)/shard_map/ppermute | solution.py:346

commit v8 on v6

--- a/solution.py
+++ b/solution.py
@@ -241,6 +241,12 @@
     )(hidden, *shares)
 
 
+def places(blocks, padded, heads):
+    shape = (blocks, padded, LANES)
+    row = lax.broadcasted_iota(jnp.int32, shape, 1)
+    return lax.broadcasted_iota(jnp.int32, shape, 2) - 2 * heads * row, row
+
+
 def attend_kernel(layer, queries, keys, values, scales, packed):
     blocks, padded, columns = queries.shape
     rows = blocks * padded
@@ -266,21 +272,26 @@
         )
         for head, cut in zip(heads, cuts)
     ]
-    lane = lax.broadcasted_iota(jnp.int32, (rows, LANES), 1)
-    sums = jnp.zeros((rows, LANES), jnp.float32)
+    place, row = places(blocks, padded, len(heads))
+    sums = jnp.zeros(place.shape, jnp.float32)
     for head in heads:
         total = jnp.sum(weights[head], axis=1, keepdims=True)
         high = total.astype(jnp.bfloat16).astype(jnp.float32)
-        sums = jnp.where(lane == 2 * head, high, sums)
-        sums = jnp.where(lane == 2 * head + 1, total - high, sums)
+        shape = (blocks, padded, 1)
+        sums = jnp.where(place == 2 * head, high.reshape(shape), sums)
+        sums = jnp.where(place == 2 * head + 1, (total - high).reshape(shape), sums)
+    sums = jnp.sum(sums, axis=1, keepdims=True)
     for part, cut in zip(parts, cuts):
-        packed[:, :, cut] = part.astype(jnp.bfloat16).reshape(blocks, padded, HEAD_DIM)
-    packed[:, :, columns:] = sums.astype(jnp.bfloat16).reshape(blocks, padded, LANES)
+        part = part.reshape(blocks, padded, HEAD_DIM)
+        if cut.start == 0:
+            front = jnp.where(row == padded - 1, sums, part[:, :, :LANES])
+            part = jnp.concatenate([front, part[:, :, LANES:]], axis=2)
+        packed[:, :, cut] = part.astype(jnp.bfloat16)
 
 
 def attend(layer, queries, keys, values, scales):
     blocks, padded, columns = queries.shape
-    shape = (blocks, padded, columns + LANES)
+    shape = (blocks, padded, columns)
     return pl.pallas_call(
         functools.partial(attend_kernel, layer),
         grid=(1,),
@@ -300,12 +311,16 @@
 
 def share_kernel(packed, w_out, share):
     width = w_out.shape[1]
+    heads = width // HEAD_DIM
+    padded = packed.shape[1]
     total = jnp.sum(packed[...].astype(jnp.float32), axis=0)
+    place = places(1, padded, heads)[0].reshape(padded, LANES)
+    tail = jnp.broadcast_to(total[padded - 1 :, :LANES], (padded, LANES))
     branch = jnp.zeros(share.shape, jnp.float32)
-    for head in range(width // HEAD_DIM):
+    for head in range(heads):
         cut = slice(head * HEAD_DIM, (head + 1) * HEAD_DIM)
-        at = width + 2 * head
-        below = total[:, at : at + 1] + total[:, at + 1 : at + 2]
+        mine = (place == 2 * head) | (place == 2 * head + 1)
+        below = jnp.sum(jnp.where(mine, tail, 0.0), axis=1, keepdims=True)
         attended = (total[:, cut] / below).astype(jnp.bfloat16)
         branch = branch + jnp.dot(attended, w_out[0, cut, :], preferred_element_type=jnp.float32)
     share[...] = branch.astype(jnp.bfloat16)
@@ -350,7 +365,7 @@
 def body(order, target, source, tgt_gain, src_gain, w_query, w_key, w_value, w_out, score_scale):
     layers = w_query.shape[0]
     blocks = lax.axis_size("sp")
-    padded = -(-target.shape[0] // SUBLANES) * SUBLANES
+    padded = -(-(target.shape[0] + 1) // SUBLANES) * SUBLANES
     hidden = target
     queries = first_queries(0, hidden, tgt_gain, w_query, blocks, padded)
     keys, values = source_side(0, source, src_gain, w_key, w_value, True)

time: 51.6 us -> 51.4 us (level)
  no operation moved by 1% of the time
where the time goes in v8:
time: 51.4 us; the launch traced here: 51 us
  blocking collectives  25.7 us (50%)
  starting transfers between devices  12.1 us (24%)
  Pallas kernels  10.1 us (20%)
  waiting for transfers between devices  2.88 us (6%)
    all_to_all x3, blocking collectives, exchange(): return lax.all_to_all(blocks, 'sp', 0, 0, axis_index_groups=[order])  25.7 us
    all_to_all x1, starting transfers between devices, exchange(): return lax.all_to_all(blocks, 'sp', 0, 0, axis_index_groups=[order])  8.32 us
    ppermute x6, starting transfers between devices, over_groups(): lax.ppermute(share, 'tp', [(i, (i ^ m) % count) for i in range(count)])  3.78 us
    pallas_call x1, Pallas kernels, source_side(): pl.pallas_call(functools.partial(streaming_source_kernel, layer), in_spec...  3.45 us
    ppermute x6, waiting for transfers between devices, over_groups(): lax.ppermute(share, 'tp', [(i, (i ^ m) % count) for i in range(count)])  2.88 us
    pallas_call x1, Pallas kernels, first_queries(): pl.pallas_call(functools.partial(first_kernel, layer), in_specs=[IN_PLACE...  2.51 us
    pallas_call x1, Pallas kernels, source_side(): pl.pallas_call(functools.partial(source_kernel, layer), grid=(1,), in_spe...  1.46 us
  transfers between devices with their start and end apart: 7, of which 4 were waited for; matrix products, arithmetic and copies ran while one was open for 0% of the time, Pallas kernels for 10%

profile of v8, /device:TPU:0, one launch (start us, length us, event | category | flops | bytes accessed | tf_op | source)
XLA Modules:
  0.0 51.0 jit_solution(1652687831983259721)
XLA Ops:
  0.0 2.5 %first_queries.1 = bf16[8,8,512]{2,1,0:T(8,128)(2,1)} custom-call(bf16[7,2048]{1,0:T(8,128)(2,1)} %hidden.3, f32[2,2048]{1,0:T(2,128)} %gain.7, bf16[2,2048,512]{2,1,0:T(8,128)(2,1)} %w_query.3), custom_call_target="tpu_custom_call" | custom-call | flops 16777216 | bytes 2097152 | tf_op jit(solution)/shard_map/first_queries/pallas_call | solution.py:193
  2.5 8.3 %all-to-all-start = ((bf16[8,8,512]{2,1,0:T(8,128)(2,1)}), bf16[8,8,512]{2,1,0:T(8,128)(2,1)S(1)}, u32[]{:S(2)}, u32[]{:S(2)}) async-start(bf16[8,8,512]{2,1,0:T(8,128)(2,1)} %first_queries.1), calls=%async_computation | async-start | bytes 131072 | tf_op jit(solution)/shard_map/all_to_all | solution.py:354
  10.8 3.5 %source_side.2 = (bf16[256,512]{1,0:T(8,128)(2,1)S(1)}, bf16[256,512]{1,0:T(8,128)(2,1)S(1)}) custom-call(bf16[256,2048]{1,0:T(8,128)(2,1)} %source.2, f32[2,2048]{1,0:T(2,128)} %gain.6, bf16[2,2048,512]{2,1,0:T(8,128)(2,1)} %w_key.3, bf16[2,2048,512]{2,1,0:T(8,128)(2,1)} %w_value.3), custom_call_target="tpu_custom_call" | custom-call | flops 1073741824 | bytes 4194304 | tf_op jit(solution)/shard_map/source_side/pallas_call | solution.py:97
  14.3 0.0 all-to-all-done.queries
  14.3 0.0 copy-start.3
  14.3 0.0 copy-start.1
  14.4 0.0 copy-start.4
  14.4 0.4 attend.2
  14.7 0.0 copy-start
  14.7 0.0 copy-start.6
  14.8 8.8 %all_to_all.20.packed = bf16[8,8,512]{2,1,0:T(8,128)(2,1)S(1)} all-to-all(bf16[8,8,512]{2,1,0:T(8,128)(2,1)S(1)} %attend.2), channel_id=1, replica_groups={{20,28,16,12,24,8,4,0},{21,29,17,13,25,9,5,1},{22,30,18,14,26,10,6,2},{..., dimensions={0} | all-to-all | bytes 131072 | tf_op jit(solution)/shard_map/all_to_all | solution.py:354
  23.5 0.4 share.2.rest_0_
  24.0 0.1 collective-permute-start.2
  24.1 1.6 %collective-permute-start.1 = (bf16[8,2048]{1,0:T(8,128)(2,1)S(1)}, bf16[8,2048]{1,0:T(8,128)(2,1)S(1)}, u32[]{:S(2)}, u32[]{:S(2)}) collective-permute-start(bf16[8,2048]{1,0:T(8,128)(2,1)S(1)} %share.2.rest_0_), channel_id=1, source_target_pairs={{0,2},{1,3},{2,0},{3,1},{4,6},{5,7},{6,4},{7,5},{8,10},{9,11},{10,... | collective-permute-start | bytes 98312 | tf_op jit(solution)/shard_map/ppermute | solution.py:360
  25.6 0.3 collective-permute-start
  25.9 0.0 copy-done
  25.9 1.5 %source_side.3 = (bf16[256,512]{1,0:T(8,128)(2,1)S(1)}, bf16[256,512]{1,0:T(8,128)(2,1)S(1)}) custom-call(bf16[256,2048]{1,0:T(8,128)(2,1)S(1)} %copy-done.4, f32[2,2048]{1,0:T(2,128)S(1)} %copy-done.6, bf16[2,2048,512]{2,1,0:T(8,128)(2,1)S(1)} %copy-done, bf16[2,2048,512]{2,1,0:T(8,128)(2,1)S(1)} %copy-done.1), custom_call_target="tpu_custom_call" | custom-call | flops 1073741824 | bytes 4194304 | tf_op jit(solution)/shard_map/source_side/pallas_call | solution.py:112
  27.4 0.3 collective-permute-done.2.rest_3_
  27.7 0.4 collective-permute-done.1.rest_2_
  28.1 0.0 collective-permute-done.rest_1_
  28.1 0.5 next_queries.1
  28.6 8.5 %all_to_all.21.queries = bf16[8,8,512]{2,1,0:T(8,128)(2,1)S(1)} all-to-all(bf16[8,8,512]{2,1,0:T(8,128)(2,1)S(1)} %get-tuple-element.30), channel_id=1, replica_groups={{20,28,16,12,24,8,4,0},{21,29,17,13,25,9,5,1},{22,30,18,14,26,10,6,2},{..., dimensions={0} | all-to-all | bytes 131072 | tf_op jit(solution)/shard_map/all_to_all | solution.py:354
  37.1 0.4 attend.3
  37.4 8.5 %all_to_all.22.packed = bf16[8,8,512]{2,1,0:T(8,128)(2,1)S(1)} all-to-all(bf16[8,8,512]{2,1,0:T(8,128)(2,1)S(1)} %attend.3), channel_id=1, replica_groups={{20,28,16,12,24,8,4,0},{21,29,17,13,25,9,5,1},{22,30,18,14,26,10,6,2},{..., dimensions={0} | all-to-all | bytes 131072 | tf_op jit(solution)/shard_map/all_to_all | solution.py:354
  45.9 0.4 share.3.rest_0_
  46.3 0.0 collective-permute-start.5
  46.3 1.6 %collective-permute-start.4 = (bf16[8,2048]{1,0:T(8,128)(2,1)S(1)}, bf16[8,2048]{1,0:T(8,128)(2,1)S(1)}, u32[]{:S(2)}, u32[]{:S(2)}) collective-permute-start(bf16[8,2048]{1,0:T(8,128)(2,1)S(1)} %share.3.rest_0_), channel_id=1, source_target_pairs={{0,2},{1,3},{2,0},{3,1},{4,6},{5,7},{6,4},{7,5},{8,10},{9,11},{10,... | collective-permute-start | bytes 98312 | tf_op jit(solution)/shard_map/ppermute | solution.py:360
  47.9 0.3 collective-permute-start.3
  48.2 1.8 %collective-permute-done.5.rest_3_ = bf16[8,2048]{1,0:T(8,128)(2,1)S(1)} collective-permute-done((bf16[8,2048]{1,0:T(8,128)(2,1)S(1)}, bf16[8,2048]{1,0:T(8,128)(2,1)S(1)}, u32[]{:S(2)}, u32[]{:S(2)}) %collective-permute-start.5) | collective-permute-done | bytes 32800 | tf_op jit(solution)/shard_map/ppermute | solution.py:360
  50.0 0.4 collective-permute-done.4.rest_2_
  50.4 0.0 collective-permute-done.3.rest_1_
  50.4 0.6 %last_rows.1 = bf16[7,2048]{1,0:T(8,128)(2,1)} custom-call(bf16[7,2048]{1,0:T(8,128)(2,1)S(1)} %get-tuple-element.29.hidden, bf16[8,2048]{1,0:T(8,128)(2,1)S(1)} %share.3.rest_0_, bf16[8,2048]{1,0:T(8,128)(2,1)S(1)} %collective-permute-done.3.rest_1_, bf16[8,2048]{1,0:T(8,128)(2,1)S(1)} %collective-permute-done.4.rest_2_, ...), custom_call_target="tpu_custom_call" | custom-call | tf_op jit(solution)/shard_map/last_rows/pallas_call | solution.py:233
  (12 shorter events, 0.0 us)
Async XLA Ops:
  2.5 11.8 %all-to-all-start = ((bf16[8,8,512]{2,1,0:T(8,128)(2,1)}), bf16[8,8,512]{2,1,0:T(8,128)(2,1)S(1)}, u32[]{:S(2)}, u32[]{:S(2)}) async-start(bf16[8,8,512]{2,1,0:T(8,128)(2,1)} %first_queries.1), calls=%async_computation | async-start | bytes 131072 | tf_op jit(solution)/shard_map/all_to_all | solution.py:354
  10.8 3.5 %copy-start.8 = (f32[2,2]{1,0:T(2,128)S(1)}, f32[2,2]{1,0:T(2,128)}, u32[]{:S(2)}) copy-start(f32[2,2]{1,0:T(2,128)} %scales.3) | copy-start | bytes 52
  14.3 9.2 %copy-start.3 = (bf16[2,512,2048]{2,1,0:T(8,128)(2,1)S(1)}, bf16[2,512,2048]{2,1,0:T(8,128)(2,1)}, u32[]{:S(2)}) copy-start(bf16[2,512,2048]{2,1,0:T(8,128)(2,1)} %w_out.3) | copy-start | bytes 12582916
  14.3 11.6 %copy-start.1 = (bf16[2,2048,512]{2,1,0:T(8,128)(2,1)S(1)}, bf16[2,2048,512]{2,1,0:T(8,128)(2,1)}, u32[]{:S(2)}) copy-start(bf16[2,2048,512]{2,1,0:T(8,128)(2,1)} %w_value.3) | copy-start | bytes 12582916
  14.4 11.6 %copy-start.4 = (bf16[256,2048]{1,0:T(8,128)(2,1)S(1)}, bf16[256,2048]{1,0:T(8,128)(2,1)}, u32[]{:S(2)}) copy-start(bf16[256,2048]{1,0:T(8,128)(2,1)} %source.2) | copy-start | bytes 3145732
  14.7 11.2 %copy-start = (bf16[2,2048,512]{2,1,0:T(8,128)(2,1)S(1)}, bf16[2,2048,512]{2,1,0:T(8,128)(2,1)}, u32[]{:S(2)}) copy-start(bf16[2,2048,512]{2,1,0:T(8,128)(2,1)} %w_key.3) | copy-start | bytes 12582916
  14.7 11.2 %copy-start.6 = (f32[2,2048]{1,0:T(2,128)S(1)}, f32[2,2048]{1,0:T(2,128)}, u32[]{:S(2)}) copy-start(f32[2,2048]{1,0:T(2,128)} %gain.6) | copy-start | bytes 49156
  24.0 4.1 %copy-start.2 = (bf16[2,2048,512]{2,1,0:T(8,128)(2,1)S(1)}, bf16[2,2048,512]{2,1,0:T(8,128)(2,1)}, u32[]{:S(2)}) copy-start(bf16[2,2048,512]{2,1,0:T(8,128)(2,1)} %w_query.3) | copy-start | bytes 12582916
  24.0 4.1 %copy-start.5 = (bf16[7,2048]{1,0:T(8,128)(2,1)S(1)}, bf16[7,2048]{1,0:T(8,128)(2,1)}, u32[]{:S(2)}) copy-start(bf16[7,2048]{1,0:T(8,128)(2,1)} %hidden.3) | copy-start | bytes 86020
  24.0 4.1 %copy-start.7 = (f32[2,2048]{1,0:T(2,128)S(1)}, f32[2,2048]{1,0:T(2,128)}, u32[]{:S(2)}) copy-start(f32[2,2048]{1,0:T(2,128)} %gain.7) | copy-start | bytes 49156
  24.0 3.7 %collective-permute-start.2 = (bf16[8,2048]{1,0:T(8,128)(2,1)S(1)}, bf16[8,2048]{1,0:T(8,128)(2,1)S(1)}, u32[]{:S(2)}, u32[]{:S(2)}) collective-permute-start(bf16[8,2048]{1,0:T(8,128)(2,1)S(1)} %share.2.rest_0_), channel_id=1, source_target_pairs={{0,3},{1,2},{2,1},{3,0},{4,7},{5,6},{6,5},{7,4},{8,11},{9,10},{10,... | collective-permute-start | bytes 98312 | tf_op jit(solution)/shard_map/ppermute | solution.py:360
  24.1 4.0 %collective-permute-start.1 = (bf16[8,2048]{1,0:T(8,128)(2,1)S(1)}, bf16[8,2048]{1,0:T(8,128)(2,1)S(1)}, u32[]{:S(2)}, u32[]{:S(2)}) collective-permute-start(bf16[8,2048]{1,0:T(8,128)(2,1)S(1)} %share.2.rest_0_), channel_id=1, source_target_pairs={{0,2},{1,3},{2,0},{3,1},{4,6},{5,7},{6,4},{7,5},{8,10},{9,11},{10,... | collective-permute-start | bytes 98312 | tf_op jit(solution)/shard_map/ppermute | solution.py:360
  25.6 2.5 %collective-permute-start = (bf16[8,2048]{1,0:T(8,128)(2,1)S(1)}, bf16[8,2048]{1,0:T(8,128)(2,1)S(1)}, u32[]{:S(2)}, u32[]{:S(2)}) collective-permute-start(bf16[8,2048]{1,0:T(8,128)(2,1)S(1)} %share.2.rest_0_), channel_id=1, source_target_pairs={{0,1},{1,0},{2,3},{3,2},{4,5},{5,4},{6,7},{7,6},{8,9},{9,8},{10,11... | collective-permute-start | bytes 98312 | tf_op jit(solution)/shard_map/ppermute | solution.py:360
  46.3 3.7 %collective-permute-start.5 = (bf16[8,2048]{1,0:T(8,128)(2,1)S(1)}, bf16[8,2048]{1,0:T(8,128)(2,1)S(1)}, u32[]{:S(2)}, u32[]{:S(2)}) collective-permute-start(bf16[8,2048]{1,0:T(8,128)(2,1)S(1)} %share.3.rest_0_), channel_id=1, source_target_pairs={{0,3},{1,2},{2,1},{3,0},{4,7},{5,6},{6,5},{7,4},{8,11},{9,10},{10,... | collective-permute-start | bytes 98312 | tf_op jit(solution)/shard_map/ppermute | solution.py:360
  46.3 4.0 %collective-permute-start.4 = (bf16[8,2048]{1,0:T(8,128)(2,1)S(1)}, bf16[8,2048]{1,0:T(8,128)(2,1)S(1)}, u32[]{:S(2)}, u32[]{:S(2)}) collective-permute-start(bf16[8,2048]{1,0:T(8,128)(2,1)S(1)} %share.3.rest_0_), channel_id=1, source_target_pairs={{0,2},{1,3},{2,0},{3,1},{4,6},{5,7},{6,4},{7,5},{8,10},{9,11},{10,... | collective-permute-start | bytes 98312 | tf_op jit(solution)/shard_map/ppermute | solution.py:360
  47.9 2.5 %collective-permute-start.3 = (bf16[8,2048]{1,0:T(8,128)(2,1)S(1)}, bf16[8,2048]{1,0:T(8,128)(2,1)S(1)}, u32[]{:S(2)}, u32[]{:S(2)}) collective-permute-start(bf16[8,2048]{1,0:T(8,128)(2,1)S(1)} %share.3.rest_0_), channel_id=1, source_target_pairs={{0,1},{1,0},{2,3},{3,2},{4,5},{5,4},{6,7},{7,6},{8,9},{9,8},{10,11... | collective-permute-start | bytes 98312 | tf_op jit(solution)/shard_map/ppermute | solution.py:360

commit v9 on v8

--- a/solution.py
+++ b/solution.py
@@ -51,12 +51,9 @@
 
 
 def streaming_source_kernel(layer, source, gain, w_key, w_value, keys, values, *scratch):
-    rows, gains, held_key, held_value, arrived = scratch
+    held_key, held_value, arrived = scratch
     depth = w_key.shape[1] // PIECES
-    copies = [
-        pltpu.make_async_copy(source, rows, arrived.at[0]),
-        pltpu.make_async_copy(gain, gains, arrived.at[1]),
-    ]
+    copies = []
     for weight, held in ((w_key, held_key), (w_value, held_value)):
         for piece in range(PIECES):
             cut = pl.ds(piece * depth, depth)
@@ -67,13 +64,11 @@
             )
     for copy in copies:
         copy.start()
-    copies[0].wait()
-    copies[1].wait()
-    normed = normed_rows(rows[...].astype(jnp.float32), gains[layer : layer + 1, :])
-    for copy in copies[2 : 2 + PIECES]:
+    normed = normed_rows(source[...].astype(jnp.float32), gain[layer : layer + 1, :])
+    for copy in copies[:PIECES]:
         copy.wait()
     keys_of(normed, held_key[...], keys)
-    for copy in copies[2 + PIECES :]:
+    for copy in copies[PIECES:]:
         copy.wait()
     values_of(normed, held_value[...], values)
 
@@ -96,18 +91,16 @@
     if streaming:
         return pl.pallas_call(
             functools.partial(streaming_source_kernel, layer),
-            in_specs=[IN_PLACE] * 4,
+            in_specs=[IN_VMEM, IN_VMEM, IN_PLACE, IN_PLACE],
             out_specs=[IN_VMEM] * 2,
             scratch_shapes=[
-                VMEM(source.shape, source.dtype),
-                VMEM(gain.shape, gain.dtype),
                 VMEM((width, columns), jnp.bfloat16),
                 VMEM((width, columns), jnp.bfloat16),
-                pltpu.SemaphoreType.DMA((2 + 2 * PIECES,)),
+                pltpu.SemaphoreType.DMA((2 * PIECES,)),
             ],
             compiler_params=pltpu.CompilerParams(vmem_limit_bytes=16 << 20),
             **common,
-        )(in_hbm(source), in_hbm(gain), in_hbm(w_key), in_hbm(w_value))
+        )(source, gain, in_hbm(w_key), in_hbm(w_value))
     weight = layer_of(w_key.shape, layer)
     return pl.pallas_call(
         functools.partial(source_kernel, layer),

time: 51.4 us -> 51.4 us (level)
  transfers between devices with their start and end apart: 7 -> 7, of which waited for: 4 -> 5; matrix products, arithmetic and copies ran while one was open for 0% -> 0% of each run, Pallas kernels for 10% -> 9%
where the time goes in v9:
time: 51.4 us; the launch traced here: 51.1 us
  blocking collectives  25.8 us (50%)
  starting transfers between devices  12.1 us (24%)
  Pallas kernels  9.89 us (19%)
  waiting for transfers between devices  3.11 us (6%)
    all_to_all x3, blocking collectives, exchange(): return lax.all_to_all(blocks, 'sp', 0, 0, axis_index_groups=[order])  25.8 us
    all_to_all x1, starting transfers between devices, exchange(): return lax.all_to_all(blocks, 'sp', 0, 0, axis_index_groups=[order])  8.32 us
    ppermute x6, starting transfers between devices, over_groups(): lax.ppermute(share, 'tp', [(i, (i ^ m) % count) for i in range(count)])  3.78 us
    pallas_call x1, Pallas kernels, source_side(): pl.pallas_call(functools.partial(streaming_source_kernel, layer), in_spec...  3.1 us
    ppermute x6, waiting for transfers between devices, over_groups(): lax.ppermute(share, 'tp', [(i, (i ^ m) % count) for i in range(count)])  2.88 us
    pallas_call x1, Pallas kernels, first_queries(): pl.pallas_call(functools.partial(first_kernel, layer), in_specs=[IN_PLACE...  2.6 us
    pallas_call x1, Pallas kernels, source_side(): pl.pallas_call(functools.partial(source_kernel, layer), grid=(1,), in_spe...  1.47 us
  transfers between devices with their start and end apart: 7, of which 5 were waited for; matrix products, arithmetic and copies ran while one was open for 0% of the time, Pallas kernels for 9%

profile of v9, /device:TPU:0, one launch (start us, length us, event | category | flops | bytes accessed | tf_op | source)
XLA Modules:
  0.0 51.1 jit_solution(16142445691637014425)
XLA Ops:
  0.0 2.6 %first_queries.1 = bf16[8,8,512]{2,1,0:T(8,128)(2,1)} custom-call(bf16[7,2048]{1,0:T(8,128)(2,1)} %hidden.3, f32[2,2048]{1,0:T(2,128)} %gain.7, bf16[2,2048,512]{2,1,0:T(8,128)(2,1)} %w_query.3), custom_call_target="tpu_custom_call" | custom-call | flops 16777216 | bytes 2097152 | tf_op jit(solution)/shard_map/first_queries/pallas_call | solution.py:186
  2.6 8.3 %all-to-all-start = ((bf16[8,8,512]{2,1,0:T(8,128)(2,1)}), bf16[8,8,512]{2,1,0:T(8,128)(2,1)S(1)}, u32[]{:S(2)}, u32[]{:S(2)}) async-start(bf16[8,8,512]{2,1,0:T(8,128)(2,1)} %first_queries.1), calls=%async_computation | async-start | bytes 131072 | tf_op jit(solution)/shard_map/all_to_all | solution.py:347
  10.9 0.0 copy-done.6
  10.9 0.0 copy-done.4
  10.9 0.0 copy-start.8
  11.0 3.1 %source_side.2 = (bf16[256,512]{1,0:T(8,128)(2,1)S(1)}, bf16[256,512]{1,0:T(8,128)(2,1)S(1)}) custom-call(bf16[256,2048]{1,0:T(8,128)(2,1)S(1)} %copy-done.4, f32[2,2048]{1,0:T(2,128)S(1)} %copy-done.6, bf16[2,2048,512]{2,1,0:T(8,128)(2,1)} %w_key.3, bf16[2,2048,512]{2,1,0:T(8,128)(2,1)} %w_value.3), custom_call_target="tpu_custom_call" | custom-call | flops 1073741824 | bytes 4194304 | tf_op jit(solution)/shard_map/source_side/pallas_call | solution.py:92
  14.1 0.2 all-to-all-done.queries
  14.3 0.0 copy-done.8
  14.3 0.4 attend.2
  14.7 0.0 copy-start
  14.7 8.9 %all_to_all.20.packed = bf16[8,8,512]{2,1,0:T(8,128)(2,1)S(1)} all-to-all(bf16[8,8,512]{2,1,0:T(8,128)(2,1)S(1)} %attend.2), channel_id=1, replica_groups={{20,28,16,12,24,8,4,0},{21,29,17,13,25,9,5,1},{22,30,18,14,26,10,6,2},{..., dimensions={0} | all-to-all | bytes 131072 | tf_op jit(solution)/shard_map/all_to_all | solution.py:347
  23.6 0.0 copy-done.3
  23.6 0.4 share.2.rest_0_
  24.1 0.1 collective-permute-start.2
  24.1 1.6 %collective-permute-start.1 = (bf16[8,2048]{1,0:T(8,128)(2,1)S(1)}, bf16[8,2048]{1,0:T(8,128)(2,1)S(1)}, u32[]{:S(2)}, u32[]{:S(2)}) collective-permute-start(bf16[8,2048]{1,0:T(8,128)(2,1)S(1)} %share.2.rest_0_), channel_id=1, source_target_pairs={{0,2},{1,3},{2,0},{3,1},{4,6},{5,7},{6,4},{7,5},{8,10},{9,11},{10,... | collective-permute-start | bytes 98312 | tf_op jit(solution)/shard_map/ppermute | solution.py:353
  25.7 0.3 collective-permute-start
  26.0 1.5 %source_side.3 = (bf16[256,512]{1,0:T(8,128)(2,1)S(1)}, bf16[256,512]{1,0:T(8,128)(2,1)S(1)}) custom-call(bf16[256,2048]{1,0:T(8,128)(2,1)S(1)} %copy-done.4, f32[2,2048]{1,0:T(2,128)S(1)} %copy-done.6, bf16[2,2048,512]{2,1,0:T(8,128)(2,1)S(1)} %copy-done, bf16[2,2048,512]{2,1,0:T(8,128)(2,1)S(1)} %copy-done.1), custom_call_target="tpu_custom_call" | custom-call | flops 1073741824 | bytes 4194304 | tf_op jit(solution)/shard_map/source_side/pallas_call | solution.py:105
  27.5 0.3 collective-permute-done.2.rest_3_
  27.8 0.4 collective-permute-done.1.rest_2_
  28.2 0.0 collective-permute-done.rest_1_
  28.2 0.5 next_queries.1
  28.7 8.5 %all_to_all.21.queries = bf16[8,8,512]{2,1,0:T(8,128)(2,1)S(1)} all-to-all(bf16[8,8,512]{2,1,0:T(8,128)(2,1)S(1)} %get-tuple-element.30), channel_id=1, replica_groups={{20,28,16,12,24,8,4,0},{21,29,17,13,25,9,5,1},{22,30,18,14,26,10,6,2},{..., dimensions={0} | all-to-all | bytes 131072 | tf_op jit(solution)/shard_map/all_to_all | solution.py:347
  37.1 0.4 attend.3
  37.5 8.5 %all_to_all.22.packed = bf16[8,8,512]{2,1,0:T(8,128)(2,1)S(1)} all-to-all(bf16[8,8,512]{2,1,0:T(8,128)(2,1)S(1)} %attend.3), channel_id=1, replica_groups={{20,28,16,12,24,8,4,0},{21,29,17,13,25,9,5,1},{22,30,18,14,26,10,6,2},{..., dimensions={0} | all-to-all | bytes 131072 | tf_op jit(solution)/shard_map/all_to_all | solution.py:347
  46.0 0.4 share.3.rest_0_
  46.4 0.0 collective-permute-start.5
  46.4 1.6 %collective-permute-start.4 = (bf16[8,2048]{1,0:T(8,128)(2,1)S(1)}, bf16[8,2048]{1,0:T(8,128)(2,1)S(1)}, u32[]{:S(2)}, u32[]{:S(2)}) collective-permute-start(bf16[8,2048]{1,0:T(8,128)(2,1)S(1)} %share.3.rest_0_), channel_id=1, source_target_pairs={{0,2},{1,3},{2,0},{3,1},{4,6},{5,7},{6,4},{7,5},{8,10},{9,11},{10,... | collective-permute-start | bytes 98312 | tf_op jit(solution)/shard_map/ppermute | solution.py:353
  48.0 0.3 collective-permute-start.3
  48.3 1.8 %collective-permute-done.5.rest_3_ = bf16[8,2048]{1,0:T(8,128)(2,1)S(1)} collective-permute-done((bf16[8,2048]{1,0:T(8,128)(2,1)S(1)}, bf16[8,2048]{1,0:T(8,128)(2,1)S(1)}, u32[]{:S(2)}, u32[]{:S(2)}) %collective-permute-start.5) | collective-permute-done | bytes 32800 | tf_op jit(solution)/shard_map/ppermute | solution.py:353
  50.1 0.4 collective-permute-done.4.rest_2_
  50.5 0.0 collective-permute-done.3.rest_1_
  50.5 0.6 %last_rows.1 = bf16[7,2048]{1,0:T(8,128)(2,1)} custom-call(bf16[7,2048]{1,0:T(8,128)(2,1)S(1)} %get-tuple-element.29.hidden, bf16[8,2048]{1,0:T(8,128)(2,1)S(1)} %share.3.rest_0_, bf16[8,2048]{1,0:T(8,128)(2,1)S(1)} %collective-permute-done.3.rest_1_, bf16[8,2048]{1,0:T(8,128)(2,1)S(1)} %collective-permute-done.4.rest_2_, ...), custom_call_target="tpu_custom_call" | custom-call | tf_op jit(solution)/shard_map/last_rows/pallas_call | solution.py:226
  (12 shorter events, 0.0 us)
Async XLA Ops:
  0.0 10.9 %copy-start.6 = (f32[2,2048]{1,0:T(2,128)S(1)}, f32[2,2048]{1,0:T(2,128)}, u32[]{:S(2)}) copy-start(f32[2,2048]{1,0:T(2,128)} %gain.6) | copy-start | bytes 49156
  0.0 10.9 %copy-start.4 = (bf16[256,2048]{1,0:T(8,128)(2,1)S(1)}, bf16[256,2048]{1,0:T(8,128)(2,1)}, u32[]{:S(2)}) copy-start(bf16[256,2048]{1,0:T(8,128)(2,1)} %source.2) | copy-start | bytes 3145732
  2.6 11.7 %all-to-all-start = ((bf16[8,8,512]{2,1,0:T(8,128)(2,1)}), bf16[8,8,512]{2,1,0:T(8,128)(2,1)S(1)}, u32[]{:S(2)}, u32[]{:S(2)}) async-start(bf16[8,8,512]{2,1,0:T(8,128)(2,1)} %first_queries.1), calls=%async_computation | async-start | bytes 131072 | tf_op jit(solution)/shard_map/all_to_all | solution.py:347
  10.9 3.4 %copy-start.8 = (f32[2,2]{1,0:T(2,128)S(1)}, f32[2,2]{1,0:T(2,128)}, u32[]{:S(2)}) copy-start(f32[2,2]{1,0:T(2,128)} %scales.3) | copy-start | bytes 52
  14.3 9.3 %copy-start.3 = (bf16[2,512,2048]{2,1,0:T(8,128)(2,1)S(1)}, bf16[2,512,2048]{2,1,0:T(8,128)(2,1)}, u32[]{:S(2)}) copy-start(bf16[2,512,2048]{2,1,0:T(8,128)(2,1)} %w_out.3) | copy-start | bytes 12582916
  14.3 11.7 %copy-start.1 = (bf16[2,2048,512]{2,1,0:T(8,128)(2,1)S(1)}, bf16[2,2048,512]{2,1,0:T(8,128)(2,1)}, u32[]{:S(2)}) copy-start(bf16[2,2048,512]{2,1,0:T(8,128)(2,1)} %w_value.3) | copy-start | bytes 12582916
  14.7 11.3 %copy-start = (bf16[2,2048,512]{2,1,0:T(8,128)(2,1)S(1)}, bf16[2,2048,512]{2,1,0:T(8,128)(2,1)}, u32[]{:S(2)}) copy-start(bf16[2,2048,512]{2,1,0:T(8,128)(2,1)} %w_key.3) | copy-start | bytes 12582916
  24.0 4.1 %copy-start.2 = (bf16[2,2048,512]{2,1,0:T(8,128)(2,1)S(1)}, bf16[2,2048,512]{2,1,0:T(8,128)(2,1)}, u32[]{:S(2)}) copy-start(bf16[2,2048,512]{2,1,0:T(8,128)(2,1)} %w_query.3) | copy-start | bytes 12582916
  24.1 4.1 %copy-start.5 = (bf16[7,2048]{1,0:T(8,128)(2,1)S(1)}, bf16[7,2048]{1,0:T(8,128)(2,1)}, u32[]{:S(2)}) copy-start(bf16[7,2048]{1,0:T(8,128)(2,1)} %hidden.3) | copy-start | bytes 86020
  24.1 4.1 %copy-start.7 = (f32[2,2048]{1,0:T(2,128)S(1)}, f32[2,2048]{1,0:T(2,128)}, u32[]{:S(2)}) copy-start(f32[2,2048]{1,0:T(2,128)} %gain.7) | copy-start | bytes 49156
  24.1 3.7 %collective-permute-start.2 = (bf16[8,2048]{1,0:T(8,128)(2,1)S(1)}, bf16[8,2048]{1,0:T(8,128)(2,1)S(1)}, u32[]{:S(2)}, u32[]{:S(2)}) collective-permute-start(bf16[8,2048]{1,0:T(8,128)(2,1)S(1)} %share.2.rest_0_), channel_id=1, source_target_pairs={{0,3},{1,2},{2,1},{3,0},{4,7},{5,6},{6,5},{7,4},{8,11},{9,10},{10,... | collective-permute-start | bytes 98312 | tf_op jit(solution)/shard_map/ppermute | solution.py:353
  24.1 4.0 %collective-permute-start.1 = (bf16[8,2048]{1,0:T(8,128)(2,1)S(1)}, bf16[8,2048]{1,0:T(8,128)(2,1)S(1)}, u32[]{:S(2)}, u32[]{:S(2)}) collective-permute-start(bf16[8,2048]{1,0:T(8,128)(2,1)S(1)} %share.2.rest_0_), channel_id=1, source_target_pairs={{0,2},{1,3},{2,0},{3,1},{4,6},{5,7},{6,4},{7,5},{8,10},{9,11},{10,... | collective-permute-start | bytes 98312 | tf_op jit(solution)/shard_map/ppermute | solution.py:353
  25.7 2.5 %collective-permute-start = (bf16[8,2048]{1,0:T(8,128)(2,1)S(1)}, bf16[8,2048]{1,0:T(8,128)(2,1)S(1)}, u32[]{:S(2)}, u32[]{:S(2)}) collective-permute-start(bf16[8,2048]{1,0:T(8,128)(2,1)S(1)} %share.2.rest_0_), channel_id=1, source_target_pairs={{0,1},{1,0},{2,3},{3,2},{4,5},{5,4},{6,7},{7,6},{8,9},{9,8},{10,11... | collective-permute-start | bytes 98312 | tf_op jit(solution)/shard_map/ppermute | solution.py:353
  46.4 3.7 %collective-permute-start.5 = (bf16[8,2048]{1,0:T(8,128)(2,1)S(1)}, bf16[8,2048]{1,0:T(8,128)(2,1)S(1)}, u32[]{:S(2)}, u32[]{:S(2)}) collective-permute-start(bf16[8,2048]{1,0:T(8,128)(2,1)S(1)} %share.3.rest_0_), channel_id=1, source_target_pairs={{0,3},{1,2},{2,1},{3,0},{4,7},{5,6},{6,5},{7,4},{8,11},{9,10},{10,... | collective-permute-start | bytes 98312 | tf_op jit(solution)/shard_map/ppermute | solution.py:353
  46.4 4.0 %collective-permute-start.4 = (bf16[8,2048]{1,0:T(8,128)(2,1)S(1)}, bf16[8,2048]{1,0:T(8,128)(2,1)S(1)}, u32[]{:S(2)}, u32[]{:S(2)}) collective-permute-start(bf16[8,2048]{1,0:T(8,128)(2,1)S(1)} %share.3.rest_0_), channel_id=1, source_target_pairs={{0,2},{1,3},{2,0},{3,1},{4,6},{5,7},{6,4},{7,5},{8,10},{9,11},{10,... | collective-permute-start | bytes 98312 | tf_op jit(solution)/shard_map/ppermute | solution.py:353
  48.0 2.5 %collective-permute-start.3 = (bf16[8,2048]{1,0:T(8,128)(2,1)S(1)}, bf16[8,2048]{1,0:T(8,128)(2,1)S(1)}, u32[]{:S(2)}, u32[]{:S(2)}) collective-permute-start(bf16[8,2048]{1,0:T(8,128)(2,1)S(1)} %share.3.rest_0_), channel_id=1, source_target_pairs={{0,1},{1,0},{2,3},{3,2},{4,5},{5,4},{6,7},{7,6},{8,9},{9,8},{10,11... | collective-permute-start | bytes 98312 | tf_op jit(solution)/shard_map/ppermute | solution.py:353

commit v10 on v9

--- a/solution.py
+++ b/solution.py
@@ -68,9 +68,14 @@
     for copy in copies[:PIECES]:
         copy.wait()
     keys_of(normed, held_key[...], keys)
-    for copy in copies[PIECES:]:
+    half = PIECES // 2 * depth
+    for copy in copies[PIECES : PIECES + PIECES // 2]:
         copy.wait()
-    values_of(normed, held_value[...], values)
+    raw = jnp.dot(normed[:, :half], held_value[:half, :], preferred_element_type=jnp.float32)
+    for copy in copies[PIECES + PIECES // 2 :]:
+        copy.wait()
+    raw += jnp.dot(normed[:, half:], held_value[half:, :], preferred_element_type=jnp.float32)
+    values[...] = raw.astype(jnp.bfloat16)
 
 
 def source_kernel(layer, source, gain, w_key, w_value, keys, values):

time: 51.4 us -> 51.4 us (level)
  no operation moved by 1% of the time
where the time goes in v10:
time: 51.4 us; the launch traced here: 51.1 us
  blocking collectives  25.8 us (50%)
  starting transfers between devices  12.1 us (24%)
  Pallas kernels  9.95 us (19%)
  waiting for transfers between devices  3.05 us (6%)
    all_to_all x3, blocking collectives, exchange(): return lax.all_to_all(blocks, 'sp', 0, 0, axis_index_groups=[order])  25.8 us
    all_to_all x1, starting transfers between devices, exchange(): return lax.all_to_all(blocks, 'sp', 0, 0, axis_index_groups=[order])  8.32 us
    ppermute x6, starting transfers between devices, over_groups(): lax.ppermute(share, 'tp', [(i, (i ^ m) % count) for i in range(count)])  3.78 us
    pallas_call x1, Pallas kernels, source_side(): pl.pallas_call(functools.partial(streaming_source_kernel, layer), in_spec...  3.16 us
    ppermute x6, waiting for transfers between devices, over_groups(): lax.ppermute(share, 'tp', [(i, (i ^ m) % count) for i in range(count)])  2.88 us
    pallas_call x1, Pallas kernels, first_queries(): pl.pallas_call(functools.partial(first_kernel, layer), in_specs=[IN_PLACE...  2.6 us
    pallas_call x1, Pallas kernels, source_side(): pl.pallas_call(functools.partial(source_kernel, layer), grid=(1,), in_spe...  1.47 us
  transfers between devices with their start and end apart: 7, of which 5 were waited for; matrix products, arithmetic and copies ran while one was open for 0% of the time, Pallas kernels for 9%

profile of v10, /device:TPU:0, one launch (start us, length us, event | category | flops | bytes accessed | tf_op | source)
XLA Modules:
  0.0 51.1 jit_solution(11651412179748088687)
XLA Ops:
  0.0 2.6 %first_queries.1 = bf16[8,8,512]{2,1,0:T(8,128)(2,1)} custom-call(bf16[7,2048]{1,0:T(8,128)(2,1)} %hidden.3, f32[2,2048]{1,0:T(2,128)} %gain.7, bf16[2,2048,512]{2,1,0:T(8,128)(2,1)} %w_query.3), custom_call_target="tpu_custom_call" | custom-call | flops 16777216 | bytes 2097152 | tf_op jit(solution)/shard_map/first_queries/pallas_call | solution.py:191
  2.6 8.3 %all-to-all-start = ((bf16[8,8,512]{2,1,0:T(8,128)(2,1)}), bf16[8,8,512]{2,1,0:T(8,128)(2,1)S(1)}, u32[]{:S(2)}, u32[]{:S(2)}) async-start(bf16[8,8,512]{2,1,0:T(8,128)(2,1)} %first_queries.1), calls=%async_computation | async-start | bytes 131072 | tf_op jit(solution)/shard_map/all_to_all | solution.py:352
  10.9 0.0 copy-done.6
  10.9 0.0 copy-done.4
  10.9 0.0 copy-start.8
  11.0 3.2 %source_side.2 = (bf16[256,512]{1,0:T(8,128)(2,1)S(1)}, bf16[256,512]{1,0:T(8,128)(2,1)S(1)}) custom-call(bf16[256,2048]{1,0:T(8,128)(2,1)S(1)} %copy-done.4, f32[2,2048]{1,0:T(2,128)S(1)} %copy-done.6, bf16[2,2048,512]{2,1,0:T(8,128)(2,1)} %w_key.3, bf16[2,2048,512]{2,1,0:T(8,128)(2,1)} %w_value.3), custom_call_target="tpu_custom_call" | custom-call | flops 1073741824 | bytes 4194304 | tf_op jit(solution)/shard_map/source_side/pallas_call | solution.py:97
  14.1 0.2 all-to-all-done.queries
  14.3 0.0 copy-done.8
  14.3 0.4 attend.2
  14.7 0.0 copy-start
  14.7 8.9 %all_to_all.20.packed = bf16[8,8,512]{2,1,0:T(8,128)(2,1)S(1)} all-to-all(bf16[8,8,512]{2,1,0:T(8,128)(2,1)S(1)} %attend.2), channel_id=1, replica_groups={{20,28,16,12,24,8,4,0},{21,29,17,13,25,9,5,1},{22,30,18,14,26,10,6,2},{..., dimensions={0} | all-to-all | bytes 131072 | tf_op jit(solution)/shard_map/all_to_all | solution.py:352
  23.6 0.0 copy-done.3
  23.6 0.4 share.2.rest_0_
  24.1 0.1 collective-permute-start.2
  24.1 1.6 %collective-permute-start.1 = (bf16[8,2048]{1,0:T(8,128)(2,1)S(1)}, bf16[8,2048]{1,0:T(8,128)(2,1)S(1)}, u32[]{:S(2)}, u32[]{:S(2)}) collective-permute-start(bf16[8,2048]{1,0:T(8,128)(2,1)S(1)} %share.2.rest_0_), channel_id=1, source_target_pairs={{0,2},{1,3},{2,0},{3,1},{4,6},{5,7},{6,4},{7,5},{8,10},{9,11},{10,... | collective-permute-start | bytes 98312 | tf_op jit(solution)/shard_map/ppermute | solution.py:358
  25.7 0.3 collective-permute-start
  26.0 1.5 %source_side.3 = (bf16[256,512]{1,0:T(8,128)(2,1)S(1)}, bf16[256,512]{1,0:T(8,128)(2,1)S(1)}) custom-call(bf16[256,2048]{1,0:T(8,128)(2,1)S(1)} %copy-done.4, f32[2,2048]{1,0:T(2,128)S(1)} %copy-done.6, bf16[2,2048,512]{2,1,0:T(8,128)(2,1)S(1)} %copy-done, bf16[2,2048,512]{2,1,0:T(8,128)(2,1)S(1)} %copy-done.1), custom_call_target="tpu_custom_call" | custom-call | flops 1073741824 | bytes 4194304 | tf_op jit(solution)/shard_map/source_side/pallas_call | solution.py:110
  27.5 0.3 collective-permute-done.2.rest_3_
  27.8 0.4 collective-permute-done.1.rest_2_
  28.2 0.0 collective-permute-done.rest_1_
  28.2 0.5 next_queries.1
  28.7 8.5 %all_to_all.21.queries = bf16[8,8,512]{2,1,0:T(8,128)(2,1)S(1)} all-to-all(bf16[8,8,512]{2,1,0:T(8,128)(2,1)S(1)} %get-tuple-element.30), channel_id=1, replica_groups={{20,28,16,12,24,8,4,0},{21,29,17,13,25,9,5,1},{22,30,18,14,26,10,6,2},{..., dimensions={0} | all-to-all | bytes 131072 | tf_op jit(solution)/shard_map/all_to_all | solution.py:352
  37.1 0.4 attend.3
  37.5 8.5 %all_to_all.22.packed = bf16[8,8,512]{2,1,0:T(8,128)(2,1)S(1)} all-to-all(bf16[8,8,512]{2,1,0:T(8,128)(2,1)S(1)} %attend.3), channel_id=1, replica_groups={{20,28,16,12,24,8,4,0},{21,29,17,13,25,9,5,1},{22,30,18,14,26,10,6,2},{..., dimensions={0} | all-to-all | bytes 131072 | tf_op jit(solution)/shard_map/all_to_all | solution.py:352
  46.0 0.4 share.3.rest_0_
  46.4 0.0 collective-permute-start.5
  46.4 1.6 %collective-permute-start.4 = (bf16[8,2048]{1,0:T(8,128)(2,1)S(1)}, bf16[8,2048]{1,0:T(8,128)(2,1)S(1)}, u32[]{:S(2)}, u32[]{:S(2)}) collective-permute-start(bf16[8,2048]{1,0:T(8,128)(2,1)S(1)} %share.3.rest_0_), channel_id=1, source_target_pairs={{0,2},{1,3},{2,0},{3,1},{4,6},{5,7},{6,4},{7,5},{8,10},{9,11},{10,... | collective-permute-start | bytes 98312 | tf_op jit(solution)/shard_map/ppermute | solution.py:358
  48.0 0.3 collective-permute-start.3
  48.3 1.8 %collective-permute-done.5.rest_3_ = bf16[8,2048]{1,0:T(8,128)(2,1)S(1)} collective-permute-done((bf16[8,2048]{1,0:T(8,128)(2,1)S(1)}, bf16[8,2048]{1,0:T(8,128)(2,1)S(1)}, u32[]{:S(2)}, u32[]{:S(2)}) %collective-permute-start.5) | collective-permute-done | bytes 32800 | tf_op jit(solution)/shard_map/ppermute | solution.py:358
  50.1 0.4 collective-permute-done.4.rest_2_
  50.5 0.0 collective-permute-done.3.rest_1_
  50.5 0.6 %last_rows.1 = bf16[7,2048]{1,0:T(8,128)(2,1)} custom-call(bf16[7,2048]{1,0:T(8,128)(2,1)S(1)} %get-tuple-element.29.hidden, bf16[8,2048]{1,0:T(8,128)(2,1)S(1)} %share.3.rest_0_, bf16[8,2048]{1,0:T(8,128)(2,1)S(1)} %collective-permute-done.3.rest_1_, bf16[8,2048]{1,0:T(8,128)(2,1)S(1)} %collective-permute-done.4.rest_2_, ...), custom_call_target="tpu_custom_call" | custom-call | tf_op jit(solution)/shard_map/last_rows/pallas_call | solution.py:231
  (12 shorter events, 0.0 us)
Async XLA Ops:
  0.0 10.9 %copy-start.6 = (f32[2,2048]{1,0:T(2,128)S(1)}, f32[2,2048]{1,0:T(2,128)}, u32[]{:S(2)}) copy-start(f32[2,2048]{1,0:T(2,128)} %gain.6) | copy-start | bytes 49156
  0.0 10.9 %copy-start.4 = (bf16[256,2048]{1,0:T(8,128)(2,1)S(1)}, bf16[256,2048]{1,0:T(8,128)(2,1)}, u32[]{:S(2)}) copy-start(bf16[256,2048]{1,0:T(8,128)(2,1)} %source.2) | copy-start | bytes 3145732
  2.6 11.7 %all-to-all-start = ((bf16[8,8,512]{2,1,0:T(8,128)(2,1)}), bf16[8,8,512]{2,1,0:T(8,128)(2,1)S(1)}, u32[]{:S(2)}, u32[]{:S(2)}) async-start(bf16[8,8,512]{2,1,0:T(8,128)(2,1)} %first_queries.1), calls=%async_computation | async-start | bytes 131072 | tf_op jit(solution)/shard_map/all_to_all | solution.py:352
  10.9 3.4 %copy-start.8 = (f32[2,2]{1,0:T(2,128)S(1)}, f32[2,2]{1,0:T(2,128)}, u32[]{:S(2)}) copy-start(f32[2,2]{1,0:T(2,128)} %scales.3) | copy-start | bytes 52
  14.3 9.3 %copy-start.3 = (bf16[2,512,2048]{2,1,0:T(8,128)(2,1)S(1)}, bf16[2,512,2048]{2,1,0:T(8,128)(2,1)}, u32[]{:S(2)}) copy-start(bf16[2,512,2048]{2,1,0:T(8,128)(2,1)} %w_out.3) | copy-start | bytes 12582916
  14.3 11.7 %copy-start.1 = (bf16[2,2048,512]{2,1,0:T(8,128)(2,1)S(1)}, bf16[2,2048,512]{2,1,0:T(8,128)(2,1)}, u32[]{:S(2)}) copy-start(bf16[2,2048,512]{2,1,0:T(8,128)(2,1)} %w_value.3) | copy-start | bytes 12582916
  14.7 11.3 %copy-start = (bf16[2,2048,512]{2,1,0:T(8,128)(2,1)S(1)}, bf16[2,2048,512]{2,1,0:T(8,128)(2,1)}, u32[]{:S(2)}) copy-start(bf16[2,2048,512]{2,1,0:T(8,128)(2,1)} %w_key.3) | copy-start | bytes 12582916
  24.0 4.1 %copy-start.2 = (bf16[2,2048,512]{2,1,0:T(8,128)(2,1)S(1)}, bf16[2,2048,512]{2,1,0:T(8,128)(2,1)}, u32[]{:S(2)}) copy-start(bf16[2,2048,512]{2,1,0:T(8,128)(2,1)} %w_query.3) | copy-start | bytes 12582916
  24.1 4.1 %copy-start.5 = (bf16[7,2048]{1,0:T(8,128)(2,1)S(1)}, bf16[7,2048]{1,0:T(8,128)(2,1)}, u32[]{:S(2)}) copy-start(bf16[7,2048]{1,0:T(8,128)(2,1)} %hidden.3) | copy-start | bytes 86020
  24.1 4.1 %copy-start.7 = (f32[2,2048]{1,0:T(2,128)S(1)}, f32[2,2048]{1,0:T(2,128)}, u32[]{:S(2)}) copy-start(f32[2,2048]{1,0:T(2,128)} %gain.7) | copy-start | bytes 49156
  24.1 3.7 %collective-permute-start.2 = (bf16[8,2048]{1,0:T(8,128)(2,1)S(1)}, bf16[8,2048]{1,0:T(8,128)(2,1)S(1)}, u32[]{:S(2)}, u32[]{:S(2)}) collective-permute-start(bf16[8,2048]{1,0:T(8,128)(2,1)S(1)} %share.2.rest_0_), channel_id=1, source_target_pairs={{0,3},{1,2},{2,1},{3,0},{4,7},{5,6},{6,5},{7,4},{8,11},{9,10},{10,... | collective-permute-start | bytes 98312 | tf_op jit(solution)/shard_map/ppermute | solution.py:358
  24.1 4.0 %collective-permute-start.1 = (bf16[8,2048]{1,0:T(8,128)(2,1)S(1)}, bf16[8,2048]{1,0:T(8,128)(2,1)S(1)}, u32[]{:S(2)}, u32[]{:S(2)}) collective-permute-start(bf16[8,2048]{1,0:T(8,128)(2,1)S(1)} %share.2.rest_0_), channel_id=1, source_target_pairs={{0,2},{1,3},{2,0},{3,1},{4,6},{5,7},{6,4},{7,5},{8,10},{9,11},{10,... | collective-permute-start | bytes 98312 | tf_op jit(solution)/shard_map/ppermute | solution.py:358
  25.7 2.5 %collective-permute-start = (bf16[8,2048]{1,0:T(8,128)(2,1)S(1)}, bf16[8,2048]{1,0:T(8,128)(2,1)S(1)}, u32[]{:S(2)}, u32[]{:S(2)}) collective-permute-start(bf16[8,2048]{1,0:T(8,128)(2,1)S(1)} %share.2.rest_0_), channel_id=1, source_target_pairs={{0,1},{1,0},{2,3},{3,2},{4,5},{5,4},{6,7},{7,6},{8,9},{9,8},{10,11... | collective-permute-start | bytes 98312 | tf_op jit(solution)/shard_map/ppermute | solution.py:358
  46.4 3.7 %collective-permute-start.5 = (bf16[8,2048]{1,0:T(8,128)(2,1)S(1)}, bf16[8,2048]{1,0:T(8,128)(2,1)S(1)}, u32[]{:S(2)}, u32[]{:S(2)}) collective-permute-start(bf16[8,2048]{1,0:T(8,128)(2,1)S(1)} %share.3.rest_0_), channel_id=1, source_target_pairs={{0,3},{1,2},{2,1},{3,0},{4,7},{5,6},{6,5},{7,4},{8,11},{9,10},{10,... | collective-permute-start | bytes 98312 | tf_op jit(solution)/shard_map/ppermute | solution.py:358
  46.4 4.0 %collective-permute-start.4 = (bf16[8,2048]{1,0:T(8,128)(2,1)S(1)}, bf16[8,2048]{1,0:T(8,128)(2,1)S(1)}, u32[]{:S(2)}, u32[]{:S(2)}) collective-permute-start(bf16[8,2048]{1,0:T(8,128)(2,1)S(1)} %share.3.rest_0_), channel_id=1, source_target_pairs={{0,2},{1,3},{2,0},{3,1},{4,6},{5,7},{6,4},{7,5},{8,10},{9,11},{10,... | collective-permute-start | bytes 98312 | tf_op jit(solution)/shard_map/ppermute | solution.py:358
  48.0 2.5 %collective-permute-start.3 = (bf16[8,2048]{1,0:T(8,128)(2,1)S(1)}, bf16[8,2048]{1,0:T(8,128)(2,1)S(1)}, u32[]{:S(2)}, u32[]{:S(2)}) collective-permute-start(bf16[8,2048]{1,0:T(8,128)(2,1)S(1)} %share.3.rest_0_), channel_id=1, source_target_pairs={{0,1},{1,0},{2,3},{3,2},{4,5},{5,4},{6,7},{7,6},{8,9},{9,8},{10,11... | collective-permute-start | bytes 98312 | tf_op jit(solution)/shard_map/ppermute | solution.py:358
